TPU v7x, 128 devices: a whole 4x4x4 slice. The times are simulated.
128 devices in a mesh: sp: 16 (over z, y), dp: 8 (over x, core).
Axes of the slice: x: 4, y: 4, z: 4, core: 2. Of those that a mesh axis runs over, the one named last changes fastest.
Arguments:
- layer_input: bfloat16 [8, 2048, 2048], P('dp', 'sp'), may hold values from -0.0390625 to 0.0390625
- queries: bfloat16 [8, 2048, 2048], P('dp', 'sp'), may hold values from -6 to 6
- key_vectors: bfloat16 [8, 2048, 2048], P('dp', 'sp'), may hold values from -6 to 6
- values: bfloat16 [8, 2048, 4096], P('dp', 'sp'), may hold values from -6 to 6
- cotangent: bfloat16 [8, 2048, 4096], P('dp', 'sp'), may hold values from -0.3125 to 0.3125
- log_decay: float32 [8, 16, 2048], P('dp', 'sp'), may hold values from -3 to 0
- key_weight: bfloat16 [2048, 2048], P('dp'), may hold values from -0.125 to 0.125
Outputs:
- grad_query: bfloat16 [8, 2048, 2048], P('dp', 'sp')
- grad_value: bfloat16 [8, 2048, 4096], P('dp', 'sp')
- grad_input: bfloat16 [8, 2048, 2048], P('dp', 'sp')
- grad_key_weight: float32 [2048, 2048], P('dp')
All inputs are finite; a program needn't handle non-finite values.
Results may differ from a plain program's by a relative error of at most 0.012.
Values may be sent and summed in bfloat16 or wider, within the bound.
No kernel may reach another device: no remote copies, remote signals or barrier semaphores. Data moves between devices by JAX's collectives and lax.ppermute only.
A program may use at most 128 MiB of HBM per device.

v0:
```python
import jax
import jax.numpy as jnp
from jax import lax
from jax.experimental import pallas as pl
from jax.experimental.pallas import tpu as pltpu
from jax.sharding import Mesh
from jax.sharding import PartitionSpec as P

HEADS = 8
BLOCK = 128
TILE = 256
SP = ("half", "lane")
DP = ("dp_0", "dp_1")
F32 = jnp.float32
BF16 = jnp.bfloat16


def dot(a, b, dims, precision=None):
    return lax.dot_general(a, b, (dims, ((), ())), precision=precision, preferred_element_type=F32)


NN = ((1,), (0,))
NT = ((1,), (1,))
TN = ((0,), (0,))


def decay_kernel(lam_ref, half_ref, rows_ref, cols_ref):
    n = BLOCK
    row = lax.broadcasted_iota(jnp.int32, (n, n), 0)
    col = lax.broadcasted_iota(jnp.int32, (n, n), 1)
    lam = lam_ref[...]
    high = lax.Precision.HIGHEST
    upto = dot(lam, (row <= col).astype(F32), NN, high)
    before = dot(lam, (row < col).astype(F32), NN, high)
    since = dot(lam, (row >= col).astype(F32), NN, high)
    after = dot(lam, (row > col).astype(F32), NN, high)
    totals = [jnp.broadcast_to(upto[b : b + 1, n - 1 : n], (1, n)) for b in range(16)]
    loc0, suf1, rem0, pre1 = [], [], [], []
    for b in range(8):
        odd = b % 2 == 1
        loc0.append(upto[b : b + 1] + totals[b - 1] if odd else upto[b : b + 1])
        suf1.append(since[8 + b : 9 + b] if odd else since[8 + b : 9 + b] + totals[9 + b])
        rem0.append(after[b : b + 1] if odd else after[b : b + 1] + totals[b + 1])
        pre1.append(before[8 + b : 9 + b] + totals[7 + b] if odd else before[8 + b : 9 + b])
    tile0 = [totals[2 * t] + totals[2 * t + 1] for t in range(4)]
    tile1 = [totals[8 + 2 * t] + totals[9 + 2 * t] for t in range(4)]
    first = half_ref[...] == 0
    key_sum, query_sum = [], []
    for b in range(8):
        t = b // 2
        later0, later1 = sum(tile0[t + 1 :]), sum(tile1[t + 1 :])
        early0, early1 = sum(tile0[:t]), sum(tile1[:t])
        key_sum.append(jnp.where(first, rem0[b] + later0, pre1[b] + early1))
        query_sum.append(jnp.where(first, suf1[b] + later1, loc0[b] + early0))
    rows_ref[...] = jnp.concatenate(loc0 + suf1 + rem0 + pre1 + tile0 + tile1, axis=0)
    keys = jnp.exp(jnp.concatenate(key_sum, axis=0))
    queries = jnp.exp(jnp.concatenate(query_sum, axis=0)) * 0.0625
    stack = [jnp.concatenate(loc0 + suf1, axis=0), keys, queries, jnp.zeros((n - 32, n), F32)]
    cols_ref[...] = jnp.transpose(jnp.concatenate(stack, axis=0))


def tall(cols, base, block_pair=None):
    picks = range(8) if block_pair is None else (2 * block_pair, 2 * block_pair + 1)
    return jnp.concatenate([cols[:, base + b : base + b + 1] for b in picks], axis=0)


def wide(rows, base, t):
    return jnp.concatenate([rows[base + 2 * t : base + 2 * t + 1], rows[base + 2 * t + 1 : base + 2 * t + 2]], axis=1)


def boundary_kernel(units_ref, cols_ref, state_ref, keys_ref):
    cols = cols_ref[...]
    keys = (units_ref[:, 256:512].astype(F32) * tall(cols, 16)).astype(BF16)
    queries = (units_ref[:, 0:256].astype(F32) * tall(cols, 24)).astype(BF16)
    keys_ref[...] = keys
    state_ref[0] = dot(keys, units_ref[:, 512:1024], TN).astype(BF16)
    state_ref[1] = dot(queries, units_ref[:, 1024:1536], TN).astype(BF16)


def inside_kernel(units_ref, rows_ref, cols_ref, out_ref, s_ref, gs_ref):
    rows, cols = rows_ref[...], cols_ref[...]
    row = lax.broadcasted_iota(jnp.int32, (TILE, TILE), 0)
    col = lax.broadcasted_iota(jnp.int32, (TILE, TILE), 1)
    for i in range(4):
        at = pl.ds(i * TILE, TILE)
        query, grad = units_ref[at, 0:256], units_ref[at, 1024:1536]
        loc0, suf1 = tall(cols, 0, i), tall(cols, 8, i)
        for j in range(4):
            to = pl.ds(j * TILE, TILE)
            if i == j:
                spread = jnp.where(row >= col, loc0 - wide(rows, 0, i), suf1 - wide(rows, 8, i))
            elif i > j:
                along = wide(rows, 16, j)
                for t in range(j + 1, i):
                    along = along + jnp.concatenate([rows[32 + t : 33 + t]] * 2, axis=1)
                spread = loc0 + along
            else:
                along = wide(rows, 24, j)
                for t in range(i + 1, j):
                    along = along + jnp.concatenate([rows[36 + t : 37 + t]] * 2, axis=1)
                spread = suf1 + along
            weights = jnp.exp(spread) * 0.0625
            scores = dot(query, units_ref[to, 256:512], NT)
            grads = dot(grad, units_ref[to, 512:1024], NT)
            s_ref[at, to] = (scores * weights).astype(BF16)
            gs_ref[at, to] = (grads * weights).astype(BF16)
    out_ref[:, 0:256] = dot(gs_ref[...], units_ref[:, 0:256], TN)
    out_ref[:, 256:512] = dot(gs_ref[...], units_ref[:, 256:512], NN)
    out_ref[:, 512:1024] = dot(s_ref[...], units_ref[:, 1024:1536], TN)


def across_kernel(units_ref, cols_ref, keys_ref, state_ref, part_ref, out_ref):
    cols = cols_ref[...]
    memory, later = state_ref[0], state_ref[1]
    key_part = dot(units_ref[:, 512:1024], later, NT) * tall(cols, 16)
    out_ref[:, 0:256] = (part_ref[:, 0:256] + key_part).astype(BF16)
    query_part = dot(units_ref[:, 1024:1536], memory, NT) * tall(cols, 24)
    out_ref[:, 256:512] = (part_ref[:, 256:512] + query_part).astype(BF16)
    value_part = dot(keys_ref[...], later, NN)
    out_ref[:, 512:1024] = (part_ref[:, 512:1024] + value_part).astype(BF16)


def kernel(body, out_shape, flops, scratch=()):
    return pl.pallas_call(
        body,
        out_shape=out_shape,
        scratch_shapes=scratch,
        cost_estimate=pl.CostEstimate(flops=flops, bytes_accessed=4 << 20, transcendentals=0),
        compiler_params=pltpu.CompilerParams(vmem_limit_bytes=48 << 20),
    )


def shape(dims, dtype):
    return jax.ShapeDtypeStruct(dims, dtype)


def shards(layer_input, queries, key_vectors, values, cotangent, log_decay, key_weight):
    tokens = layer_input.shape[1]
    half = lax.axis_index("half")
    peers = lax.axis_size(SP)
    weight = lax.all_gather(key_weight, DP, tiled=True)

    decay = log_decay.reshape(2, 8, BLOCK)
    own = lax.axis_index("lane") % 2
    near = lax.dynamic_index_in_dim(decay, own, 0, keepdims=False)
    far = lax.dynamic_index_in_dim(decay, 1 - own, 0, keepdims=False)
    near = lax.ppermute(near, SP, [(u, u % 2 * 8 + u // 2) for u in range(peers)])
    far = lax.ppermute(far, SP, [(u, (1 - u % 2) * 8 + u // 2) for u in range(peers)])
    lam = jnp.where(half == 0, jnp.concatenate([near, far]), jnp.concatenate([far, near]))
    rows, cols = kernel(decay_kernel, (shape((40, 128), F32), shape((128, 128), F32)), 1 << 20)(
        lam, jnp.full((1, 128), half, jnp.int32)
    )

    def by_head(array):
        return jnp.moveaxis(array[0].reshape(tokens, HEADS, -1), 1, 0)

    sent = jnp.concatenate([by_head(a) for a in (queries, key_vectors, values, cotangent)], axis=2)
    units = lax.all_to_all(sent, "lane", 0, 0, tiled=True).reshape(8 * tokens, -1)
    gathered = lax.all_gather(layer_input[0], "lane", tiled=True)

    state, keys = kernel(
        boundary_kernel, (shape((2, 256, 512), BF16), shape((1024, 256), BF16)), 540 << 20
    )(units, cols)
    state = lax.ppermute(state, SP, [(u, (u + 8) % 16) for u in range(peers)])
    part = kernel(
        inside_kernel,
        shape((1024, 1024), F32),
        3760 << 20,
        (pltpu.VMEM((1024, 1024), BF16), pltpu.VMEM((1024, 1024), BF16)),
    )(units, rows, cols)
    grads = kernel(across_kernel, shape((1024, 1024), BF16), 800 << 20)(
        units, cols, keys, state, part
    )

    home = lax.all_to_all(grads.reshape(8, tokens, -1), "lane", 0, 0, tiled=True)

    def to_rows(array):
        return jnp.moveaxis(array, 0, 1).reshape(tokens, -1)

    grad_key = to_rows(home[:, :, 0:256])
    grad_query = to_rows(home[:, :, 256:512])
    grad_value = to_rows(home[:, :, 512:1024])
    grad_input = dot(grad_key, weight, NT).astype(BF16)

    terms = dot(gathered, grads[:, 0:256], TN).astype(BF16)
    group = DP + ("half",)
    terms = terms.reshape(lax.axis_size(group), -1, 256)
    terms = lax.all_to_all(terms, group, 0, 0, tiled=True)
    total = jnp.sum(terms.astype(F32), axis=0).astype(BF16)
    span = total.shape[0]
    spread = jnp.broadcast_to(total[None], (peers, span, 256))
    spread = lax.all_to_all(spread, SP, 0, 0, tiled=True)
    grad_weight = jnp.moveaxis(spread.reshape(2, 8, span, 256), 1, 2).reshape(2 * span, -1)
    return grad_query[None], grad_value[None], grad_input[None], grad_weight.astype(F32)


def solution(mesh):
    dp = mesh.shape["dp"]
    outer = (dp // 2, 2) if dp > 1 else (1, 1)
    finer = Mesh(mesh.devices.reshape(2, 8, *outer), SP + DP)
    part = P(DP, SP, None)
    return jax.shard_map(
        shards,
        mesh=finer,
        in_specs=(part, part, part, part, part, part, P(DP, None)),
        out_specs=(part, part, part, P(DP, None)),
        check_vma=False,
    )
```

profile of v0, /device:TPU:1, one launch (start us, length us, event | category | flops | bytes accessed | tf_op | source)
XLA Modules:
  0.0 241.6 jit_solution(4708464847869016365)
XLA Ops:
  7.2 0.0 copy-start.2
  7.2 0.0 all-gather.6.cloned.1.call-start
  7.2 0.7 all-gather.6.cloned.1.call-update
  7.9 0.0 all-gather.4.cloned.1.call-start
  8.0 0.7 all-gather.4.cloned.1.call-update
  8.7 1.6 copy.48
  10.3 0.0 copy-done.2
  10.3 0.4 copy.47
  10.7 0.0 copy-done.3
  10.7 0.1 copy.46
  10.8 0.1 copy.45
  11.0 0.2 copy_bitcast_fusion.3
  11.2 0.7 copy_bitcast_fusion.1
  11.9 1.8 pad_maximum_fusion
  13.7 6.5 %all-to-all-start = ((bf16[8,128,1536]{2,1,0:T(8,128)(2,1)}), bf16[8,128,1536]{2,1,0:T(8,128)(2,1)S(1)}, u32[]{:S(2)}, u32[]{:S(2)}) async-start(bf16[8,128,1536]{2,1,0:T(8,128)(2,1)} %pad_maximum_fusion), calls=%async_computation | async-start | bytes 6291456 | tf_op jit(solution)/shard_map/all_to_all | solution.py:158
  20.2 3.4 %collective-permute-start.1 = (f32[8,128]{1,0:T(8,128)S(1)}, f32[8,128]{1,0:T(8,128)S(1)}, u32[]{:S(2)}, u32[]{:S(2)}) collective-permute-start(f32[8,128]{1,0:T(8,128)S(1)} %get-tuple-element.27), channel_id=1, source_target_pairs={{0,64},{8,0},{16,72},{24,8},{32,80},{40,16},{48,88},{56,24},{64,96... | collective-permute-start | bytes 12296 | tf_op jit(solution)/shard_map/ppermute | solution.py:148
  23.6 0.6 collective-permute-start
  24.2 56.4 %collective-permute-done.1 = f32[8,128]{1,0:T(8,128)S(1)} collective-permute-done((f32[8,128]{1,0:T(8,128)S(1)}, f32[8,128]{1,0:T(8,128)S(1)}, u32[]{:S(2)}, u32[]{:S(2)}) %collective-permute-start.1) | collective-permute-done | bytes 4128 | tf_op jit(solution)/shard_map/ppermute | solution.py:148
  80.7 0.0 collective-permute-done
  80.7 0.4 shard_map.102
  81.1 0.0 all-to-all-done
  81.2 1.5 shard_map.103
  82.6 2.5 %collective-permute-start.2 = (bf16[2,256,512]{2,1,0:T(8,128)(2,1)S(1)}, bf16[2,256,512]{2,1,0:T(8,128)(2,1)S(1)}, u32[]{:S(2)}, u32[]{:S(2)}) collective-permute-start(bf16[2,256,512]{2,1,0:T(8,128)(2,1)S(1)} %get-tuple-element.10), channel_id=1, source_target_pairs={{0,64},{8,72},{16,80},{24,88},{32,96},{40,104},{48,112},{56,120},{... | collective-permute-start | bytes 1572872 | tf_op jit(solution)/shard_map/ppermute | solution.py:164
  85.2 6.2 %shard_map.104.part_ref = f32[1024,1024]{1,0:T(8,128)} custom-call(bf16[1024,1536]{1,0:T(8,128)(2,1)S(1)} %bitcast.61, f32[40,128]{1,0:T(8,128)S(1)} %get-tuple-element.11.rows_ref, f32[128,128]{1,0:T(8,128)S(1)} %get-tuple-element.8.cols_ref), custom_call_target="tpu_custom_call" | custom-call | flops 3942645760 | bytes 4194304 | tf_op jit(solution)/shard_map/pallas_call | solution.py:165
  91.3 26.2 %collective-permute-done.2.state_ref = bf16[2,256,512]{2,1,0:T(8,128)(2,1)S(1)} collective-permute-done((bf16[2,256,512]{2,1,0:T(8,128)(2,1)S(1)}, bf16[2,256,512]{2,1,0:T(8,128)(2,1)S(1)}, u32[]{:S(2)}, u32[]{:S(2)}) %collective-permute-start.2) | collective-permute-done | bytes 524320 | tf_op jit(solution)/shard_map/ppermute | solution.py:164
  117.5 4.2 %shard_map.105 = bf16[1024,1024]{1,0:T(8,128)(2,1)S(1)} custom-call(bf16[1024,1536]{1,0:T(8,128)(2,1)} %bitcast.62, f32[128,128]{1,0:T(8,128)S(1)} %get-tuple-element.8.cols_ref, bf16[1024,256]{1,0:T(8,128)(2,1)S(1)} %get-tuple-element.9.keys_ref, bf16[2,256,512]{2,1,0:T(8,128)(2,1)S(1)} %collective-permute-done.2.state_ref, f32[1024,1024]{1,0:T(8,128)} %shard_map.104.part_ref), custom_call_target="tpu_custom_call" | custom-call | flops 838860800 | bytes 4194304 | tf_op jit(solution)/shard_map/pallas_call | solution.py:171
  121.7 0.0 all-gather.6.cloned.1.call-done
  121.7 3.9 %fusion.6 = bf16[32,16,8,128]{3,2,1,0:T(8,128)(2,1)S(1)} fusion(bf16[1,1024,2048]{2,1,0:T(8,128)(2,1)} %all-gather.6.cloned.1.call-done, bf16[1024,1024]{1,0:T(8,128)(2,1)S(1)} %shard_map.105), kind=kOutput, calls=%fused_computation.7 | convolution fusion | flops 1074266112 | bytes 5767168 | tf_op jit(solution)/shard_map/dot_general | solution.py:19
  125.6 1.2 copy.55
  126.9 7.7 %all-to-all-start.2 = ((bf16[16,128,256]{1,2,0:T(8,128)(2,1)}), bf16[16,128,256]{1,2,0:T(8,128)(2,1)S(1)}, u32[]{:S(2)}, u32[]{:S(2)}) async-start(bf16[16,128,256]{1,2,0:T(8,128)(2,1)} %bitcast.66), calls=%async_computation.2 | async-start | bytes 2097152 | tf_op jit(solution)/shard_map/all_to_all | solution.py:188
  134.5 2.4 copy.36
  136.9 26.9 %all-to-all-done.2 = bf16[16,128,256]{1,2,0:T(8,128)(2,1)S(1)} async-done(((bf16[16,128,256]{1,2,0:T(8,128)(2,1)}), bf16[16,128,256]{1,2,0:T(8,128)(2,1)S(1)}, u32[]{:S(2)}, u32[]{:S(2)}) %all-to-all-start.2) | async-done | bytes 1048608 | tf_op jit(solution)/shard_map/all_to_all | solution.py:188
  163.9 6.5 %all-to-all-start.1 = ((bf16[8,128,1024]{1,2,0:T(8,128)(2,1)}), bf16[8,128,1024]{1,2,0:T(8,128)(2,1)S(1)}, u32[]{:S(2)}, u32[]{:S(2)}) async-start(bf16[8,128,1024]{1,2,0:T(8,128)(2,1)} %copy.36), calls=%async_computation.1 | async-start | bytes 4194304 | tf_op jit(solution)/shard_map/all_to_all | solution.py:175
  170.3 0.1 reduce_sum.12
  170.5 0.1 copy.39
  170.6 25.7 %all-to-all-done.1 = bf16[8,128,1024]{1,2,0:T(8,128)(2,1)S(1)} async-done(((bf16[8,128,1024]{1,2,0:T(8,128)(2,1)}), bf16[8,128,1024]{1,2,0:T(8,128)(2,1)S(1)}, u32[]{:S(2)}, u32[]{:S(2)}) %all-to-all-start.1) | async-done | bytes 2097184 | tf_op jit(solution)/shard_map/all_to_all | solution.py:175
  196.3 1.2 broadcast_in_dim.14
  197.5 6.6 %all-to-all-start.3 = ((bf16[16,128,256]{2,1,0:T(8,128)(2,1)}), bf16[16,128,256]{2,1,0:T(8,128)(2,1)S(1)}, u32[]{:S(2)}, u32[]{:S(2)}) async-start(bf16[16,128,256]{2,1,0:T(8,128)(2,1)} %broadcast_in_dim.14), calls=%async_computation.3 | async-start | bytes 2097152 | tf_op jit(solution)/shard_map/all_to_all | solution.py:192
  204.1 1.0 fusion.10
  205.2 2.0 copy.41
  207.2 1.0 slice.17
  208.2 2.3 copy.42
  210.5 13.5 %all-to-all-done.3 = bf16[16,128,256]{2,1,0:T(8,128)(2,1)S(1)} async-done(((bf16[16,128,256]{2,1,0:T(8,128)(2,1)}), bf16[16,128,256]{2,1,0:T(8,128)(2,1)S(1)}, u32[]{:S(2)}, u32[]{:S(2)}) %all-to-all-start.3) | async-done | bytes 1048608 | tf_op jit(solution)/shard_map/all_to_all | solution.py:192
  224.0 0.2 convert_bitcast_fusion
  224.3 1.2 copy.40
  225.5 0.0 copy-start.1
  225.5 2.2 copy.49
  227.7 7.1 %fusion.5 = bf16[1,128,2048]{2,1,0:T(8,128)(2,1)} fusion(bf16[128,2048]{0,1:T(8,128)(2,1)S(1)} %bitcast.71, bf16[2048,2048]{1,0:T(8,128)(2,1)} %all-gather.4.cloned.1.call-done), kind=kOutput, calls=%fused_computation.5 | convolution fusion | flops 1074003968 | bytes 9437184 | tf_op jit(solution)/shard_map/dot_general | solution.py:19
  (12 shorter events, 0.0 us)
Async XLA Ops:
  7.2 3.1 %copy-start.2 = (bf16[1,128,4096]{2,1,0:T(8,128)(2,1)S(1)}, bf16[1,128,4096]{2,1,0:T(8,128)(2,1)}, u32[]{:S(2)}) copy-start(bf16[1,128,4096]{2,1,0:T(8,128)(2,1)} %param.10) | copy-start | bytes 3145732
  7.2 3.5 %copy-start.3 = (bf16[1,128,2048]{2,1,0:T(8,128)(2,1)S(1)}, bf16[1,128,2048]{2,1,0:T(8,128)(2,1)}, u32[]{:S(2)}) copy-start(bf16[1,128,2048]{2,1,0:T(8,128)(2,1)} %param.9) | copy-start | bytes 1572868
  7.2 114.5 %all-gather.6.cloned.1.call-start = ((), (), s32[]{:S(2)}) async-start(), calls=%async_computation.5 | async-start | bytes 4718592 | tf_op jit(solution)/shard_map/all_gather | solution.py:159
  7.9 2.9 %copy-start.4 = (bf16[1,128,2048]{2,1,0:T(8,128)(2,1)S(1)}, bf16[1,128,2048]{2,1,0:T(8,128)(2,1)}, u32[]{:S(2)}) copy-start(bf16[1,128,2048]{2,1,0:T(8,128)(2,1)} %param.8) | copy-start | bytes 1572868
  7.9 219.8 %all-gather.4.cloned.1.call-start = ((), (), s32[]{:S(2)}) async-start(), calls=%async_computation.4 | async-start | bytes 9437184 | tf_op jit(solution)/shard_map/all_gather | solution.py:141
  13.7 6.5 %copy-start.5 = (f32[1,1,2048]{2,1,0:T(1,128)S(1)}, f32[1,1,2048]{2,1,0:T(1,128)}, u32[]{:S(2)}) copy-start(f32[1,1,2048]{2,1,0:T(1,128)} %param.12) | copy-start | bytes 24580
  13.7 67.5 %all-to-all-start = ((bf16[8,128,1536]{2,1,0:T(8,128)(2,1)}), bf16[8,128,1536]{2,1,0:T(8,128)(2,1)S(1)}, u32[]{:S(2)}, u32[]{:S(2)}) async-start(bf16[8,128,1536]{2,1,0:T(8,128)(2,1)} %pad_maximum_fusion), calls=%async_computation | async-start | bytes 6291456 | tf_op jit(solution)/shard_map/all_to_all | solution.py:158
  20.2 60.5 %collective-permute-start.1 = (f32[8,128]{1,0:T(8,128)S(1)}, f32[8,128]{1,0:T(8,128)S(1)}, u32[]{:S(2)}, u32[]{:S(2)}) collective-permute-start(f32[8,128]{1,0:T(8,128)S(1)} %get-tuple-element.27), channel_id=1, source_target_pairs={{0,64},{8,0},{16,72},{24,8},{32,80},{40,16},{48,88},{56,24},{64,96... | collective-permute-start | bytes 12296 | tf_op jit(solution)/shard_map/ppermute | solution.py:148
  23.6 57.1 %collective-permute-start = (f32[8,128]{1,0:T(8,128)S(1)}, f32[8,128]{1,0:T(8,128)S(1)}, u32[]{:S(2)}, u32[]{:S(2)}) collective-permute-start(f32[8,128]{1,0:T(8,128)S(1)} %get-tuple-element.26), channel_id=1, source_target_pairs={{0,0},{8,64},{16,8},{24,72},{32,16},{40,80},{48,24},{56,88},{64,32... | collective-permute-start | bytes 12296 | tf_op jit(solution)/shard_map/ppermute | solution.py:147
  81.2 10.2 %copy-start = (bf16[8,128,1536]{2,1,0:T(8,128)(2,1)}, bf16[8,128,1536]{2,1,0:T(8,128)(2,1)S(1)}, u32[]{:S(2)}) copy-start(bf16[8,128,1536]{2,1,0:T(8,128)(2,1)S(1)} %all-to-all-done) | copy-start | bytes 9437188
  82.6 34.9 %collective-permute-start.2 = (bf16[2,256,512]{2,1,0:T(8,128)(2,1)S(1)}, bf16[2,256,512]{2,1,0:T(8,128)(2,1)S(1)}, u32[]{:S(2)}, u32[]{:S(2)}) collective-permute-start(bf16[2,256,512]{2,1,0:T(8,128)(2,1)S(1)} %get-tuple-element.10), channel_id=1, source_target_pairs={{0,64},{8,72},{16,80},{24,88},{32,96},{40,104},{48,112},{56,120},{... | collective-permute-start | bytes 1572872 | tf_op jit(solution)/shard_map/ppermute | solution.py:164
  126.9 37.0 %all-to-all-start.2 = ((bf16[16,128,256]{1,2,0:T(8,128)(2,1)}), bf16[16,128,256]{1,2,0:T(8,128)(2,1)S(1)}, u32[]{:S(2)}, u32[]{:S(2)}) async-start(bf16[16,128,256]{1,2,0:T(8,128)(2,1)} %bitcast.66), calls=%async_computation.2 | async-start | bytes 2097152 | tf_op jit(solution)/shard_map/all_to_all | solution.py:188
  163.9 32.5 %all-to-all-start.1 = ((bf16[8,128,1024]{1,2,0:T(8,128)(2,1)}), bf16[8,128,1024]{1,2,0:T(8,128)(2,1)S(1)}, u32[]{:S(2)}, u32[]{:S(2)}) async-start(bf16[8,128,1024]{1,2,0:T(8,128)(2,1)} %copy.36), calls=%async_computation.1 | async-start | bytes 4194304 | tf_op jit(solution)/shard_map/all_to_all | solution.py:175
  197.5 26.5 %all-to-all-start.3 = ((bf16[16,128,256]{2,1,0:T(8,128)(2,1)}), bf16[16,128,256]{2,1,0:T(8,128)(2,1)S(1)}, u32[]{:S(2)}, u32[]{:S(2)}) async-start(bf16[16,128,256]{2,1,0:T(8,128)(2,1)} %broadcast_in_dim.14), calls=%async_computation.3 | async-start | bytes 2097152 | tf_op jit(solution)/shard_map/all_to_all | solution.py:192
  225.5 2.2 copy-start.1
Sparse Core Ops, SparseCore 0:
  9.6 97.6 all-gather.5
  109.0 64.8 all-gather.3
where the time goes:
time: 242 us
  waiting for transfers between devices  150 us (62%)
  starting transfers between devices  33.9 us (14%)
  local copies, waits for them, and re-layouts  17.9 us (7%)
  between operations  14.3 us (6%)
  Pallas kernels  12.2 us (5%)
  matrix products  11 us (5%)
    ppermute x1, waiting for transfers between devices, shards(): lax.ppermute(far, SP, [(u, (1 - u % 2) * 8 + u // 2) for u in range(peers)])  56.4 us
    all_to_all x1, waiting for transfers between devices, shards(): terms = lax.all_to_all(terms, group, 0, 0, tiled=True)  26.9 us
    ppermute x1, waiting for transfers between devices, shards(): state = lax.ppermute(state, SP, [(u, (u + 8) % 16) for u in range(peers)])  26.2 us
    all_to_all x1, waiting for transfers between devices, shards(): lax.all_to_all(grads.reshape(8, tokens, -1), 'lane', 0, 0, tiled=True)  25.7 us
    all_to_all x1, waiting for transfers between devices, shards(): spread = lax.all_to_all(spread, SP, 0, 0, tiled=True)  13.5 us
    dot_general x2, matrix products, dot(): lax.dot_general(a, b, (dims, ((), ())), precision=precision, preferred_el...  11 us
    unnamed x19, local copies, waits for them, and re-layouts  8.77 us
    all_to_all x1, starting transfers between devices, shards(): terms = lax.all_to_all(terms, group, 0, 0, tiled=True)  7.66 us
  transfers between devices with their start and end apart: 9, of which 5 were waited for; matrix products, arithmetic and copies ran while one was open for 10% of the time, Pallas kernels for 5%

commit v1 on v0

--- a/solution.py
+++ b/solution.py
@@ -5,6 +5,7 @@
 from jax.experimental.pallas import tpu as pltpu
 from jax.sharding import Mesh
 from jax.sharding import PartitionSpec as P
+
 
 HEADS = 8
 BLOCK = 128
@@ -120,28 +121,78 @@
     out_ref[:, 512:1024] = (part_ref[:, 512:1024] + value_part).astype(BF16)
 
 
-def kernel(body, out_shape, flops, scratch=()):
+def kernel(body, out_shape, flops, scratch=(), **grid):
     return pl.pallas_call(
         body,
         out_shape=out_shape,
         scratch_shapes=scratch,
         cost_estimate=pl.CostEstimate(flops=flops, bytes_accessed=4 << 20, transcendentals=0),
         compiler_params=pltpu.CompilerParams(vmem_limit_bytes=48 << 20),
+        **grid,
     )
 
 
 def shape(dims, dtype):
     return jax.ShapeDtypeStruct(dims, dtype)
+
+
+def pack_kernel(query_ref, key_ref, value_ref, grad_ref, out_ref):
+    out_ref[0, :, 0:256] = query_ref[...]
+    out_ref[0, :, 256:512] = key_ref[...]
+    out_ref[0, :, 512:1024] = value_ref[...]
+    out_ref[0, :, 1024:1536] = grad_ref[...]
+
+
+def by_head(width):
+    return pl.BlockSpec((BLOCK, width), lambda h: (0, h))
+
+
+def term_kernel(lane_ref, grads_ref, own_ref, before_ref, after_ref, far_ref, out_ref):
+    lane = lane_ref[0]
+    deep, y = lane // 4, lane % 4
+    total = None
+    for pair, step in ((own_ref, 0), (before_ref, 3), (after_ref, 1), (far_ref, 2)):
+        for other in range(2):
+            block = (deep ^ other) * 4 + (y + step) % 4
+            grad = grads_ref[pl.ds(pl.multiple_of(block * BLOCK, BLOCK), BLOCK), 0:256]
+            part = dot(pair[other], grad, TN)
+            total = part if total is None else total + part
+    out_ref[...] = total.astype(BF16)
+
+
+def home_kernel(home_ref, weight_ref, query_ref, value_ref, input_ref, sum_ref):
+    query_ref[...] = home_ref[0, :, 256:512]
+    value_ref[...] = home_ref[0, :, 512:1024]
+    part = dot(home_ref[0, :, 0:256], weight_ref[...], NT)
+    first = pl.program_id(0) == 0
+
+    @pl.when(first)
+    def _():
+        sum_ref[...] = part
+
+    @pl.when(jnp.logical_not(first))
+    def _():
+        sum_ref[...] += part
+
+    @pl.when(pl.program_id(0) == pl.num_programs(0) - 1)
+    def _():
+        input_ref[...] = sum_ref[...].astype(BF16)
+
+
+def widen_kernel(in_ref, out_ref):
+    out_ref[...] = in_ref[0].astype(F32)
 
 
 def shards(layer_input, queries, key_vectors, values, cotangent, log_decay, key_weight):
     tokens = layer_input.shape[1]
     half = lax.axis_index("half")
+    lane = lax.axis_index("lane")
     peers = lax.axis_size(SP)
+    ring = lax.axis_size("dp_0")
     weight = lax.all_gather(key_weight, DP, tiled=True)
 
     decay = log_decay.reshape(2, 8, BLOCK)
-    own = lax.axis_index("lane") % 2
+    own = lane % 2
     near = lax.dynamic_index_in_dim(decay, own, 0, keepdims=False)
     far = lax.dynamic_index_in_dim(decay, 1 - own, 0, keepdims=False)
     near = lax.ppermute(near, SP, [(u, u % 2 * 8 + u // 2) for u in range(peers)])
@@ -151,12 +202,26 @@
         lam, jnp.full((1, 128), half, jnp.int32)
     )
 
-    def by_head(array):
-        return jnp.moveaxis(array[0].reshape(tokens, HEADS, -1), 1, 0)
-
-    sent = jnp.concatenate([by_head(a) for a in (queries, key_vectors, values, cotangent)], axis=2)
+    sent = kernel(
+        pack_kernel,
+        shape((8, tokens, 1536), BF16),
+        1 << 20,
+        grid=(HEADS,),
+        in_specs=[by_head(256), by_head(256), by_head(512), by_head(512)],
+        out_specs=pl.BlockSpec((1, tokens, 1536), lambda h: (h, 0, 0)),
+    )(queries[0], key_vectors[0], values[0], cotangent[0])
     units = lax.all_to_all(sent, "lane", 0, 0, tiled=True).reshape(8 * tokens, -1)
-    gathered = lax.all_gather(layer_input[0], "lane", tiled=True)
+
+    def lane_step(array, step):
+        return lax.ppermute(
+            array, "lane", [(i, i // 4 * 4 + (i + step) % 4) for i in range(8)]
+        )
+
+    across = lax.ppermute(layer_input, "lane", [(i, (i + 4) % 8) for i in range(8)])
+    pair = jnp.concatenate([layer_input, across])
+    pair, units = lax.optimization_barrier((pair, units))
+    before, after = lane_step(pair, 1), lane_step(pair, 3)
+    opposite = jnp.concatenate([lane_step(before[0:1], 1), lane_step(after[1:2], 3)])
 
     state, keys = kernel(
         boundary_kernel, (shape((2, 256, 512), BF16), shape((1024, 256), BF16)), 540 << 20
@@ -173,25 +238,60 @@
     )
 
     home = lax.all_to_all(grads.reshape(8, tokens, -1), "lane", 0, 0, tiled=True)
-
-    def to_rows(array):
-        return jnp.moveaxis(array, 0, 1).reshape(tokens, -1)
-
-    grad_key = to_rows(home[:, :, 0:256])
-    grad_query = to_rows(home[:, :, 256:512])
-    grad_value = to_rows(home[:, :, 512:1024])
-    grad_input = dot(grad_key, weight, NT).astype(BF16)
-
-    terms = dot(gathered, grads[:, 0:256], TN).astype(BF16)
-    group = DP + ("half",)
-    terms = terms.reshape(lax.axis_size(group), -1, 256)
-    terms = lax.all_to_all(terms, group, 0, 0, tiled=True)
-    total = jnp.sum(terms.astype(F32), axis=0).astype(BF16)
+    grad_query, grad_value, grad_input = kernel(
+        home_kernel,
+        (shape((tokens, 2048), BF16), shape((tokens, 4096), BF16), shape((tokens, 2048), BF16)),
+        1070 << 20,
+        (pltpu.VMEM((tokens, 2048), F32),),
+        grid=(HEADS,),
+        in_specs=[
+            pl.BlockSpec((1, tokens, 1024), lambda h: (h, 0, 0)),
+            pl.BlockSpec((2048, 256), lambda h: (0, h)),
+        ],
+        out_specs=(by_head(256), by_head(512), pl.BlockSpec((tokens, 2048), lambda h: (0, 0))),
+    )(home, weight)
+
+    whole = pl.BlockSpec(memory_space=pltpu.VMEM)
+    terms = kernel(
+        term_kernel,
+        shape((2048, 256), BF16),
+        1070 << 20,
+        in_specs=[pl.BlockSpec(memory_space=pltpu.SMEM)] + [whole] * 5,
+        out_specs=whole,
+    )(lane.reshape(1), grads, pair, before, after, opposite)
+
+    core = lax.axis_index("dp_1")
+    across_ring = lax.axis_index("dp_0")
+    cores = lax.axis_size("dp_1")
+    if cores == 2:
+        terms = terms.reshape(ring, 2, -1, 256)
+        mine = lax.dynamic_index_in_dim(terms, core, 1, keepdims=False)
+        theirs = lax.dynamic_index_in_dim(terms, 1 - core, 1, keepdims=False)
+        theirs = lax.ppermute(theirs, "dp_1", [(0, 1), (1, 0)])
+        terms = (mine.astype(F32) + theirs.astype(F32)).astype(BF16)
+        total = lax.dynamic_index_in_dim(terms, across_ring, 0, keepdims=False).astype(F32)
+        for step in range(1, ring):
+            piece = lax.dynamic_index_in_dim(terms, (across_ring + step) % ring, 0, keepdims=False)
+            piece = lax.ppermute(piece, "dp_0", [(i, (i + step) % ring) for i in range(ring)])
+            total = total + piece.astype(F32)
+        terms = total.astype(BF16)
+    terms = terms.reshape(2, -1, 256)
+    mine = lax.dynamic_index_in_dim(terms, half, 0, keepdims=False)
+    theirs = lax.dynamic_index_in_dim(terms, 1 - half, 0, keepdims=False)
+    theirs = lax.ppermute(theirs, "half", [(0, 1), (1, 0)])
+    total = (mine.astype(F32) + theirs.astype(F32)).astype(BF16)
     span = total.shape[0]
     spread = jnp.broadcast_to(total[None], (peers, span, 256))
     spread = lax.all_to_all(spread, SP, 0, 0, tiled=True)
-    grad_weight = jnp.moveaxis(spread.reshape(2, 8, span, 256), 1, 2).reshape(2 * span, -1)
-    return grad_query[None], grad_value[None], grad_input[None], grad_weight.astype(F32)
+    grad_weight = kernel(
+        widen_kernel,
+        shape((2 * span, 2048), F32),
+        1 << 20,
+        grid=(2, HEADS),
+        in_specs=[pl.BlockSpec((1, span, 256), lambda s, h: (s * 8 + h, 0, 0))],
+        out_specs=pl.BlockSpec((span, 256), lambda s, h: (s, h)),
+    )(spread)
+    return grad_query[None], grad_value[None], grad_input[None], grad_weight
 
 
 def solution(mesh):

time: 242 us -> 214 us (0.88)
  waiting for transfers between devices: 150 us -> 95.4 us
  Pallas kernels: 12.2 us -> 37.3 us
  blocking collectives: 0 us -> 18.3 us
  matrix products: 11 us -> 0 us
  local copies, waits for them, and re-layouts: 17.9 us -> 9.28 us
    ppermute x0 -> x10, waiting for transfers between devices: none -> 55.7 us  [the longest x1 45 us: shards(): lax.ppermute(layer_input, 'lane', [(i, (i + 4) % 8) for i in range(8)])]
    all_to_all x2 -> x0, waiting for transfers between devices: 40.5 us -> none  [the longest x1 26.9 us: shards(): terms = lax.all_to_all(terms, group, 0, 0, tiled=True)]
    ppermute x1, waiting for transfers between devices: 56.4 us -> 17.4 us  [shards(): lax.ppermute(far, SP, [(u, (1 - u % 2) * 8 + u // 2) for u in range(peers)])]
    ppermute x1, waiting for transfers between devices: 26.2 us -> 0.01 us  [shards(): state = lax.ppermute(state, SP, [(u, (u + 8) % 16) for u in range(peers)])]
    pallas_call x0 -> x4, Pallas kernels: none -> 22.6 us  [the longest x1 9.17 us: shards(): kernel(home_kernel, (shape((tokens, 2048), BF16), shape((tokens, 4096), B...]
    all_to_all x0 -> x1, blocking collectives: none -> 18.3 us  [shards(): spread = lax.all_to_all(spread, SP, 0, 0, tiled=True)]
    ppermute x0 -> x10, starting transfers between devices: none -> 16 us  [the longest x4 6.46 us: lane_step(): lax.ppermute(array, 'lane', [(i, i // 4 * 4 + (i + step) % 4) for i in ra...]
    all_to_all x2 -> x0, starting transfers between devices: 14.3 us -> none  [the longest x1 7.66 us: shards(): terms = lax.all_to_all(terms, group, 0, 0, tiled=True)]
  transfers between devices with their start and end apart: 9 -> 16, of which waited for: 5 -> 8; matrix products, arithmetic and copies ran while one was open for 10% -> 4% of each run, Pallas kernels for 5% -> 13%
where the time goes in v1:
time: 214 us; the launch traced here: 212 us
  waiting for transfers between devices  95.4 us (45%)
  Pallas kernels  37.3 us (17%)
  starting transfers between devices  33.7 us (16%)
  blocking collectives  18.3 us (9%)
  between operations  14.2 us (7%)
  local copies, waits for them, and re-layouts  9.28 us (4%)
  other arithmetic  3.62 us (2%)
    ppermute x1, waiting for transfers between devices, shards(): lax.ppermute(layer_input, 'lane', [(i, (i + 4) % 8) for i in range(8)])  45 us
    all_to_all x1, waiting for transfers between devices, shards(): lax.all_to_all(grads.reshape(8, tokens, -1), 'lane', 0, 0, tiled=True)  21.7 us
    all_to_all x1, blocking collectives, shards(): spread = lax.all_to_all(spread, SP, 0, 0, tiled=True)  18.3 us
    ppermute x1, waiting for transfers between devices, shards(): lax.ppermute(far, SP, [(u, (1 - u % 2) * 8 + u // 2) for u in range(peers)])  17.4 us
    pallas_call x1, Pallas kernels, shards(): kernel(home_kernel, (shape((tokens, 2048), BF16), shape((tokens, 4096), B...  9.17 us
    all_to_all x1, starting transfers between devices, shards(): lax.all_to_all(sent, 'lane', 0, 0, tiled=True).reshape(8 * tokens, -1)  6.49 us
    ppermute x4, starting transfers between devices, lane_step(): lax.ppermute(array, 'lane', [(i, i // 4 * 4 + (i + step) % 4) for i in ra...  6.46 us
    pallas_call x1, Pallas kernels, shards(): kernel(inside_kernel, shape((1024, 1024), F32), 3760 << 20, (pltpu.VMEM((...  6.25 us
  transfers between devices with their start and end apart: 16, of which 8 were waited for; matrix products, arithmetic and copies ran while one was open for 4% of the time, Pallas kernels for 13%

profile of v1, /device:TPU:1, one launch (start us, length us, event | category | flops | bytes accessed | tf_op | source)
XLA Modules:
  0.0 211.8 jit_solution(402539167318562598)
XLA Ops:
  7.2 0.0 all-gather.2.cloned.1.call-start
  7.2 0.7 all-gather.2.cloned.1.call-update
  7.9 1.2 copy-done.2
  9.1 1.2 copy-done.3
  10.4 1.0 copy-done.4
  11.4 1.0 copy-done.5
  12.4 3.5 %shard_map.102 = bf16[8,128,1536]{2,1,0:T(8,128)(2,1)} custom-call(bf16[128,2048]{1,0:T(8,128)(2,1)S(1)} %bitcast.43, bf16[128,2048]{1,0:T(8,128)(2,1)S(1)} %bitcast.44, bf16[128,4096]{1,0:T(8,128)(2,1)S(1)} %bitcast.41, bf16[128,4096]{1,0:T(8,128)(2,1)S(1)} %bitcast.42), custom_call_target="tpu_custom_call" | custom-call | flops 1048576 | bytes 4194304 | tf_op jit(solution)/shard_map/pallas_call | solution.py:205
  15.9 6.5 %all-to-all-start = ((bf16[8,128,1536]{2,1,0:T(8,128)(2,1)}), bf16[8,128,1536]{2,1,0:T(8,128)(2,1)S(1)}, u32[]{:S(2)}, u32[]{:S(2)}) async-start(bf16[8,128,1536]{2,1,0:T(8,128)(2,1)} %shard_map.102), calls=%async_computation | async-start | bytes 6291456 | tf_op jit(solution)/shard_map/all_to_all | solution.py:213
  22.4 1.5 collective-permute-start
  23.9 45.0 %collective-permute-done = bf16[1,128,2048]{2,1,0:T(8,128)(2,1)S(1)} collective-permute-done((bf16[1,128,2048]{2,1,0:T(8,128)(2,1)}, bf16[1,128,2048]{2,1,0:T(8,128)(2,1)S(1)}, u32[]{:S(2)}, u32[]{:S(2)}) %collective-permute-start) | collective-permute-done | bytes 524320 | tf_op jit(solution)/shard_map/ppermute | solution.py:220
  68.9 2.1 pad_maximum_fusion.own_ref
  71.0 0.0 all-to-all-done
  71.0 1.2 collective-permute-start.4
  72.2 2.6 %collective-permute-start.5 = (bf16[2,128,2048]{2,1,0:T(8,128)(2,1)}, bf16[2,128,2048]{2,1,0:T(8,128)(2,1)}, u32[]{:S(2)}, u32[]{:S(2)}) collective-permute-start(bf16[2,128,2048]{2,1,0:T(8,128)(2,1)} %pad_maximum_fusion.own_ref), channel_id=1, source_target_pairs={{0,24},{8,0},{16,8},{24,16},{32,56},{40,32},{48,40},{56,48},{1,25}... | collective-permute-start | bytes 3145736 | tf_op jit(solution)/shard_map/ppermute | solution.py:216
  74.8 0.7 collective-permute-start.1
  75.4 4.6 %collective-permute-start.2 = (f32[8,128]{1,0:T(8,128)S(1)}, f32[8,128]{1,0:T(8,128)S(1)}, u32[]{:S(2)}, u32[]{:S(2)}) collective-permute-start(f32[8,128]{1,0:T(8,128)S(1)} %get-tuple-element.26), channel_id=1, source_target_pairs={{0,64},{8,0},{16,72},{24,8},{32,80},{40,16},{48,88},{56,24},{64,96... | collective-permute-start | bytes 12296 | tf_op jit(solution)/shard_map/ppermute | solution.py:199
  80.1 17.4 %collective-permute-done.2 = f32[8,128]{1,0:T(8,128)S(1)} collective-permute-done((f32[8,128]{1,0:T(8,128)S(1)}, f32[8,128]{1,0:T(8,128)S(1)}, u32[]{:S(2)}, u32[]{:S(2)}) %collective-permute-start.2) | collective-permute-done | bytes 4128 | tf_op jit(solution)/shard_map/ppermute | solution.py:199
  97.4 0.4 shard_map.103
  97.9 2.3 %shard_map.104 = (bf16[2,256,512]{2,1,0:T(8,128)(2,1)}, bf16[1024,256]{1,0:T(8,128)(2,1)S(1)}) custom-call(bf16[1024,1536]{1,0:T(8,128)(2,1)S(1)} %bitcast.36, f32[128,128]{1,0:T(8,128)S(1)} %get-tuple-element.14.cols_ref), custom_call_target="tpu_custom_call" | custom-call | flops 566231040 | bytes 4194304 | tf_op jit(solution)/shard_map/pallas_call | solution.py:226
  100.2 0.8 copy-done.6
  101.0 2.3 %collective-permute-start.3 = (bf16[2,256,512]{2,1,0:T(8,128)(2,1)}, bf16[2,256,512]{2,1,0:T(8,128)(2,1)}, u32[]{:S(2)}, u32[]{:S(2)}) collective-permute-start(bf16[2,256,512]{2,1,0:T(8,128)(2,1)} %get-tuple-element.16), channel_id=1, source_target_pairs={{0,64},{8,72},{16,80},{24,88},{32,96},{40,104},{48,112},{56,120},{... | collective-permute-start | bytes 1572872 | tf_op jit(solution)/shard_map/ppermute | solution.py:229
  103.3 1.9 slice.8
  105.2 2.2 %collective-permute-start.6 = (bf16[1,128,2048]{2,1,0:T(8,128)(2,1)}, bf16[1,128,2048]{2,1,0:T(8,128)(2,1)}, u32[]{:S(2)}, u32[]{:S(2)}) collective-permute-start(bf16[1,128,2048]{2,1,0:T(8,128)(2,1)} %slice.8), channel_id=1, source_target_pairs={{0,8},{8,16},{16,24},{24,0},{32,40},{40,48},{48,56},{56,32},{1,9},... | collective-permute-start | bytes 1572872 | tf_op jit(solution)/shard_map/ppermute | solution.py:216
  107.4 1.9 slice.9
  109.2 0.5 collective-permute-start.7
  109.7 6.2 %shard_map.105.part_ref = f32[1024,1024]{1,0:T(8,128)} custom-call(bf16[1024,1536]{1,0:T(8,128)(2,1)S(1)} %bitcast.37, f32[40,128]{1,0:T(8,128)S(1)} %get-tuple-element.17.rows_ref, f32[128,128]{1,0:T(8,128)S(1)} %get-tuple-element.14.cols_ref), custom_call_target="tpu_custom_call" | custom-call | flops 3942645760 | bytes 4194304 | tf_op jit(solution)/shard_map/pallas_call | solution.py:230
  116.0 0.0 copy-start.1
  116.0 5.7 %shard_map.106.grads_ref = bf16[1024,1024]{1,0:T(8,128)(2,1)} custom-call(bf16[1024,1536]{1,0:T(8,128)(2,1)} %bitcast.38, f32[128,128]{1,0:T(8,128)S(1)} %get-tuple-element.14.cols_ref, bf16[1024,256]{1,0:T(8,128)(2,1)S(1)} %copy-done.7, bf16[2,256,512]{2,1,0:T(8,128)(2,1)} %collective-permute-done.3.state_ref, f32[1024,1024]{1,0:T(8,128)} %shard_map.105.part_ref), custom_call_target="tpu_custom_call" | custom-call | flops 838860800 | bytes 4194304 | tf_op jit(solution)/shard_map/pallas_call | solution.py:236
  121.8 1.3 pad_maximum_fusion.1.far_ref
  123.1 4.6 %shard_map.108 = bf16[2048,256]{1,0:T(8,128)(2,1)S(1)} custom-call(s32[1]{0:T(128)} %bitcast.12.lane_ref, bf16[1024,1024]{1,0:T(8,128)(2,1)} %shard_map.106.grads_ref, bf16[2,128,2048]{2,1,0:T(8,128)(2,1)S(1)} %copy-done.1, bf16[2,128,2048]{2,1,0:T(8,128)(2,1)} %collective-permute-done.4.before_ref, bf16[2,128,2048]{2,1,0:T(8,128)(2,1)} %collective-permute-done.5.after_ref, ...), custom_call_target="tpu_custom_call" | custom-call | flops 1121976320 | bytes 4194304 | tf_op jit(solution)/shard_map/pallas_call | solution.py:255
  127.7 3.2 %collective-permute-start.8 = (bf16[4,256,256]{2,1,0:T(8,128)(2,1)S(1)}, bf16[4,256,256]{2,1,0:T(8,128)(2,1)S(1)}, u32[]{:S(2)}, u32[]{:S(2)}) collective-permute-start(bf16[4,256,256]{2,1,0:T(8,128)(2,1)S(1)} %dynamic-slice_bitcast_fusion), channel_id=1, source_target_pairs={{0,1},{1,0},{2,3},{3,2},{4,5},{5,4},{6,7},{7,6},{8,9},{9,8},{10,11... | collective-permute-start | bytes 1572872 | tf_op jit(solution)/shard_map/ppermute | solution.py:270
  130.9 1.5 collective-permute-done.8
  132.4 0.1 fusion
  132.6 2.8 %collective-permute-start.10 = (bf16[256,256]{1,0:T(8,128)(2,1)S(1)}, bf16[256,256]{1,0:T(8,128)(2,1)S(1)}, u32[]{:S(2)}, u32[]{:S(2)}) collective-permute-start(bf16[256,256]{1,0:T(8,128)(2,1)S(1)} %get-tuple-element.24), channel_id=1, source_target_pairs={{0,4},{2,6},{4,0},{6,2},{1,5},{3,7},{5,1},{7,3},{8,12},{10,14},{12... | collective-permute-start | bytes 393224 | tf_op jit(solution)/shard_map/ppermute | solution.py:275
  135.4 0.9 collective-permute-start.11
  136.3 0.6 collective-permute-start.9
  136.9 2.0 collective-permute-done.10
  138.9 2.9 %collective-permute-done.11 = bf16[256,256]{1,0:T(8,128)(2,1)S(1)} collective-permute-done((bf16[256,256]{1,0:T(8,128)(2,1)S(1)}, bf16[256,256]{1,0:T(8,128)(2,1)S(1)}, u32[]{:S(2)}, u32[]{:S(2)}) %collective-permute-start.11) | collective-permute-done | bytes 131104 | tf_op jit(solution)/shard_map/ppermute | solution.py:275
  141.8 0.2 collective-permute-done.9
  141.9 0.1 fusion.3
  142.0 0.6 collective-permute-start.12
  142.6 4.1 %collective-permute-done.12 = bf16[128,256]{1,0:T(8,128)(2,1)S(1)} collective-permute-done((bf16[128,256]{1,0:T(8,128)(2,1)S(1)}, bf16[128,256]{1,0:T(8,128)(2,1)S(1)}, u32[]{:S(2)}, u32[]{:S(2)}) %collective-permute-start.12) | collective-permute-done | bytes 65568 | tf_op jit(solution)/shard_map/ppermute | solution.py:281
  146.8 0.1 broadcast_in_dim.22
  146.9 18.3 %all_to_all.15.in_ref = bf16[16,128,256]{2,1,0:T(8,128)(2,1)S(1)} all-to-all(bf16[16,128,256]{2,1,0:T(8,128)(2,1)S(1)} %broadcast_in_dim.22), channel_id=1, replica_groups=mesh['half'=2,'lane'=8,'dp_0'=4,'dp_1'=2] {'half','lane'}, dimensions={0} | all-to-all | bytes 2097152 | tf_op jit(solution)/shard_map/all_to_all | solution.py:285
  165.1 3.6 %all-to-all-start.1 = ((bf16[8,128,1024]{2,1,0:T(8,128)(2,1)}), bf16[8,128,1024]{2,1,0:T(8,128)(2,1)S(1)}, u32[]{:S(2)}, u32[]{:S(2)}) async-start(bf16[8,128,1024]{2,1,0:T(8,128)(2,1)} %bitcast.8), calls=%async_computation.1 | async-start | bytes 4194304 | tf_op jit(solution)/shard_map/all_to_all | solution.py:240
  168.7 5.4 %shard_map.109 = f32[256,2048]{1,0:T(8,128)} custom-call(bf16[16,128,256]{2,1,0:T(8,128)(2,1)S(1)} %all_to_all.15.in_ref), custom_call_target="tpu_custom_call" | custom-call | flops 1048576 | bytes 4194304 | tf_op jit(solution)/shard_map/pallas_call | solution.py:286
  174.1 21.7 %all-to-all-done.1.home_ref = bf16[8,128,1024]{2,1,0:T(8,128)(2,1)S(1)} async-done(((bf16[8,128,1024]{2,1,0:T(8,128)(2,1)}), bf16[8,128,1024]{2,1,0:T(8,128)(2,1)S(1)}, u32[]{:S(2)}, u32[]{:S(2)}) %all-to-all-start.1) | async-done | bytes 2097184 | tf_op jit(solution)/shard_map/all_to_all | solution.py:240
  195.8 9.2 %shard_map.107 = (bf16[128,2048]{1,0:T(8,128)(2,1)}, bf16[128,4096]{1,0:T(8,128)(2,1)}, bf16[128,2048]{1,0:T(8,128)(2,1)}) custom-call(bf16[8,128,1024]{2,1,0:T(8,128)(2,1)S(1)} %all-to-all-done.1.home_ref, bf16[2048,2048]{1,0:T(8,128)(2,1)} %all-gather.2.cloned.1.call-done.weight_ref), custom_call_target="tpu_custom_call" | custom-call | flops 1121976320 | bytes 4194304 | tf_op jit(solution)/shard_map/pallas_call | solution.py:241
  (26 shorter events, 0.2 us)
Async XLA Ops:
  7.2 188.6 %all-gather.2.cloned.1.call-start = ((), (), s32[]{:S(2)}) async-start(), calls=%async_computation.3 | async-start | bytes 9437184 | tf_op jit(solution)/shard_map/all_gather | solution.py:192
  7.9 1.2 copy-start.2
  9.1 1.2 copy-start.3
  10.4 1.0 copy-start.4
  11.4 1.0 copy-start.5
  15.9 58.8 %copy-start.8 = (f32[1,1,2048]{2,1,0:T(1,128)S(1)}, f32[1,1,2048]{2,1,0:T(1,128)}, u32[]{:S(2)}) copy-start(f32[1,1,2048]{2,1,0:T(1,128)} %param.12) | copy-start | bytes 24580
  15.9 55.0 %all-to-all-start = ((bf16[8,128,1536]{2,1,0:T(8,128)(2,1)}), bf16[8,128,1536]{2,1,0:T(8,128)(2,1)S(1)}, u32[]{:S(2)}, u32[]{:S(2)}) async-start(bf16[8,128,1536]{2,1,0:T(8,128)(2,1)} %shard_map.102), calls=%async_computation | async-start | bytes 6291456 | tf_op jit(solution)/shard_map/all_to_all | solution.py:213
  22.4 46.4 %collective-permute-start = (bf16[1,128,2048]{2,1,0:T(8,128)(2,1)}, bf16[1,128,2048]{2,1,0:T(8,128)(2,1)S(1)}, u32[]{:S(2)}, u32[]{:S(2)}) collective-permute-start(bf16[1,128,2048]{2,1,0:T(8,128)(2,1)} %param.7), channel_id=1, source_target_pairs={{0,32},{8,40},{16,48},{24,56},{32,0},{40,8},{48,16},{56,24},{1,33}... | collective-permute-start | bytes 1572872 | tf_op jit(solution)/shard_map/ppermute | solution.py:220
  71.0 45.0 %copy-start = (bf16[8,128,1536]{2,1,0:T(8,128)(2,1)}, bf16[8,128,1536]{2,1,0:T(8,128)(2,1)S(1)}, u32[]{:S(2)}) copy-start(bf16[8,128,1536]{2,1,0:T(8,128)(2,1)S(1)} %all-to-all-done) | copy-start | bytes 9437188
  71.0 32.3 %collective-permute-start.4 = (bf16[2,128,2048]{2,1,0:T(8,128)(2,1)}, bf16[2,128,2048]{2,1,0:T(8,128)(2,1)}, u32[]{:S(2)}, u32[]{:S(2)}) collective-permute-start(bf16[2,128,2048]{2,1,0:T(8,128)(2,1)} %pad_maximum_fusion.own_ref), channel_id=1, source_target_pairs={{0,8},{8,16},{16,24},{24,0},{32,40},{40,48},{48,56},{56,32},{1,9},... | collective-permute-start | bytes 3145736 | tf_op jit(solution)/shard_map/ppermute | solution.py:216
  72.2 35.2 %collective-permute-start.5 = (bf16[2,128,2048]{2,1,0:T(8,128)(2,1)}, bf16[2,128,2048]{2,1,0:T(8,128)(2,1)}, u32[]{:S(2)}, u32[]{:S(2)}) collective-permute-start(bf16[2,128,2048]{2,1,0:T(8,128)(2,1)} %pad_maximum_fusion.own_ref), channel_id=1, source_target_pairs={{0,24},{8,0},{16,8},{24,16},{32,56},{40,32},{48,40},{56,48},{1,25}... | collective-permute-start | bytes 3145736 | tf_op jit(solution)/shard_map/ppermute | solution.py:216
  74.8 5.3 %collective-permute-start.1 = (f32[8,128]{1,0:T(8,128)S(1)}, f32[8,128]{1,0:T(8,128)S(1)}, u32[]{:S(2)}, u32[]{:S(2)}) collective-permute-start(f32[8,128]{1,0:T(8,128)S(1)} %get-tuple-element.25), channel_id=1, source_target_pairs={{0,0},{8,64},{16,8},{24,72},{32,16},{40,80},{48,24},{56,88},{64,32... | collective-permute-start | bytes 12296 | tf_op jit(solution)/shard_map/ppermute | solution.py:198
  75.4 22.0 %collective-permute-start.2 = (f32[8,128]{1,0:T(8,128)S(1)}, f32[8,128]{1,0:T(8,128)S(1)}, u32[]{:S(2)}, u32[]{:S(2)}) collective-permute-start(f32[8,128]{1,0:T(8,128)S(1)} %get-tuple-element.26), channel_id=1, source_target_pairs={{0,64},{8,0},{16,72},{24,8},{32,80},{40,16},{48,88},{56,24},{64,96... | collective-permute-start | bytes 12296 | tf_op jit(solution)/shard_map/ppermute | solution.py:199
  100.2 0.8 copy-start.6
  101.0 15.0 %collective-permute-start.3 = (bf16[2,256,512]{2,1,0:T(8,128)(2,1)}, bf16[2,256,512]{2,1,0:T(8,128)(2,1)}, u32[]{:S(2)}, u32[]{:S(2)}) collective-permute-start(bf16[2,256,512]{2,1,0:T(8,128)(2,1)} %get-tuple-element.16), channel_id=1, source_target_pairs={{0,64},{8,72},{16,80},{24,88},{32,96},{40,104},{48,112},{56,120},{... | collective-permute-start | bytes 1572872 | tf_op jit(solution)/shard_map/ppermute | solution.py:229
  105.2 16.6 %collective-permute-start.6 = (bf16[1,128,2048]{2,1,0:T(8,128)(2,1)}, bf16[1,128,2048]{2,1,0:T(8,128)(2,1)}, u32[]{:S(2)}, u32[]{:S(2)}) collective-permute-start(bf16[1,128,2048]{2,1,0:T(8,128)(2,1)} %slice.8), channel_id=1, source_target_pairs={{0,8},{8,16},{16,24},{24,0},{32,40},{40,48},{48,56},{56,32},{1,9},... | collective-permute-start | bytes 1572872 | tf_op jit(solution)/shard_map/ppermute | solution.py:216
  109.2 12.5 %collective-permute-start.7 = (bf16[1,128,2048]{2,1,0:T(8,128)(2,1)}, bf16[1,128,2048]{2,1,0:T(8,128)(2,1)}, u32[]{:S(2)}, u32[]{:S(2)}) collective-permute-start(bf16[1,128,2048]{2,1,0:T(8,128)(2,1)} %slice.9), channel_id=1, source_target_pairs={{0,24},{8,0},{16,8},{24,16},{32,56},{40,32},{48,40},{56,48},{1,25}... | collective-permute-start | bytes 1572872 | tf_op jit(solution)/shard_map/ppermute | solution.py:216
  109.7 6.3 %copy-start.7 = (bf16[1024,256]{1,0:T(8,128)(2,1)S(1)}, bf16[1024,256]{1,0:T(8,128)(2,1)}, u32[]{:S(2)}) copy-start(bf16[1024,256]{1,0:T(8,128)(2,1)} %copy-done.6) | copy-start | bytes 1572868
  116.0 7.1 %copy-start.1 = (bf16[2,128,2048]{2,1,0:T(8,128)(2,1)S(1)}, bf16[2,128,2048]{2,1,0:T(8,128)(2,1)}, u32[]{:S(2)}) copy-start(bf16[2,128,2048]{2,1,0:T(8,128)(2,1)} %pad_maximum_fusion.own_ref) | copy-start | bytes 3145732
  127.7 4.7 %collective-permute-start.8 = (bf16[4,256,256]{2,1,0:T(8,128)(2,1)S(1)}, bf16[4,256,256]{2,1,0:T(8,128)(2,1)S(1)}, u32[]{:S(2)}, u32[]{:S(2)}) collective-permute-start(bf16[4,256,256]{2,1,0:T(8,128)(2,1)S(1)} %dynamic-slice_bitcast_fusion), channel_id=1, source_target_pairs={{0,1},{1,0},{2,3},{3,2},{4,5},{5,4},{6,7},{7,6},{8,9},{9,8},{10,11... | collective-permute-start | bytes 1572872 | tf_op jit(solution)/shard_map/ppermute | solution.py:270
  132.6 6.3 %collective-permute-start.10 = (bf16[256,256]{1,0:T(8,128)(2,1)S(1)}, bf16[256,256]{1,0:T(8,128)(2,1)S(1)}, u32[]{:S(2)}, u32[]{:S(2)}) collective-permute-start(bf16[256,256]{1,0:T(8,128)(2,1)S(1)} %get-tuple-element.24), channel_id=1, source_target_pairs={{0,4},{2,6},{4,0},{6,2},{1,5},{3,7},{5,1},{7,3},{8,12},{10,14},{12... | collective-permute-start | bytes 393224 | tf_op jit(solution)/shard_map/ppermute | solution.py:275
  135.4 6.3 %collective-permute-start.11 = (bf16[256,256]{1,0:T(8,128)(2,1)S(1)}, bf16[256,256]{1,0:T(8,128)(2,1)S(1)}, u32[]{:S(2)}, u32[]{:S(2)}) collective-permute-start(bf16[256,256]{1,0:T(8,128)(2,1)S(1)} %get-tuple-element.23), channel_id=1, source_target_pairs={{0,6},{2,0},{4,2},{6,4},{1,7},{3,1},{5,3},{7,5},{8,14},{10,8},{12,... | collective-permute-start | bytes 393224 | tf_op jit(solution)/shard_map/ppermute | solution.py:275
  136.3 5.7 %collective-permute-start.9 = (bf16[256,256]{1,0:T(8,128)(2,1)S(1)}, bf16[256,256]{1,0:T(8,128)(2,1)S(1)}, u32[]{:S(2)}, u32[]{:S(2)}) collective-permute-start(bf16[256,256]{1,0:T(8,128)(2,1)S(1)} %get-tuple-element.22), channel_id=1, source_target_pairs={{0,2},{2,4},{4,6},{6,0},{1,3},{3,5},{5,7},{7,1},{8,10},{10,12},{12... | collective-permute-start | bytes 393224 | tf_op jit(solution)/shard_map/ppermute | solution.py:275
  142.0 4.7 %collective-permute-start.12 = (bf16[128,256]{1,0:T(8,128)(2,1)S(1)}, bf16[128,256]{1,0:T(8,128)(2,1)S(1)}, u32[]{:S(2)}, u32[]{:S(2)}) collective-permute-start(bf16[128,256]{1,0:T(8,128)(2,1)S(1)} %dynamic-slice_bitcast_fusion.4), channel_id=1, source_target_pairs={{0,64},{64,0},{1,65},{65,1},{2,66},{66,2},{3,67},{67,3},{4,68},{68... | collective-permute-start | bytes 196616 | tf_op jit(solution)/shard_map/ppermute | solution.py:281
  165.1 30.7 %all-to-all-start.1 = ((bf16[8,128,1024]{2,1,0:T(8,128)(2,1)}), bf16[8,128,1024]{2,1,0:T(8,128)(2,1)S(1)}, u32[]{:S(2)}, u32[]{:S(2)}) async-start(bf16[8,128,1024]{2,1,0:T(8,128)(2,1)} %bitcast.8), calls=%async_computation.1 | async-start | bytes 4194304 | tf_op jit(solution)/shard_map/all_to_all | solution.py:240
Sparse Core Ops, SparseCore 0:
  9.7 53.2 all-gather.1

commit v2 on v1

v2 whole, which is shorter than its diff:
```python
import jax
import jax.numpy as jnp
from jax import lax
from jax.experimental import pallas as pl
from jax.experimental.pallas import tpu as pltpu
from jax.sharding import Mesh
from jax.sharding import PartitionSpec as P


HEADS = 8
BLOCK = 128
TILE = 256
SP = ("half", "lane")
DP = ("dp_0", "dp_1")
F32 = jnp.float32
BF16 = jnp.bfloat16


def dot(a, b, dims, precision=None):
    return lax.dot_general(a, b, (dims, ((), ())), precision=precision, preferred_element_type=F32)


NN = ((1,), (0,))
NT = ((1,), (1,))
TN = ((0,), (0,))


def decay_kernel(lam_ref, half_ref, rows_ref, tall_ref):
    n = BLOCK
    row = lax.broadcasted_iota(jnp.int32, (n, n), 0)
    col = lax.broadcasted_iota(jnp.int32, (n, n), 1)
    lam = lam_ref[...]
    high = lax.Precision.HIGHEST
    upto = dot(lam, (row <= col).astype(F32), NN, high)
    before = dot(lam, (row < col).astype(F32), NN, high)
    since = dot(lam, (row >= col).astype(F32), NN, high)
    after = dot(lam, (row > col).astype(F32), NN, high)
    totals = [jnp.broadcast_to(upto[b : b + 1, n - 1 : n], (1, n)) for b in range(16)]
    loc0, suf1, rem0, pre1 = [], [], [], []
    for b in range(8):
        odd = b % 2 == 1
        loc0.append(upto[b : b + 1] + totals[b - 1] if odd else upto[b : b + 1])
        suf1.append(since[8 + b : 9 + b] if odd else since[8 + b : 9 + b] + totals[9 + b])
        rem0.append(after[b : b + 1] if odd else after[b : b + 1] + totals[b + 1])
        pre1.append(before[8 + b : 9 + b] + totals[7 + b] if odd else before[8 + b : 9 + b])
    tile0 = [totals[2 * t] + totals[2 * t + 1] for t in range(4)]
    tile1 = [totals[8 + 2 * t] + totals[9 + 2 * t] for t in range(4)]
    first = half_ref[...] == 0
    key_sum, query_sum = [], []
    for b in range(8):
        t = b // 2
        later0, later1 = sum(tile0[t + 1 :]), sum(tile1[t + 1 :])
        early0, early1 = sum(tile0[:t]), sum(tile1[:t])
        key_sum.append(jnp.where(first, rem0[b] + later0, pre1[b] + early1))
        query_sum.append(jnp.where(first, suf1[b] + later1, loc0[b] + early0))
    rows_ref[...] = jnp.concatenate(loc0 + suf1 + rem0 + pre1 + tile0 + tile1, axis=0)
    keys = jnp.exp(jnp.concatenate(key_sum, axis=0))
    queries = jnp.exp(jnp.concatenate(query_sum, axis=0)) * 0.0625
    stack = [jnp.concatenate(loc0 + suf1, axis=0), keys, queries, jnp.zeros((n - 32, n), F32)]
    cols = jnp.transpose(jnp.concatenate(stack, axis=0))
    for b in range(8):
        picks = [cols[:, v * 8 + b : v * 8 + b + 1] for v in range(4)]
        tall_ref[b * n : b * n + n, :] = jnp.concatenate(picks, axis=1)


def wide(rows, base, t):
    return jnp.concatenate([rows[base + 2 * t : base + 2 * t + 1], rows[base + 2 * t + 1 : base + 2 * t + 2]], axis=1)


def boundary_kernel(units_ref, tall_ref, state_ref):
    keys = (units_ref[:, 256:512].astype(F32) * tall_ref[:, 2:3]).astype(BF16)
    queries = (units_ref[:, 0:256].astype(F32) * tall_ref[:, 3:4]).astype(BF16)
    state_ref[0] = dot(keys, units_ref[:, 512:1024], TN).astype(BF16)
    state_ref[1] = dot(queries, units_ref[:, 1024:1536], TN).astype(BF16)


def inside_kernel(units_ref, rows_ref, tall_ref, out_ref, s_ref, gs_ref):
    rows = rows_ref[...]
    row = lax.broadcasted_iota(jnp.int32, (TILE, TILE), 0)
    col = lax.broadcasted_iota(jnp.int32, (TILE, TILE), 1)
    for i in range(4):
        at = pl.ds(i * TILE, TILE)
        query, grad = units_ref[at, 0:256], units_ref[at, 1024:1536]
        loc0, suf1 = tall_ref[at, 0:1], tall_ref[at, 1:2]
        for j in range(4):
            to = pl.ds(j * TILE, TILE)
            if i == j:
                spread = jnp.where(row >= col, loc0 - wide(rows, 0, i), suf1 - wide(rows, 8, i))
            elif i > j:
                along = wide(rows, 16, j)
                for t in range(j + 1, i):
                    along = along + jnp.concatenate([rows[32 + t : 33 + t]] * 2, axis=1)
                spread = loc0 + along
            else:
                along = wide(rows, 24, j)
                for t in range(i + 1, j):
                    along = along + jnp.concatenate([rows[36 + t : 37 + t]] * 2, axis=1)
                spread = suf1 + along
            weights = jnp.exp(spread) * 0.0625
            scores = dot(query, units_ref[to, 256:512], NT)
            grads = dot(grad, units_ref[to, 512:1024], NT)
            s_ref[at, to] = (scores * weights).astype(BF16)
            gs_ref[at, to] = (grads * weights).astype(BF16)
    out_ref[:, 0:256] = dot(gs_ref[...], units_ref[:, 0:256], TN).astype(BF16)
    out_ref[:, 256:512] = dot(gs_ref[...], units_ref[:, 256:512], NN).astype(BF16)
    out_ref[:, 512:1024] = dot(s_ref[...], units_ref[:, 1024:1536], TN).astype(BF16)


def across_kernel(units_ref, tall_ref, state_ref, part_ref, out_ref):
    memory, later = state_ref[0], state_ref[1]
    keys = (units_ref[:, 256:512].astype(F32) * tall_ref[:, 2:3]).astype(BF16)
    part = dot(units_ref[:, 512:1024], later, NT) * tall_ref[:, 2:3]
    out_ref[:, 0:256] = (part_ref[:, 0:256].astype(F32) + part).astype(BF16)
    part = dot(units_ref[:, 1024:1536], memory, NT) * tall_ref[:, 3:4]
    out_ref[:, 256:512] = (part_ref[:, 256:512].astype(F32) + part).astype(BF16)
    part = dot(keys, later, NN)
    out_ref[:, 512:1024] = (part_ref[:, 512:1024].astype(F32) + part).astype(BF16)


def kernel(body, out_shape, flops, scratch=(), **grid):
    return pl.pallas_call(
        body,
        out_shape=out_shape,
        scratch_shapes=scratch,
        cost_estimate=pl.CostEstimate(flops=flops, bytes_accessed=4 << 20, transcendentals=0),
        compiler_params=pltpu.CompilerParams(vmem_limit_bytes=24 << 20),
        **grid,
    )


def in_hbm(array):
    return pltpu.with_memory_space_constraint(array, pltpu.HBM)


def shape(dims, dtype):
    return jax.ShapeDtypeStruct(dims, dtype)


def pack_kernel(query_ref, key_ref, value_ref, grad_ref, out_ref, sems):
    copies, at = [], 0
    for source in (query_ref, key_ref, value_ref, grad_ref):
        width = source.shape[1] // HEADS
        for h in range(HEADS):
            copies.append(
                pltpu.make_async_copy(
                    source.at[:, pl.ds(h * width, width)],
                    out_ref.at[h, :, pl.ds(at, width)],
                    sems.at[len(copies)],
                )
            )
        at += width
    for copy in copies:
        copy.start()
    for copy in copies:
        copy.wait()


STEPS = ((0, 0), (1, 0), (0, 3), (0, 1), (1, 3), (1, 1), (0, 2), (1, 2))


def term_kernel(lane_ref, grads_ref, *refs):
    lane = lane_ref[0]
    deep, y = lane // 4, lane % 4
    total = None
    for piece, (other, step) in zip(refs[:-1], STEPS, strict=True):
        block = (deep ^ other) * 4 + (y + step) % 4
        grad = grads_ref[pl.ds(pl.multiple_of(block * BLOCK, BLOCK), BLOCK), :]
        part = dot(piece[0], grad, TN)
        total = part if total is None else total + part
    refs[-1][...] = total.astype(BF16)


def home_kernel(owner_ref, home_ref, *refs):
    weights, (query_ref, value_ref, input_ref, key_ref) = refs[:-4], refs[-4:]
    for h in range(HEADS):
        key_ref[:, h * 256 : h * 256 + 256] = home_ref[h, :, 0:256]
        query_ref[:, h * 256 : h * 256 + 256] = home_ref[h, :, 256:512]
        value_ref[:, h * 512 : h * 512 + 512] = home_ref[h, :, 512:1024]
    for k, weight in enumerate(weights):
        span = weight.shape[0]
        at = pl.multiple_of(owner_ref[k] * span, span)
        input_ref[:, pl.ds(at, span)] = dot(key_ref[...], weight[...], NT).astype(BF16)


def widen_kernel(in_ref, out_ref):
    for s in range(2):
        for h in range(2):
            span = in_ref.shape[2]
            out_ref[s * span : s * span + span, h * 256 : h * 256 + 256] = in_ref[s, h].astype(F32)


def shards(layer_input, queries, key_vectors, values, cotangent, log_decay, key_weight):
    tokens = layer_input.shape[1]
    half = lax.axis_index("half")
    lane = lax.axis_index("lane")
    peers = lax.axis_size(SP)
    ring = lax.axis_size("dp_0")
    cores = lax.axis_size("dp_1")
    core, turn = lax.axis_index("dp_1"), lax.axis_index("dp_0")

    decay = log_decay.reshape(2, 8, BLOCK)
    own = lane % 2
    near = lax.dynamic_index_in_dim(decay, own, 0, keepdims=False)
    far = lax.dynamic_index_in_dim(decay, 1 - own, 0, keepdims=False)
    near = lax.ppermute(near, SP, [(u, u % 2 * 8 + u // 2) for u in range(peers)])
    far = lax.ppermute(far, SP, [(u, (1 - u % 2) * 8 + u // 2) for u in range(peers)])
    deep = lax.ppermute(layer_input, "lane", [(i, (i + 4) % 8) for i in range(8)])
    lam = jnp.where(half == 0, jnp.concatenate([near, far]), jnp.concatenate([far, near]))
    rows, tall = kernel(decay_kernel, (shape((40, 128), F32), pltpu.HBM((1024, 4), F32)), 1 << 20)(
        lam, jnp.full((1, 128), half, jnp.int32)
    )

    outside = pl.BlockSpec(memory_space=pltpu.HBM)
    whole = pl.BlockSpec(memory_space=pltpu.VMEM)
    scalars = pl.BlockSpec(memory_space=pltpu.SMEM)
    sent = kernel(
        pack_kernel,
        pltpu.HBM((8, tokens, 1536), BF16),
        1 << 20,
        (pltpu.SemaphoreType.DMA((32,)),),
        in_specs=[outside] * 4,
        out_specs=outside,
    )(*[in_hbm(a[0]) for a in (queries, key_vectors, values, cotangent)])
    units = lax.all_to_all(sent, "lane", 0, 0, tiled=True).reshape(8 * tokens, -1)

    def lane_step(array, step):
        return lax.ppermute(
            array, "lane", [(i, i // 4 * 4 + (i + step) % 4) for i in range(8)]
        )

    weights, owners = [key_weight], [turn * cores + core]
    for step in range(1, ring):
        moves = [(i, (i + step) % ring) for i in range(ring)]
        weights.append(lax.ppermute(key_weight, "dp_0", moves))
        owners.append((turn - step) % ring * cores + core)
    if cores == 2:
        weights += [lax.ppermute(w, "dp_1", [(0, 1), (1, 0)]) for w in weights]
        owners += [o + 1 - 2 * core for o in owners]

    own, deep, units = lax.optimization_barrier((layer_input, deep, units))
    own_before, own_after = lane_step(own, 1), lane_step(own, 3)
    deep_before, deep_after = lane_step(deep, 1), lane_step(deep, 3)
    own_last, deep_last = lane_step(own_before, 1), lane_step(deep_after, 3)

    state = kernel(boundary_kernel, pltpu.HBM((2, 256, 512), BF16), 540 << 20)(units, tall)
    state = lax.ppermute(state, SP, [(u, (u + 8) % 16) for u in range(peers)])
    part = kernel(
        inside_kernel,
        pltpu.HBM((1024, 1024), BF16),
        3760 << 20,
        (pltpu.VMEM((1024, 1024), BF16), pltpu.VMEM((1024, 1024), BF16)),
    )(units, rows, tall)

    def by_tile(width):
        return pl.BlockSpec((TILE, width), lambda i: (i, 0))

    grads = kernel(
        across_kernel,
        pltpu.HBM((1024, 1024), BF16),
        800 << 20,
        grid=(4,),
        in_specs=[
            by_tile(1536),
            by_tile(4),
            pl.BlockSpec((2, 256, 512), lambda i: (0, 0, 0)),
            by_tile(1024),
        ],
        out_specs=by_tile(1024),
    )(units, tall, state, in_hbm(part))

    home = lax.all_to_all(grads.reshape(8, tokens, -1), "lane", 0, 0, tiled=True)
    grad_query, grad_value, grad_input = kernel(
        home_kernel,
        (shape((tokens, 2048), BF16), shape((tokens, 4096), BF16), shape((tokens, 2048), BF16)),
        1070 << 20,
        (pltpu.VMEM((tokens, 2048), BF16),),
        in_specs=[scalars] + [whole] * (1 + len(weights)),
        out_specs=(whole, whole, whole),
    )(jnp.stack(owners), home, *weights)

    terms = kernel(
        term_kernel,
        shape((2048, 256), BF16),
        1070 << 20,
        grid=(1,),
        in_specs=[scalars, pl.BlockSpec((1024, 256), lambda i: (0, 0))] + [whole] * 8,
        out_specs=whole,
    )(
        lane.reshape(1),
        in_hbm(grads),
        own,
        deep,
        own_before,
        own_after,
        deep_before,
        deep_after,
        own_last,
        deep_last,
    )

    if cores == 2:
        terms = terms.reshape(ring, 2, -1, 256)
        mine = lax.dynamic_index_in_dim(terms, core, 1, keepdims=False)
        theirs = lax.dynamic_index_in_dim(terms, 1 - core, 1, keepdims=False)
        theirs = lax.ppermute(theirs, "dp_1", [(0, 1), (1, 0)])
        terms = (mine.astype(F32) + theirs.astype(F32)).astype(BF16)
        total = lax.dynamic_index_in_dim(terms, turn, 0, keepdims=False).astype(F32)
        for step in range(1, ring):
            piece = lax.dynamic_index_in_dim(terms, (turn + step) % ring, 0, keepdims=False)
            piece = lax.ppermute(piece, "dp_0", [(i, (i + step) % ring) for i in range(ring)])
            total = total + piece.astype(F32)
        terms = total.astype(BF16)
    terms = terms.reshape(2, -1, 256)
    mine = lax.dynamic_index_in_dim(terms, half, 0, keepdims=False)
    theirs = lax.dynamic_index_in_dim(terms, 1 - half, 0, keepdims=False)
    theirs = lax.ppermute(theirs, "half", [(0, 1), (1, 0)])
    total = (mine.astype(F32) + theirs.astype(F32)).astype(BF16)
    span = total.shape[0]
    spread = jnp.broadcast_to(total[None], (peers, span, 256))
    spread = lax.all_to_all(spread, SP, 0, 0, tiled=True)
    grad_weight = kernel(
        widen_kernel,
        shape((2 * span, 2048), F32),
        1 << 20,
        grid=(4,),
        in_specs=[pl.BlockSpec((2, 2, span, 256), lambda h: (0, h, 0, 0))],
        out_specs=pl.BlockSpec((2 * span, 512), lambda h: (0, h)),
    )(spread.reshape(2, 8, span, 256))
    return grad_query[None], grad_value[None], grad_input[None], grad_weight


def solution(mesh):
    dp = mesh.shape["dp"]
    outer = (dp // 2, 2) if dp > 1 else (1, 1)
    finer = Mesh(mesh.devices.reshape(2, 8, *outer), SP + DP)
    part = P(DP, SP, None)
    return jax.shard_map(
        shards,
        mesh=finer,
        in_specs=(part, part, part, part, part, part, P(DP, None)),
        out_specs=(part, part, part, P(DP, None)),
        check_vma=False,
    )
```

time: 214 us -> 313 us (1.46)
  Pallas kernels: 37.3 us -> 125 us
  starting transfers between devices: 33.7 us -> 60.6 us
  waiting for transfers between devices: 95.4 us -> 114 us
  blocking collectives: 18.3 us -> 0 us
  between operations: 14.2 us -> 0.83 us
  local copies, waits for them, and re-layouts: 9.28 us -> 5.16 us
    pallas_call x7, Pallas kernels: 28.2 us -> 117 us  [the longest x1 96.7 us: shards(): kernel(pack_kernel, pltpu.HBM((8, tokens, 1536), BF16), 1 << 20, (pltpu.S...]
    ppermute x3, waiting for transfers between devices: 5.05 us -> 50.8 us  [shards(): lax.ppermute(piece, 'dp_0', [(i, (i + step) % ring) for i in range(ring)])]
    all_to_all x1, waiting for transfers between devices: 21.7 us -> 0.01 us  [shards(): lax.all_to_all(grads.reshape(8, tokens, -1), 'lane', 0, 0, tiled=True)]
    all_to_all x1 -> x0, blocking collectives: 18.3 us -> none  [shards(): spread = lax.all_to_all(spread, SP, 0, 0, tiled=True)]
    ppermute x1, starting transfers between devices: 3.21 us -> 17 us  [shards(): theirs = lax.ppermute(theirs, 'dp_1', [(0, 1), (1, 0)])]
    ppermute x1, waiting for transfers between devices: 17.4 us -> 6.12 us  [shards(): lax.ppermute(far, SP, [(u, (1 - u % 2) * 8 + u // 2) for u in range(peers)])]
    ppermute x0 -> x7, starting transfers between devices: none -> 7.21 us  [the longest x3 4.22 us: shards(): weights.append(lax.ppermute(key_weight, 'dp_0', moves))]
    all_to_all x0 -> x1, waiting for transfers between devices: none -> 5.95 us  [shards(): spread = lax.all_to_all(spread, SP, 0, 0, tiled=True)]
  transfers between devices with their start and end apart: 16 -> 25, of which waited for: 8 -> 7; matrix products, arithmetic and copies ran while one was open for 4% -> 2% of each run, Pallas kernels for 13% -> 9%
where the time goes in v2:
time: 313 us; the launch traced here: 309 us
  Pallas kernels  125 us (40%)
  waiting for transfers between devices  114 us (36%)
  starting transfers between devices  60.6 us (19%)
  local copies, waits for them, and re-layouts  5.16 us (2%)
    pallas_call x1, Pallas kernels, shards(): kernel(pack_kernel, pltpu.HBM((8, tokens, 1536), BF16), 1 << 20, (pltpu.S...  96.7 us
    ppermute x3, waiting for transfers between devices, shards(): lax.ppermute(piece, 'dp_0', [(i, (i + step) % ring) for i in range(ring)])  50.8 us
    ppermute x1, waiting for transfers between devices, shards(): lax.ppermute(layer_input, 'lane', [(i, (i + 4) % 8) for i in range(8)])  45.1 us
    ppermute x1, starting transfers between devices, shards(): theirs = lax.ppermute(theirs, 'dp_1', [(0, 1), (1, 0)])  17 us
    ppermute x6, starting transfers between devices, lane_step(): lax.ppermute(array, 'lane', [(i, i // 4 * 4 + (i + step) % 4) for i in ra...  8.65 us
    pallas_call x1, Pallas kernels, shards(): kernel(home_kernel, (shape((tokens, 2048), BF16), shape((tokens, 4096), B...  7.54 us
    all_to_all x1, starting transfers between devices, shards(): lax.all_to_all(sent, 'lane', 0, 0, tiled=True).reshape(8 * tokens, -1)  6.37 us
  transfers between devices with their start and end apart: 25, of which 7 were waited for; matrix products, arithmetic and copies ran while one was open for 2% of the time, Pallas kernels for 9%

profile of v2, /device:TPU:1, one launch (start us, length us, event | category | flops | bytes accessed | tf_op | source)
XLA Modules:
  0.0 308.5 jit_solution(3687947196921755194)
XLA Ops:
  0.6 96.7 %shard_map.102 = bf16[8,128,1536]{2,1,0:T(8,128)(2,1)} custom-call(bf16[128,2048]{1,0:T(8,128)(2,1)} %bitcast.54, bf16[128,2048]{1,0:T(8,128)(2,1)} %bitcast.55, bf16[128,4096]{1,0:T(8,128)(2,1)} %bitcast.52, bf16[128,4096]{1,0:T(8,128)(2,1)} %bitcast.53), custom_call_target="tpu_custom_call" | custom-call | flops 1048576 | bytes 4194304 | tf_op jit(solution)/shard_map/pallas_call | solution.py:216
  97.3 0.0 copy-start.2
  97.3 6.4 %all-to-all-start = ((bf16[8,128,1536]{2,1,0:T(8,128)(2,1)}), bf16[8,128,1536]{2,1,0:T(8,128)(2,1)S(1)}, u32[]{:S(2)}, u32[]{:S(2)}) async-start(bf16[8,128,1536]{2,1,0:T(8,128)(2,1)} %shard_map.102), calls=%async_computation | async-start | bytes 6291456 | tf_op jit(solution)/shard_map/all_to_all | solution.py:224
  103.7 1.5 collective-permute-start
  105.2 45.1 %collective-permute-done.refs_1_ = bf16[1,128,2048]{2,1,0:T(8,128)(2,1)} collective-permute-done((bf16[1,128,2048]{2,1,0:T(8,128)(2,1)}, bf16[1,128,2048]{2,1,0:T(8,128)(2,1)}, u32[]{:S(2)}, u32[]{:S(2)}) %collective-permute-start) | collective-permute-done | bytes 524320 | tf_op jit(solution)/shard_map/ppermute | solution.py:207
  150.3 0.0 all-to-all-done
  150.3 1.2 collective-permute-start.11
  151.4 2.5 collective-permute-start.14
  154.0 0.7 collective-permute-start.1
  154.6 4.6 %collective-permute-start.2 = (f32[8,128]{1,0:T(8,128)S(1)}, f32[8,128]{1,0:T(8,128)S(1)}, u32[]{:S(2)}, u32[]{:S(2)}) collective-permute-start(f32[8,128]{1,0:T(8,128)S(1)} %get-tuple-element.24), channel_id=1, source_target_pairs={{0,64},{8,0},{16,72},{24,8},{32,80},{40,16},{48,88},{56,24},{64,96... | collective-permute-start | bytes 12296 | tf_op jit(solution)/shard_map/ppermute | solution.py:206
  159.3 6.1 %collective-permute-done.2 = f32[8,128]{1,0:T(8,128)S(1)} collective-permute-done((f32[8,128]{1,0:T(8,128)S(1)}, f32[8,128]{1,0:T(8,128)S(1)}, u32[]{:S(2)}, u32[]{:S(2)}) %collective-permute-start.2) | collective-permute-done | bytes 4128 | tf_op jit(solution)/shard_map/ppermute | solution.py:206
  165.4 1.8 shard_map.103
  167.2 1.0 copy-done
  168.2 2.2 shard_map.104
  170.4 2.3 collective-permute-start.3
  172.7 1.9 collective-permute-start.12
  174.6 0.3 collective-permute-start.13
  174.9 1.5 collective-permute-start.15
  176.4 1.2 collective-permute-start.16
  177.6 1.0 copy-done.1
  178.7 5.6 %shard_map.105.part_ref = bf16[1024,1024]{1,0:T(8,128)(2,1)} custom-call(bf16[1024,1536]{1,0:T(8,128)(2,1)S(1)} %bitcast.46, f32[40,128]{1,0:T(8,128)S(1)} %get-tuple-element.14.rows_ref, f32[1024,4]{1,0:T(8,128)S(1)} %copy-done.1), custom_call_target="tpu_custom_call" | custom-call | flops 3942645760 | bytes 4194304 | tf_op jit(solution)/shard_map/pallas_call | solution.py:247
  184.3 4.7 %shard_map.106.grads_ref = bf16[1024,1024]{1,0:T(8,128)(2,1)} custom-call(bf16[1024,1536]{1,0:T(8,128)(2,1)S(1)} %bitcast.47, f32[1024,4]{1,0:T(8,128)S(1)} %copy-done.1, bf16[2,256,512]{2,1,0:T(8,128)(2,1)} %collective-permute-done.3.state_ref, bf16[1024,1024]{1,0:T(8,128)(2,1)} %shard_map.105.part_ref), custom_call_target="tpu_custom_call" | custom-call | flops 838860800 | bytes 4194304 | tf_op jit(solution)/shard_map/pallas_call | solution.py:257
  188.9 5.3 %all-to-all-start.1 = ((bf16[8,128,1024]{2,1,0:T(8,128)(2,1)}), bf16[8,128,1024]{2,1,0:T(8,128)(2,1)S(1)}, u32[]{:S(2)}, u32[]{:S(2)}) async-start(bf16[8,128,1024]{2,1,0:T(8,128)(2,1)} %bitcast.51), calls=%async_computation.1 | async-start | bytes 4194304 | tf_op jit(solution)/shard_map/all_to_all | solution.py:271
  194.3 4.4 %collective-permute-done.15.refs_6_ = bf16[1,128,2048]{2,1,0:T(8,128)(2,1)} collective-permute-done((bf16[1,128,2048]{2,1,0:T(8,128)(2,1)}, bf16[1,128,2048]{2,1,0:T(8,128)(2,1)}, u32[]{:S(2)}, u32[]{:S(2)}) %collective-permute-start.15) | collective-permute-done | bytes 524320 | tf_op jit(solution)/shard_map/ppermute | solution.py:227
  198.6 4.7 %shard_map.108 = bf16[2048,256]{1,0:T(8,128)(2,1)S(1)} custom-call(s32[1]{0:T(128)} %bitcast.20.lane_ref, bf16[1024,1024]{1,0:T(8,128)(2,1)} %shard_map.106.grads_ref, bf16[1,128,2048]{2,1,0:T(8,128)(2,1)} %refs_0_.2, bf16[1,128,2048]{2,1,0:T(8,128)(2,1)} %collective-permute-done.refs_1_, bf16[1,128,2048]{2,1,0:T(8,128)(2,1)} %collective-permute-done.11.refs_2_, ...), custom_call_target="tpu_custom_call" | custom-call | flops 1121976320 | bytes 4194304 | tf_op jit(solution)/shard_map/pallas_call | solution.py:281
  203.4 0.8 dynamic-slice_bitcast_fusion
  204.2 17.0 %collective-permute-start.17 = (bf16[4,256,256]{2,1,0:T(8,128)(2,1)}, bf16[4,256,256]{2,1,0:T(8,128)(2,1)}, u32[]{:S(2)}, u32[]{:S(2)}) collective-permute-start(bf16[4,256,256]{2,1,0:T(8,128)(2,1)} %dynamic-slice_bitcast_fusion), channel_id=1, source_target_pairs={{0,1},{1,0},{2,3},{3,2},{4,5},{5,4},{6,7},{7,6},{8,9},{9,8},{10,11... | collective-permute-start | bytes 1572872 | tf_op jit(solution)/shard_map/ppermute | solution.py:305
  221.2 2.5 collective-permute-start.6
  223.6 1.7 collective-permute-start.5
  225.4 2.0 fusion
  227.3 1.1 dynamic-slice_bitcast_fusion.3
  228.4 1.6 collective-permute-start.18
  230.0 0.6 collective-permute-start.19
  230.6 47.0 %collective-permute-done.18 = bf16[256,256]{1,0:T(8,128)(2,1)S(1)} collective-permute-done((bf16[256,256]{1,0:T(8,128)(2,1)S(1)}, bf16[256,256]{1,0:T(8,128)(2,1)S(1)}, u32[]{:S(2)}, u32[]{:S(2)}) %collective-permute-start.18) | collective-permute-done | bytes 131104 | tf_op jit(solution)/shard_map/ppermute | solution.py:310
  277.6 3.8 %collective-permute-done.20 = bf16[256,256]{1,0:T(8,128)(2,1)S(1)} collective-permute-done((bf16[256,256]{1,0:T(8,128)(2,1)S(1)}, bf16[256,256]{1,0:T(8,128)(2,1)S(1)}, u32[]{:S(2)}, u32[]{:S(2)}) %collective-permute-start.20) | collective-permute-done | bytes 131104 | tf_op jit(solution)/shard_map/ppermute | solution.py:310
  281.4 1.0 fusion.3
  282.4 0.1 collective-permute-start.21
  282.5 2.4 collective-permute-start.7
  284.9 0.1 collective-permute-start.10
  285.0 0.4 collective-permute-start.8
  285.4 0.1 collective-permute-start.9
  285.5 1.6 collective-permute-done.21
  287.1 1.1 broadcast_in_dim.22
  288.2 4.8 %all-to-all-start.2 = ((bf16[16,128,256]{2,1,0:T(8,128)(2,1)}), bf16[16,128,256]{2,1,0:T(8,128)(2,1)S(1)}, u32[]{:S(2)}, u32[]{:S(2)}) async-start(bf16[16,128,256]{2,1,0:T(8,128)(2,1)} %broadcast_in_dim.22), calls=%async_computation.2 | async-start | bytes 2097152 | tf_op jit(solution)/shard_map/all_to_all | solution.py:320
  293.0 0.1 stack.35.owner_ref
  293.1 7.5 %shard_map.107 = (bf16[128,2048]{1,0:T(8,128)(2,1)}, bf16[128,4096]{1,0:T(8,128)(2,1)}, bf16[128,2048]{1,0:T(8,128)(2,1)}) custom-call(s32[8]{0:T(128)S(1)} %stack.35.owner_ref, bf16[8,128,1024]{2,1,0:T(8,128)(2,1)S(1)} %all-to-all-done.1.home_ref, bf16[256,2048]{1,0:T(8,128)(2,1)} %refs_0_.1, bf16[256,2048]{1,0:T(8,128)(2,1)} %collective-permute-done.4.refs_1_, ...), custom_call_target="tpu_custom_call" | custom-call | flops 1121976320 | bytes 4194304 | tf_op jit(solution)/shard_map/pallas_call | solution.py:272
  300.7 6.0 %all-to-all-done.2 = bf16[16,128,256]{2,1,0:T(8,128)(2,1)S(1)} async-done(((bf16[16,128,256]{2,1,0:T(8,128)(2,1)}), bf16[16,128,256]{2,1,0:T(8,128)(2,1)S(1)}, u32[]{:S(2)}, u32[]{:S(2)}) %all-to-all-start.2) | async-done | bytes 1048608 | tf_op jit(solution)/shard_map/all_to_all | solution.py:320
  306.6 1.9 shard_map.109
  (27 shorter events, 0.1 us)
Async XLA Ops:
  97.3 56.7 %copy-start.2 = (f32[1,1,2048]{2,1,0:T(1,128)S(1)}, f32[1,1,2048]{2,1,0:T(1,128)}, u32[]{:S(2)}) copy-start(f32[1,1,2048]{2,1,0:T(1,128)} %param.12) | copy-start | bytes 24580
  97.3 52.9 %all-to-all-start = ((bf16[8,128,1536]{2,1,0:T(8,128)(2,1)}), bf16[8,128,1536]{2,1,0:T(8,128)(2,1)S(1)}, u32[]{:S(2)}, u32[]{:S(2)}) async-start(bf16[8,128,1536]{2,1,0:T(8,128)(2,1)} %shard_map.102), calls=%async_computation | async-start | bytes 6291456 | tf_op jit(solution)/shard_map/all_to_all | solution.py:224
  103.7 46.5 %collective-permute-start = (bf16[1,128,2048]{2,1,0:T(8,128)(2,1)}, bf16[1,128,2048]{2,1,0:T(8,128)(2,1)}, u32[]{:S(2)}, u32[]{:S(2)}) collective-permute-start(bf16[1,128,2048]{2,1,0:T(8,128)(2,1)} %refs_0_.2), channel_id=1, source_target_pairs={{0,32},{8,40},{16,48},{24,56},{32,0},{40,8},{48,16},{56,24},{1,33}... | collective-permute-start | bytes 1572872 | tf_op jit(solution)/shard_map/ppermute | solution.py:207
  150.3 24.7 %collective-permute-start.11 = (bf16[1,128,2048]{2,1,0:T(8,128)(2,1)}, bf16[1,128,2048]{2,1,0:T(8,128)(2,1)}, u32[]{:S(2)}, u32[]{:S(2)}) collective-permute-start(bf16[1,128,2048]{2,1,0:T(8,128)(2,1)} %refs_0_.2), channel_id=1, source_target_pairs={{0,8},{8,16},{16,24},{24,0},{32,40},{40,48},{48,56},{56,32},{1,9},... | collective-permute-start | bytes 1572872 | tf_op jit(solution)/shard_map/ppermute | solution.py:227
  151.4 25.0 %collective-permute-start.14 = (bf16[1,128,2048]{2,1,0:T(8,128)(2,1)}, bf16[1,128,2048]{2,1,0:T(8,128)(2,1)}, u32[]{:S(2)}, u32[]{:S(2)}) collective-permute-start(bf16[1,128,2048]{2,1,0:T(8,128)(2,1)} %collective-permute-done.refs_1_), channel_id=1, source_target_pairs={{0,24},{8,0},{16,8},{24,16},{32,56},{40,32},{48,40},{56,48},{1,25}... | collective-permute-start | bytes 1572872 | tf_op jit(solution)/shard_map/ppermute | solution.py:227
  154.0 5.3 %collective-permute-start.1 = (f32[8,128]{1,0:T(8,128)S(1)}, f32[8,128]{1,0:T(8,128)S(1)}, u32[]{:S(2)}, u32[]{:S(2)}) collective-permute-start(f32[8,128]{1,0:T(8,128)S(1)} %get-tuple-element.23), channel_id=1, source_target_pairs={{0,0},{8,64},{16,8},{24,72},{32,16},{40,80},{48,24},{56,88},{64,32... | collective-permute-start | bytes 12296 | tf_op jit(solution)/shard_map/ppermute | solution.py:205
  154.6 10.8 %collective-permute-start.2 = (f32[8,128]{1,0:T(8,128)S(1)}, f32[8,128]{1,0:T(8,128)S(1)}, u32[]{:S(2)}, u32[]{:S(2)}) collective-permute-start(f32[8,128]{1,0:T(8,128)S(1)} %get-tuple-element.24), channel_id=1, source_target_pairs={{0,64},{8,0},{16,72},{24,8},{32,80},{40,16},{48,88},{56,24},{64,96... | collective-permute-start | bytes 12296 | tf_op jit(solution)/shard_map/ppermute | solution.py:206
  167.2 1.0 copy-start
  170.4 13.9 %collective-permute-start.3 = (bf16[2,256,512]{2,1,0:T(8,128)(2,1)}, bf16[2,256,512]{2,1,0:T(8,128)(2,1)}, u32[]{:S(2)}, u32[]{:S(2)}) collective-permute-start(bf16[2,256,512]{2,1,0:T(8,128)(2,1)} %shard_map.104), channel_id=1, source_target_pairs={{0,64},{8,72},{16,80},{24,88},{32,96},{40,104},{48,112},{56,120},{... | collective-permute-start | bytes 1572872 | tf_op jit(solution)/shard_map/ppermute | solution.py:246
  172.7 21.6 %collective-permute-start.12 = (bf16[1,128,2048]{2,1,0:T(8,128)(2,1)}, bf16[1,128,2048]{2,1,0:T(8,128)(2,1)}, u32[]{:S(2)}, u32[]{:S(2)}) collective-permute-start(bf16[1,128,2048]{2,1,0:T(8,128)(2,1)} %refs_0_.2), channel_id=1, source_target_pairs={{0,24},{8,0},{16,8},{24,16},{32,56},{40,32},{48,40},{56,48},{1,25}... | collective-permute-start | bytes 1572872 | tf_op jit(solution)/shard_map/ppermute | solution.py:227
  174.6 19.6 %collective-permute-start.13 = (bf16[1,128,2048]{2,1,0:T(8,128)(2,1)}, bf16[1,128,2048]{2,1,0:T(8,128)(2,1)}, u32[]{:S(2)}, u32[]{:S(2)}) collective-permute-start(bf16[1,128,2048]{2,1,0:T(8,128)(2,1)} %collective-permute-done.refs_1_), channel_id=1, source_target_pairs={{0,8},{8,16},{16,24},{24,0},{32,40},{40,48},{48,56},{56,32},{1,9},... | collective-permute-start | bytes 1572872 | tf_op jit(solution)/shard_map/ppermute | solution.py:227
  174.9 23.7 %collective-permute-start.15 = (bf16[1,128,2048]{2,1,0:T(8,128)(2,1)}, bf16[1,128,2048]{2,1,0:T(8,128)(2,1)}, u32[]{:S(2)}, u32[]{:S(2)}) collective-permute-start(bf16[1,128,2048]{2,1,0:T(8,128)(2,1)} %collective-permute-done.11.refs_2_), channel_id=1, source_target_pairs={{0,8},{8,16},{16,24},{24,0},{32,40},{40,48},{48,56},{56,32},{1,9},... | collective-permute-start | bytes 1572872 | tf_op jit(solution)/shard_map/ppermute | solution.py:227
  176.4 22.2 %collective-permute-start.16 = (bf16[1,128,2048]{2,1,0:T(8,128)(2,1)}, bf16[1,128,2048]{2,1,0:T(8,128)(2,1)}, u32[]{:S(2)}, u32[]{:S(2)}) collective-permute-start(bf16[1,128,2048]{2,1,0:T(8,128)(2,1)} %collective-permute-done.14.refs_5_), channel_id=1, source_target_pairs={{0,24},{8,0},{16,8},{24,16},{32,56},{40,32},{48,40},{56,48},{1,25}... | collective-permute-start | bytes 1572872 | tf_op jit(solution)/shard_map/ppermute | solution.py:227
  177.6 1.0 copy-start.1
  188.9 98.2 %all-to-all-start.1 = ((bf16[8,128,1024]{2,1,0:T(8,128)(2,1)}), bf16[8,128,1024]{2,1,0:T(8,128)(2,1)S(1)}, u32[]{:S(2)}, u32[]{:S(2)}) async-start(bf16[8,128,1024]{2,1,0:T(8,128)(2,1)} %bitcast.51), calls=%async_computation.1 | async-start | bytes 4194304 | tf_op jit(solution)/shard_map/all_to_all | solution.py:271
  204.2 21.2 %collective-permute-start.17 = (bf16[4,256,256]{2,1,0:T(8,128)(2,1)}, bf16[4,256,256]{2,1,0:T(8,128)(2,1)}, u32[]{:S(2)}, u32[]{:S(2)}) collective-permute-start(bf16[4,256,256]{2,1,0:T(8,128)(2,1)} %dynamic-slice_bitcast_fusion), channel_id=1, source_target_pairs={{0,1},{1,0},{2,3},{3,2},{4,5},{5,4},{6,7},{7,6},{8,9},{9,8},{10,11... | collective-permute-start | bytes 1572872 | tf_op jit(solution)/shard_map/ppermute | solution.py:305
  221.2 63.7 %collective-permute-start.6 = (bf16[256,2048]{1,0:T(8,128)(2,1)}, bf16[256,2048]{1,0:T(8,128)(2,1)}, u32[]{:S(2)}, u32[]{:S(2)}) collective-permute-start(bf16[256,2048]{1,0:T(8,128)(2,1)} %refs_0_.1), channel_id=1, source_target_pairs={{0,6},{2,0},{4,2},{6,4},{1,7},{3,1},{5,3},{7,5},{8,14},{10,8},{12,... | collective-permute-start | bytes 3145736 | tf_op jit(solution)/shard_map/ppermute | solution.py:234
  223.6 61.3 %collective-permute-start.4 = (bf16[256,2048]{1,0:T(8,128)(2,1)}, bf16[256,2048]{1,0:T(8,128)(2,1)}, u32[]{:S(2)}, u32[]{:S(2)}) collective-permute-start(bf16[256,2048]{1,0:T(8,128)(2,1)} %refs_0_.1), channel_id=1, source_target_pairs={{0,2},{2,4},{4,6},{6,0},{1,3},{3,5},{5,7},{7,1},{8,10},{10,12},{12... | collective-permute-start | bytes 3145736 | tf_op jit(solution)/shard_map/ppermute | solution.py:234
  223.6 61.7 %collective-permute-start.5 = (bf16[256,2048]{1,0:T(8,128)(2,1)}, bf16[256,2048]{1,0:T(8,128)(2,1)}, u32[]{:S(2)}, u32[]{:S(2)}) collective-permute-start(bf16[256,2048]{1,0:T(8,128)(2,1)} %refs_0_.1), channel_id=1, source_target_pairs={{0,4},{2,6},{4,0},{6,2},{1,5},{3,7},{5,1},{7,3},{8,12},{10,14},{12... | collective-permute-start | bytes 3145736 | tf_op jit(solution)/shard_map/ppermute | solution.py:234
  228.4 49.2 %collective-permute-start.18 = (bf16[256,256]{1,0:T(8,128)(2,1)S(1)}, bf16[256,256]{1,0:T(8,128)(2,1)S(1)}, u32[]{:S(2)}, u32[]{:S(2)}) collective-permute-start(bf16[256,256]{1,0:T(8,128)(2,1)S(1)} %get-tuple-element.20), channel_id=1, source_target_pairs={{0,2},{2,4},{4,6},{6,0},{1,3},{3,5},{5,7},{7,1},{8,10},{10,12},{12... | collective-permute-start | bytes 393224 | tf_op jit(solution)/shard_map/ppermute | solution.py:310
  230.0 47.6 %collective-permute-start.19 = (bf16[256,256]{1,0:T(8,128)(2,1)S(1)}, bf16[256,256]{1,0:T(8,128)(2,1)S(1)}, u32[]{:S(2)}, u32[]{:S(2)}) collective-permute-start(bf16[256,256]{1,0:T(8,128)(2,1)S(1)} %get-tuple-element.22), channel_id=1, source_target_pairs={{0,4},{2,6},{4,0},{6,2},{1,5},{3,7},{5,1},{7,3},{8,12},{10,14},{12... | collective-permute-start | bytes 393224 | tf_op jit(solution)/shard_map/ppermute | solution.py:310
  277.6 3.8 %collective-permute-start.20 = (bf16[256,256]{1,0:T(8,128)(2,1)S(1)}, bf16[256,256]{1,0:T(8,128)(2,1)S(1)}, u32[]{:S(2)}, u32[]{:S(2)}) collective-permute-start(bf16[256,256]{1,0:T(8,128)(2,1)S(1)} %get-tuple-element.21), channel_id=1, source_target_pairs={{0,6},{2,0},{4,2},{6,4},{1,7},{3,1},{5,3},{7,5},{8,14},{10,8},{12,... | collective-permute-start | bytes 393224 | tf_op jit(solution)/shard_map/ppermute | solution.py:310
  282.4 4.7 %collective-permute-start.21 = (bf16[128,256]{1,0:T(8,128)(2,1)S(1)}, bf16[128,256]{1,0:T(8,128)(2,1)S(1)}, u32[]{:S(2)}, u32[]{:S(2)}) collective-permute-start(bf16[128,256]{1,0:T(8,128)(2,1)S(1)} %dynamic-slice_bitcast_fusion.4), channel_id=1, source_target_pairs={{0,64},{64,0},{1,65},{65,1},{2,66},{66,2},{3,67},{67,3},{4,68},{68... | collective-permute-start | bytes 196616 | tf_op jit(solution)/shard_map/ppermute | solution.py:316
  282.5 10.6 %collective-permute-start.7 = (bf16[256,2048]{1,0:T(8,128)(2,1)}, bf16[256,2048]{1,0:T(8,128)(2,1)}, u32[]{:S(2)}, u32[]{:S(2)}) collective-permute-start(bf16[256,2048]{1,0:T(8,128)(2,1)} %refs_0_.1), channel_id=1, source_target_pairs={{0,1},{1,0},{2,3},{3,2},{4,5},{5,4},{6,7},{7,6},{8,9},{9,8},{10,11... | collective-permute-start | bytes 3145736 | tf_op jit(solution)/shard_map/ppermute | solution.py:237
  284.9 8.3 %collective-permute-start.10 = (bf16[256,2048]{1,0:T(8,128)(2,1)}, bf16[256,2048]{1,0:T(8,128)(2,1)}, u32[]{:S(2)}, u32[]{:S(2)}) collective-permute-start(bf16[256,2048]{1,0:T(8,128)(2,1)} %collective-permute-done.6.refs_3_), channel_id=1, source_target_pairs={{0,1},{1,0},{2,3},{3,2},{4,5},{5,4},{6,7},{7,6},{8,9},{9,8},{10,11... | collective-permute-start | bytes 3145736 | tf_op jit(solution)/shard_map/ppermute | solution.py:237
  285.0 8.2 %collective-permute-start.8 = (bf16[256,2048]{1,0:T(8,128)(2,1)}, bf16[256,2048]{1,0:T(8,128)(2,1)}, u32[]{:S(2)}, u32[]{:S(2)}) collective-permute-start(bf16[256,2048]{1,0:T(8,128)(2,1)} %collective-permute-done.4.refs_1_), channel_id=1, source_target_pairs={{0,1},{1,0},{2,3},{3,2},{4,5},{5,4},{6,7},{7,6},{8,9},{9,8},{10,11... | collective-permute-start | bytes 3145736 | tf_op jit(solution)/shard_map/ppermute | solution.py:237
  285.4 7.8 %collective-permute-start.9 = (bf16[256,2048]{1,0:T(8,128)(2,1)}, bf16[256,2048]{1,0:T(8,128)(2,1)}, u32[]{:S(2)}, u32[]{:S(2)}) collective-permute-start(bf16[256,2048]{1,0:T(8,128)(2,1)} %collective-permute-done.5.refs_2_), channel_id=1, source_target_pairs={{0,1},{1,0},{2,3},{3,2},{4,5},{5,4},{6,7},{7,6},{8,9},{9,8},{10,11... | collective-permute-start | bytes 3145736 | tf_op jit(solution)/shard_map/ppermute | solution.py:237
  288.2 18.4 %all-to-all-start.2 = ((bf16[16,128,256]{2,1,0:T(8,128)(2,1)}), bf16[16,128,256]{2,1,0:T(8,128)(2,1)S(1)}, u32[]{:S(2)}, u32[]{:S(2)}) async-start(bf16[16,128,256]{2,1,0:T(8,128)(2,1)} %broadcast_in_dim.22), calls=%async_computation.2 | async-start | bytes 2097152 | tf_op jit(solution)/shard_map/all_to_all | solution.py:320

commit v3 on v2

--- a/solution.py
+++ b/solution.py
@@ -136,23 +136,34 @@
     return jax.ShapeDtypeStruct(dims, dtype)
 
 
-def pack_kernel(query_ref, key_ref, value_ref, grad_ref, out_ref, sems):
-    copies, at = [], 0
-    for source in (query_ref, key_ref, value_ref, grad_ref):
-        width = source.shape[1] // HEADS
-        for h in range(HEADS):
-            copies.append(
-                pltpu.make_async_copy(
-                    source.at[:, pl.ds(h * width, width)],
-                    out_ref.at[h, :, pl.ds(at, width)],
-                    sems.at[len(copies)],
-                )
-            )
-        at += width
-    for copy in copies:
-        copy.start()
-    for copy in copies:
-        copy.wait()
+def pack_kernel(half_ref, query_ref, key_ref, value_ref, grad_ref, out_ref):
+    del half_ref
+    out_ref[0, :, 0:256] = query_ref[...]
+    out_ref[0, :, 256:512] = key_ref[...]
+    out_ref[0, :, 512:1024] = value_ref[...]
+    out_ref[0, :, 1024:1536] = grad_ref[...]
+
+
+def pack(half, arrays):
+    def columns(width):
+        return pl.BlockSpec((BLOCK, width), lambda h, half: (0, (h + 4 * half[0]) & 7))
+
+    return pl.pallas_call(
+        pack_kernel,
+        out_shape=pltpu.HBM((HEADS, BLOCK, 1536), BF16),
+        grid_spec=pltpu.PrefetchScalarGridSpec(
+            num_scalar_prefetch=1,
+            grid=(HEADS,),
+            in_specs=[columns(a.shape[1] // HEADS) for a in arrays],
+            out_specs=pl.BlockSpec((1, BLOCK, 1536), lambda h, half: (h, 0, 0)),
+        ),
+        cost_estimate=pl.CostEstimate(flops=1 << 20, bytes_accessed=6 << 20, transcendentals=0),
+        compiler_params=pltpu.CompilerParams(vmem_limit_bytes=16 << 20),
+    )(half.reshape(1), *[in_hbm(a) for a in arrays])
+
+
+def worker(half, head):
+    return half * 8 + (head + 4 * half) % 8
 
 
 STEPS = ((0, 0), (1, 0), (0, 3), (0, 1), (1, 3), (1, 1), (0, 2), (1, 2))
@@ -170,23 +181,24 @@
     refs[-1][...] = total.astype(BF16)
 
 
-def home_kernel(owner_ref, home_ref, *refs):
+def home_kernel(half_ref, owner_ref, home_ref, *refs):
     weights, (query_ref, value_ref, input_ref, key_ref) = refs[:-4], refs[-4:]
     for h in range(HEADS):
-        key_ref[:, h * 256 : h * 256 + 256] = home_ref[h, :, 0:256]
-        query_ref[:, h * 256 : h * 256 + 256] = home_ref[h, :, 256:512]
-        value_ref[:, h * 512 : h * 512 + 512] = home_ref[h, :, 512:1024]
+        lane = (h + 4 * half_ref[0]) & 7
+        key_ref[:, h * 256 : h * 256 + 256] = home_ref[lane, :, 0:256]
+        query_ref[:, h * 256 : h * 256 + 256] = home_ref[lane, :, 256:512]
+        value_ref[:, h * 512 : h * 512 + 512] = home_ref[lane, :, 512:1024]
     for k, weight in enumerate(weights):
         span = weight.shape[0]
         at = pl.multiple_of(owner_ref[k] * span, span)
         input_ref[:, pl.ds(at, span)] = dot(key_ref[...], weight[...], NT).astype(BF16)
 
 
-def widen_kernel(in_ref, out_ref):
-    for s in range(2):
+def widen_kernel(first_ref, second_ref, out_ref):
+    span = first_ref.shape[2]
+    for s, ref in enumerate((first_ref, second_ref)):
         for h in range(2):
-            span = in_ref.shape[2]
-            out_ref[s * span : s * span + span, h * 256 : h * 256 + 256] = in_ref[s, h].astype(F32)
+            out_ref[s * span : s * span + span, h * 256 : h * 256 + 256] = ref[0, h].astype(F32)
 
 
 def shards(layer_input, queries, key_vectors, values, cotangent, log_decay, key_weight):
@@ -202,25 +214,17 @@
     own = lane % 2
     near = lax.dynamic_index_in_dim(decay, own, 0, keepdims=False)
     far = lax.dynamic_index_in_dim(decay, 1 - own, 0, keepdims=False)
-    near = lax.ppermute(near, SP, [(u, u % 2 * 8 + u // 2) for u in range(peers)])
-    far = lax.ppermute(far, SP, [(u, (1 - u % 2) * 8 + u // 2) for u in range(peers)])
+    near = lax.ppermute(near, SP, [(u, worker(u % 2, u // 2)) for u in range(peers)])
+    far = lax.ppermute(far, SP, [(u, worker(1 - u % 2, u // 2)) for u in range(peers)])
     deep = lax.ppermute(layer_input, "lane", [(i, (i + 4) % 8) for i in range(8)])
     lam = jnp.where(half == 0, jnp.concatenate([near, far]), jnp.concatenate([far, near]))
     rows, tall = kernel(decay_kernel, (shape((40, 128), F32), pltpu.HBM((1024, 4), F32)), 1 << 20)(
         lam, jnp.full((1, 128), half, jnp.int32)
     )
 
-    outside = pl.BlockSpec(memory_space=pltpu.HBM)
     whole = pl.BlockSpec(memory_space=pltpu.VMEM)
     scalars = pl.BlockSpec(memory_space=pltpu.SMEM)
-    sent = kernel(
-        pack_kernel,
-        pltpu.HBM((8, tokens, 1536), BF16),
-        1 << 20,
-        (pltpu.SemaphoreType.DMA((32,)),),
-        in_specs=[outside] * 4,
-        out_specs=outside,
-    )(*[in_hbm(a[0]) for a in (queries, key_vectors, values, cotangent)])
+    sent = pack(half, [a[0] for a in (queries, key_vectors, values, cotangent)])
     units = lax.all_to_all(sent, "lane", 0, 0, tiled=True).reshape(8 * tokens, -1)
 
     def lane_step(array, step):
@@ -237,13 +241,13 @@
         weights += [lax.ppermute(w, "dp_1", [(0, 1), (1, 0)]) for w in weights]
         owners += [o + 1 - 2 * core for o in owners]
 
-    own, deep, units = lax.optimization_barrier((layer_input, deep, units))
+    own = layer_input
     own_before, own_after = lane_step(own, 1), lane_step(own, 3)
     deep_before, deep_after = lane_step(deep, 1), lane_step(deep, 3)
     own_last, deep_last = lane_step(own_before, 1), lane_step(deep_after, 3)
 
     state = kernel(boundary_kernel, pltpu.HBM((2, 256, 512), BF16), 540 << 20)(units, tall)
-    state = lax.ppermute(state, SP, [(u, (u + 8) % 16) for u in range(peers)])
+    state = lax.ppermute(state, SP, [(u, u ^ 12) for u in range(peers)])
     part = kernel(
         inside_kernel,
         pltpu.HBM((1024, 1024), BF16),
@@ -274,9 +278,9 @@
         (shape((tokens, 2048), BF16), shape((tokens, 4096), BF16), shape((tokens, 2048), BF16)),
         1070 << 20,
         (pltpu.VMEM((tokens, 2048), BF16),),
-        in_specs=[scalars] + [whole] * (1 + len(weights)),
+        in_specs=[scalars] * 2 + [whole] * (1 + len(weights)),
         out_specs=(whole, whole, whole),
-    )(jnp.stack(owners), home, *weights)
+    )(half.reshape(1), jnp.stack(owners), home, *weights)
 
     terms = kernel(
         term_kernel,
@@ -313,7 +317,7 @@
     terms = terms.reshape(2, -1, 256)
     mine = lax.dynamic_index_in_dim(terms, half, 0, keepdims=False)
     theirs = lax.dynamic_index_in_dim(terms, 1 - half, 0, keepdims=False)
-    theirs = lax.ppermute(theirs, "half", [(0, 1), (1, 0)])
+    theirs = lax.ppermute(theirs, SP, [(u, u ^ 12) for u in range(peers)])
     total = (mine.astype(F32) + theirs.astype(F32)).astype(BF16)
     span = total.shape[0]
     spread = jnp.broadcast_to(total[None], (peers, span, 256))
@@ -323,9 +327,12 @@
         shape((2 * span, 2048), F32),
         1 << 20,
         grid=(4,),
-        in_specs=[pl.BlockSpec((2, 2, span, 256), lambda h: (0, h, 0, 0))],
+        in_specs=[
+            pl.BlockSpec((1, 2, span, 256), lambda h: (0, h, 0, 0)),
+            pl.BlockSpec((1, 2, span, 256), lambda h: (1, (h + 2) & 3, 0, 0)),
+        ],
         out_specs=pl.BlockSpec((2 * span, 512), lambda h: (0, h)),
-    )(spread.reshape(2, 8, span, 256))
+    )(*[spread.reshape(2, 8, span, 256)] * 2)
     return grad_query[None], grad_value[None], grad_input[None], grad_weight
 
 

time: 313 us -> 198 us (0.63); the launches traced: 309 us -> 198 us
  Pallas kernels: 125 us -> 34.5 us
  waiting for transfers between devices: 114 us -> 95 us
  starting transfers between devices: 60.6 us -> 63.8 us
    pallas_call x1, Pallas kernels: 96.7 us -> 6.32 us  [pack(): pl.pallas_call(pack_kernel, out_shape=pltpu.HBM((HEADS, BLOCK, 1536), BF1...]
    ppermute x3, waiting for transfers between devices: 50.8 us -> 4.87 us  [shards(): lax.ppermute(piece, 'dp_0', [(i, (i + step) % ring) for i in range(ring)])]
    ppermute x3, waiting for transfers between devices: 0.01 us -> 18.9 us  [shards(): weights.append(lax.ppermute(key_weight, 'dp_0', moves))]
    ppermute x1, starting transfers between devices: 17 us -> 3.05 us  [shards(): theirs = lax.ppermute(theirs, 'dp_1', [(0, 1), (1, 0)])]
    ppermute x4, starting transfers between devices: 2.98 us -> 12.9 us  [shards(): weights += [lax.ppermute(w, 'dp_1', [(0, 1), (1, 0)]) for w in weights]]
    all_to_all x1, waiting for transfers between devices: 5.95 us -> 10.6 us  [shards(): spread = lax.all_to_all(spread, SP, 0, 0, tiled=True)]
    ppermute x6, starting transfers between devices: 8.65 us -> 12.3 us  [lane_step(): lax.ppermute(array, 'lane', [(i, i // 4 * 4 + (i + step) % 4) for i in ra...]
    ppermute x6, waiting for transfers between devices: 4.4 us -> 7.94 us  [lane_step(): lax.ppermute(array, 'lane', [(i, i // 4 * 4 + (i + step) % 4) for i in ra...]
  transfers between devices with their start and end apart: 25 -> 25, of which waited for: 7 -> 13; matrix products, arithmetic and copies ran while one was open for 2% -> 0% of each run, Pallas kernels for 9% -> 8%
where the time goes in v3:
time: 198 us
  waiting for transfers between devices  95 us (48%)
  starting transfers between devices  63.8 us (32%)
  Pallas kernels  34.5 us (17%)
  local copies, waits for them, and re-layouts  3.34 us (2%)
    ppermute x1, waiting for transfers between devices, shards(): lax.ppermute(layer_input, 'lane', [(i, (i + 4) % 8) for i in range(8)])  43.9 us
    ppermute x3, waiting for transfers between devices, shards(): weights.append(lax.ppermute(key_weight, 'dp_0', moves))  18.9 us
    ppermute x4, starting transfers between devices, shards(): weights += [lax.ppermute(w, 'dp_1', [(0, 1), (1, 0)]) for w in weights]  12.9 us
    ppermute x6, starting transfers between devices, lane_step(): lax.ppermute(array, 'lane', [(i, i // 4 * 4 + (i + step) % 4) for i in ra...  12.3 us
    all_to_all x1, waiting for transfers between devices, shards(): spread = lax.all_to_all(spread, SP, 0, 0, tiled=True)  10.6 us
    ppermute x6, waiting for transfers between devices, lane_step(): lax.ppermute(array, 'lane', [(i, i // 4 * 4 + (i + step) % 4) for i in ra...  7.94 us
    pallas_call x1, Pallas kernels, shards(): kernel(home_kernel, (shape((tokens, 2048), BF16), shape((tokens, 4096), B...  7.53 us
    all_to_all x1, starting transfers between devices, shards(): lax.all_to_all(sent, 'lane', 0, 0, tiled=True).reshape(8 * tokens, -1)  6.49 us
  transfers between devices with their start and end apart: 25, of which 13 were waited for; matrix products, arithmetic and copies ran while one was open for 0% of the time, Pallas kernels for 8%

profile of v3, /device:TPU:1, one launch (start us, length us, event | category | flops | bytes accessed | tf_op | source)
XLA Modules:
  0.0 197.6 jit_solution(15627289947119184468)
XLA Ops:
  0.6 6.3 %shard_map.102 = bf16[8,128,1536]{2,1,0:T(8,128)(2,1)} custom-call(s32[1]{0:T(128)} %bitcast.half_ref, bf16[128,2048]{1,0:T(8,128)(2,1)} %bitcast.56, bf16[128,2048]{1,0:T(8,128)(2,1)} %bitcast.57, bf16[128,4096]{1,0:T(8,128)(2,1)} %bitcast.54, bf16[128,4096]{1,0:T(8,128)(2,1)} %bitcast.55), custom_call_target="tpu_custom_call" | custom-call | flops 1048576 | bytes 6291456 | tf_op jit(solution)/shard_map/pallas_call | solution.py:151
  7.0 6.5 %all-to-all-start = ((bf16[8,128,1536]{2,1,0:T(8,128)(2,1)}), bf16[8,128,1536]{2,1,0:T(8,128)(2,1)S(1)}, u32[]{:S(2)}, u32[]{:S(2)}) async-start(bf16[8,128,1536]{2,1,0:T(8,128)(2,1)} %shard_map.102), calls=%async_computation | async-start | bytes 6291456 | tf_op jit(solution)/shard_map/all_to_all | solution.py:228
  13.5 1.5 collective-permute-start.10
  14.9 1.2 collective-permute-start.11
  16.1 43.9 %collective-permute-done.10.refs_1_ = bf16[1,128,2048]{2,1,0:T(8,128)(2,1)} collective-permute-done((bf16[1,128,2048]{2,1,0:T(8,128)(2,1)}, bf16[1,128,2048]{2,1,0:T(8,128)(2,1)}, u32[]{:S(2)}, u32[]{:S(2)}) %collective-permute-start.10) | collective-permute-done | bytes 524320 | tf_op jit(solution)/shard_map/ppermute | solution.py:219
  60.0 3.7 %collective-permute-start.14 = (bf16[1,128,2048]{2,1,0:T(8,128)(2,1)}, bf16[1,128,2048]{2,1,0:T(8,128)(2,1)}, u32[]{:S(2)}, u32[]{:S(2)}) collective-permute-start(bf16[1,128,2048]{2,1,0:T(8,128)(2,1)} %collective-permute-done.10.refs_1_), channel_id=1, source_target_pairs={{0,24},{8,0},{16,8},{24,16},{32,56},{40,32},{48,40},{56,48},{1,25}... | collective-permute-start | bytes 1572872 | tf_op jit(solution)/shard_map/ppermute | solution.py:231
  63.7 0.7 collective-permute-start
  64.4 5.6 %collective-permute-start.1 = (f32[8,128]{1,0:T(8,128)S(1)}, f32[8,128]{1,0:T(8,128)S(1)}, u32[]{:S(2)}, u32[]{:S(2)}) collective-permute-start(f32[8,128]{1,0:T(8,128)S(1)} %get-tuple-element.18), channel_id=1, source_target_pairs={{0,96},{8,0},{16,104},{24,8},{32,112},{40,16},{48,120},{56,24},{64... | collective-permute-start | bytes 12296 | tf_op jit(solution)/shard_map/ppermute | solution.py:218
  70.0 2.3 %collective-permute-done.1 = f32[8,128]{1,0:T(8,128)S(1)} collective-permute-done((f32[8,128]{1,0:T(8,128)S(1)}, f32[8,128]{1,0:T(8,128)S(1)}, u32[]{:S(2)}, u32[]{:S(2)}) %collective-permute-start.1) | collective-permute-done | bytes 4128 | tf_op jit(solution)/shard_map/ppermute | solution.py:218
  72.3 1.8 shard_map.103
  74.0 1.0 copy-done
  75.1 2.2 %shard_map.104 = bf16[2,256,512]{2,1,0:T(8,128)(2,1)} custom-call(bf16[1024,1536]{1,0:T(8,128)(2,1)S(1)} %bitcast.46, f32[1024,4]{1,0:T(8,128)S(1)} %copy-done), custom_call_target="tpu_custom_call" | custom-call | flops 566231040 | bytes 4194304 | tf_op jit(solution)/shard_map/pallas_call | solution.py:249
  77.2 1.8 collective-permute-start.2
  79.1 2.5 %collective-permute-start.12 = (bf16[1,128,2048]{2,1,0:T(8,128)(2,1)}, bf16[1,128,2048]{2,1,0:T(8,128)(2,1)}, u32[]{:S(2)}, u32[]{:S(2)}) collective-permute-start(bf16[1,128,2048]{2,1,0:T(8,128)(2,1)} %refs_0_.3), channel_id=1, source_target_pairs={{0,24},{8,0},{16,8},{24,16},{32,56},{40,32},{48,40},{56,48},{1,25}... | collective-permute-start | bytes 1572872 | tf_op jit(solution)/shard_map/ppermute | solution.py:231
  81.5 2.3 %collective-permute-start.13 = (bf16[1,128,2048]{2,1,0:T(8,128)(2,1)}, bf16[1,128,2048]{2,1,0:T(8,128)(2,1)}, u32[]{:S(2)}, u32[]{:S(2)}) collective-permute-start(bf16[1,128,2048]{2,1,0:T(8,128)(2,1)} %collective-permute-done.10.refs_1_), channel_id=1, source_target_pairs={{0,8},{8,16},{16,24},{24,0},{32,40},{40,48},{48,56},{56,32},{1,9},... | collective-permute-start | bytes 1572872 | tf_op jit(solution)/shard_map/ppermute | solution.py:231
  83.8 1.5 collective-permute-start.15
  85.2 1.2 collective-permute-start.16
  86.5 1.0 copy-done.1
  87.5 5.5 %shard_map.105.part_ref = bf16[1024,1024]{1,0:T(8,128)(2,1)} custom-call(bf16[1024,1536]{1,0:T(8,128)(2,1)S(1)} %bitcast.47, f32[40,128]{1,0:T(8,128)S(1)} %get-tuple-element.10.rows_ref, f32[1024,4]{1,0:T(8,128)S(1)} %copy-done.1), custom_call_target="tpu_custom_call" | custom-call | flops 3942645760 | bytes 4194304 | tf_op jit(solution)/shard_map/pallas_call | solution.py:251
  93.1 4.7 %shard_map.106.grads_ref = bf16[1024,1024]{1,0:T(8,128)(2,1)} custom-call(bf16[1024,1536]{1,0:T(8,128)(2,1)S(1)} %bitcast.48, f32[1024,4]{1,0:T(8,128)S(1)} %copy-done.1, bf16[2,256,512]{2,1,0:T(8,128)(2,1)} %collective-permute-done.2.state_ref, bf16[1024,1024]{1,0:T(8,128)(2,1)} %shard_map.105.part_ref), custom_call_target="tpu_custom_call" | custom-call | flops 838860800 | bytes 4194304 | tf_op jit(solution)/shard_map/pallas_call | solution.py:261
  97.7 7.3 %collective-permute-done.15.refs_6_ = bf16[1,128,2048]{2,1,0:T(8,128)(2,1)} collective-permute-done((bf16[1,128,2048]{2,1,0:T(8,128)(2,1)}, bf16[1,128,2048]{2,1,0:T(8,128)(2,1)}, u32[]{:S(2)}, u32[]{:S(2)}) %collective-permute-start.15) | collective-permute-done | bytes 524320 | tf_op jit(solution)/shard_map/ppermute | solution.py:231
  105.0 0.7 collective-permute-done.16.refs_7_
  105.7 4.7 %shard_map.108 = bf16[2048,256]{1,0:T(8,128)(2,1)S(1)} custom-call(s32[1]{0:T(128)} %bitcast.21.lane_ref, bf16[1024,1024]{1,0:T(8,128)(2,1)} %shard_map.106.grads_ref, bf16[1,128,2048]{2,1,0:T(8,128)(2,1)} %refs_0_.3, bf16[1,128,2048]{2,1,0:T(8,128)(2,1)} %collective-permute-done.10.refs_1_, bf16[1,128,2048]{2,1,0:T(8,128)(2,1)} %collective-permute-done.11.refs_2_, ...), custom_call_target="tpu_custom_call" | custom-call | flops 1121976320 | bytes 4194304 | tf_op jit(solution)/shard_map/pallas_call | solution.py:285
  110.4 3.0 %collective-permute-start.17 = (bf16[4,256,256]{2,1,0:T(8,128)(2,1)S(1)}, bf16[4,256,256]{2,1,0:T(8,128)(2,1)S(1)}, u32[]{:S(2)}, u32[]{:S(2)}) collective-permute-start(bf16[4,256,256]{2,1,0:T(8,128)(2,1)S(1)} %dynamic-slice_bitcast_fusion), channel_id=1, source_target_pairs={{0,1},{1,0},{2,3},{3,2},{4,5},{5,4},{6,7},{7,6},{8,9},{9,8},{10,11... | collective-permute-start | bytes 1572872 | tf_op jit(solution)/shard_map/ppermute | solution.py:309
  113.5 1.5 collective-permute-done.17
  115.2 1.5 collective-permute-start.18
  116.6 2.4 %collective-permute-start.19 = (bf16[256,256]{1,0:T(8,128)(2,1)S(1)}, bf16[256,256]{1,0:T(8,128)(2,1)S(1)}, u32[]{:S(2)}, u32[]{:S(2)}) collective-permute-start(bf16[256,256]{1,0:T(8,128)(2,1)S(1)} %get-tuple-element.16), channel_id=1, source_target_pairs={{0,4},{2,6},{4,0},{6,2},{1,5},{3,7},{5,1},{7,3},{8,12},{10,14},{12... | collective-permute-start | bytes 393224 | tf_op jit(solution)/shard_map/ppermute | solution.py:314
  119.1 1.2 collective-permute-start.20
  120.2 1.1 collective-permute-done.18
  121.3 3.8 %collective-permute-done.19 = bf16[256,256]{1,0:T(8,128)(2,1)S(1)} collective-permute-done((bf16[256,256]{1,0:T(8,128)(2,1)S(1)}, bf16[256,256]{1,0:T(8,128)(2,1)S(1)}, u32[]{:S(2)}, u32[]{:S(2)}) %collective-permute-start.19) | collective-permute-done | bytes 131104 | tf_op jit(solution)/shard_map/ppermute | solution.py:314
  125.2 1.7 collective-permute-start.21
  126.9 2.7 %collective-permute-done.21 = bf16[128,256]{1,0:T(8,128)(2,1)S(1)} collective-permute-done((bf16[128,256]{1,0:T(8,128)(2,1)S(1)}, bf16[128,256]{1,0:T(8,128)(2,1)S(1)}, u32[]{:S(2)}, u32[]{:S(2)}) %collective-permute-start.21) | collective-permute-done | bytes 65568 | tf_op jit(solution)/shard_map/ppermute | solution.py:320
  129.6 1.1 broadcast_in_dim.22
  130.7 4.9 %all-to-all-start.2 = ((bf16[16,128,256]{2,1,0:T(8,128)(2,1)}), bf16[16,128,256]{2,1,0:T(8,128)(2,1)S(1)}, u32[]{:S(2)}, u32[]{:S(2)}) async-start(bf16[16,128,256]{2,1,0:T(8,128)(2,1)} %broadcast_in_dim.22), calls=%async_computation.2 | async-start | bytes 2097152 | tf_op jit(solution)/shard_map/all_to_all | solution.py:324
  135.6 1.2 collective-permute-start.3
  136.8 2.2 %collective-permute-start.4 = (bf16[256,2048]{1,0:T(8,128)(2,1)}, bf16[256,2048]{1,0:T(8,128)(2,1)}, u32[]{:S(2)}, u32[]{:S(2)}) collective-permute-start(bf16[256,2048]{1,0:T(8,128)(2,1)} %refs_0_.2), channel_id=1, source_target_pairs={{0,4},{2,6},{4,0},{6,2},{1,5},{3,7},{5,1},{7,3},{8,12},{10,14},{12... | collective-permute-start | bytes 3145736 | tf_op jit(solution)/shard_map/ppermute | solution.py:238
  139.0 0.9 collective-permute-start.5
  139.9 10.6 %all-to-all-done.2 = bf16[16,128,256]{2,1,0:T(8,128)(2,1)S(1)} async-done(((bf16[16,128,256]{2,1,0:T(8,128)(2,1)}), bf16[16,128,256]{2,1,0:T(8,128)(2,1)S(1)}, u32[]{:S(2)}, u32[]{:S(2)}) %all-to-all-start.2) | async-done | bytes 1048608 | tf_op jit(solution)/shard_map/all_to_all | solution.py:324
  150.5 3.6 %all-to-all-start.1 = ((bf16[8,128,1024]{2,1,0:T(8,128)(2,1)}), bf16[8,128,1024]{2,1,0:T(8,128)(2,1)S(1)}, u32[]{:S(2)}, u32[]{:S(2)}) async-start(bf16[8,128,1024]{2,1,0:T(8,128)(2,1)} %bitcast.53), calls=%async_computation.1 | async-start | bytes 4194304 | tf_op jit(solution)/shard_map/all_to_all | solution.py:275
  154.1 3.7 %collective-permute-start.6 = (bf16[256,2048]{1,0:T(8,128)(2,1)}, bf16[256,2048]{1,0:T(8,128)(2,1)}, u32[]{:S(2)}, u32[]{:S(2)}) collective-permute-start(bf16[256,2048]{1,0:T(8,128)(2,1)} %refs_0_.2), channel_id=1, source_target_pairs={{0,1},{1,0},{2,3},{3,2},{4,5},{5,4},{6,7},{7,6},{8,9},{9,8},{10,11... | collective-permute-start | bytes 3145736 | tf_op jit(solution)/shard_map/ppermute | solution.py:241
  157.8 1.5 collective-permute-done.3.refs_1_
  159.3 5.8 %collective-permute-start.7 = (bf16[256,2048]{1,0:T(8,128)(2,1)}, bf16[256,2048]{1,0:T(8,128)(2,1)}, u32[]{:S(2)}, u32[]{:S(2)}) collective-permute-start(bf16[256,2048]{1,0:T(8,128)(2,1)} %collective-permute-done.3.refs_1_), channel_id=1, source_target_pairs={{0,1},{1,0},{2,3},{3,2},{4,5},{5,4},{6,7},{7,6},{8,9},{9,8},{10,11... | collective-permute-start | bytes 3145736 | tf_op jit(solution)/shard_map/ppermute | solution.py:241
  165.1 17.4 %collective-permute-done.4.refs_2_ = bf16[256,2048]{1,0:T(8,128)(2,1)} collective-permute-done((bf16[256,2048]{1,0:T(8,128)(2,1)}, bf16[256,2048]{1,0:T(8,128)(2,1)}, u32[]{:S(2)}, u32[]{:S(2)}) %collective-permute-start.4) | collective-permute-done | bytes 1048608 | tf_op jit(solution)/shard_map/ppermute | solution.py:238
  182.5 3.4 %collective-permute-start.8 = (bf16[256,2048]{1,0:T(8,128)(2,1)}, bf16[256,2048]{1,0:T(8,128)(2,1)}, u32[]{:S(2)}, u32[]{:S(2)}) collective-permute-start(bf16[256,2048]{1,0:T(8,128)(2,1)} %collective-permute-done.4.refs_2_), channel_id=1, source_target_pairs={{0,1},{1,0},{2,3},{3,2},{4,5},{5,4},{6,7},{7,6},{8,9},{9,8},{10,11... | collective-permute-start | bytes 3145736 | tf_op jit(solution)/shard_map/ppermute | solution.py:241
  186.0 1.8 shard_map.109
  187.8 0.7 collective-permute-done.8.refs_6_
  188.5 1.5 collective-permute-done.9.refs_7_
  190.0 7.5 %shard_map.107 = (bf16[128,2048]{1,0:T(8,128)(2,1)}, bf16[128,4096]{1,0:T(8,128)(2,1)}, bf16[128,2048]{1,0:T(8,128)(2,1)}) custom-call(s32[1]{0:T(128)} %bitcast.half_ref, s32[8]{0:T(128)S(1)} %stack.35.owner_ref, bf16[8,128,1024]{2,1,0:T(8,128)(2,1)S(1)} %all-to-all-done.1.home_ref, bf16[256,2048]{1,0:T(8,128)(2,1)} %refs_0_.2, ...), custom_call_target="tpu_custom_call" | custom-call | flops 1121976320 | bytes 4194304 | tf_op jit(solution)/shard_map/pallas_call | solution.py:276
  (27 shorter events, 0.4 us)
Async XLA Ops:
  7.0 56.8 %copy-start.2 = (f32[1,1,2048]{2,1,0:T(1,128)S(1)}, f32[1,1,2048]{2,1,0:T(1,128)}, u32[]{:S(2)}) copy-start(f32[1,1,2048]{2,1,0:T(1,128)} %param.12) | copy-start | bytes 24580
  7.0 67.1 %all-to-all-start = ((bf16[8,128,1536]{2,1,0:T(8,128)(2,1)}), bf16[8,128,1536]{2,1,0:T(8,128)(2,1)S(1)}, u32[]{:S(2)}, u32[]{:S(2)}) async-start(bf16[8,128,1536]{2,1,0:T(8,128)(2,1)} %shard_map.102), calls=%async_computation | async-start | bytes 6291456 | tf_op jit(solution)/shard_map/all_to_all | solution.py:228
  13.5 46.5 %collective-permute-start.10 = (bf16[1,128,2048]{2,1,0:T(8,128)(2,1)}, bf16[1,128,2048]{2,1,0:T(8,128)(2,1)}, u32[]{:S(2)}, u32[]{:S(2)}) collective-permute-start(bf16[1,128,2048]{2,1,0:T(8,128)(2,1)} %refs_0_.3), channel_id=1, source_target_pairs={{0,32},{8,40},{16,48},{24,56},{32,0},{40,8},{48,16},{56,24},{1,33}... | collective-permute-start | bytes 1572872 | tf_op jit(solution)/shard_map/ppermute | solution.py:219
  14.9 68.9 %collective-permute-start.11 = (bf16[1,128,2048]{2,1,0:T(8,128)(2,1)}, bf16[1,128,2048]{2,1,0:T(8,128)(2,1)}, u32[]{:S(2)}, u32[]{:S(2)}) collective-permute-start(bf16[1,128,2048]{2,1,0:T(8,128)(2,1)} %refs_0_.3), channel_id=1, source_target_pairs={{0,8},{8,16},{16,24},{24,0},{32,40},{40,48},{48,56},{56,32},{1,9},... | collective-permute-start | bytes 1572872 | tf_op jit(solution)/shard_map/ppermute | solution.py:231
  60.0 25.2 %collective-permute-start.14 = (bf16[1,128,2048]{2,1,0:T(8,128)(2,1)}, bf16[1,128,2048]{2,1,0:T(8,128)(2,1)}, u32[]{:S(2)}, u32[]{:S(2)}) collective-permute-start(bf16[1,128,2048]{2,1,0:T(8,128)(2,1)} %collective-permute-done.10.refs_1_), channel_id=1, source_target_pairs={{0,24},{8,0},{16,8},{24,16},{32,56},{40,32},{48,40},{56,48},{1,25}... | collective-permute-start | bytes 1572872 | tf_op jit(solution)/shard_map/ppermute | solution.py:231
  63.7 6.3 %collective-permute-start = (f32[8,128]{1,0:T(8,128)S(1)}, f32[8,128]{1,0:T(8,128)S(1)}, u32[]{:S(2)}, u32[]{:S(2)}) collective-permute-start(f32[8,128]{1,0:T(8,128)S(1)} %get-tuple-element.17), channel_id=1, source_target_pairs={{0,0},{8,96},{16,8},{24,104},{32,16},{40,112},{48,24},{56,120},{64... | collective-permute-start | bytes 12296 | tf_op jit(solution)/shard_map/ppermute | solution.py:217
  64.4 7.9 %collective-permute-start.1 = (f32[8,128]{1,0:T(8,128)S(1)}, f32[8,128]{1,0:T(8,128)S(1)}, u32[]{:S(2)}, u32[]{:S(2)}) collective-permute-start(f32[8,128]{1,0:T(8,128)S(1)} %get-tuple-element.18), channel_id=1, source_target_pairs={{0,96},{8,0},{16,104},{24,8},{32,112},{40,16},{48,120},{56,24},{64... | collective-permute-start | bytes 12296 | tf_op jit(solution)/shard_map/ppermute | solution.py:218
  74.0 1.0 copy-start
  77.2 15.8 %collective-permute-start.2 = (bf16[2,256,512]{2,1,0:T(8,128)(2,1)}, bf16[2,256,512]{2,1,0:T(8,128)(2,1)}, u32[]{:S(2)}, u32[]{:S(2)}) collective-permute-start(bf16[2,256,512]{2,1,0:T(8,128)(2,1)} %shard_map.104), channel_id=1, source_target_pairs={{0,96},{8,104},{16,112},{24,120},{32,64},{40,72},{48,80},{56,88},{... | collective-permute-start | bytes 1572872 | tf_op jit(solution)/shard_map/ppermute | solution.py:250
  79.1 18.7 %collective-permute-start.12 = (bf16[1,128,2048]{2,1,0:T(8,128)(2,1)}, bf16[1,128,2048]{2,1,0:T(8,128)(2,1)}, u32[]{:S(2)}, u32[]{:S(2)}) collective-permute-start(bf16[1,128,2048]{2,1,0:T(8,128)(2,1)} %refs_0_.3), channel_id=1, source_target_pairs={{0,24},{8,0},{16,8},{24,16},{32,56},{40,32},{48,40},{56,48},{1,25}... | collective-permute-start | bytes 1572872 | tf_op jit(solution)/shard_map/ppermute | solution.py:231
  81.5 16.2 %collective-permute-start.13 = (bf16[1,128,2048]{2,1,0:T(8,128)(2,1)}, bf16[1,128,2048]{2,1,0:T(8,128)(2,1)}, u32[]{:S(2)}, u32[]{:S(2)}) collective-permute-start(bf16[1,128,2048]{2,1,0:T(8,128)(2,1)} %collective-permute-done.10.refs_1_), channel_id=1, source_target_pairs={{0,8},{8,16},{16,24},{24,0},{32,40},{40,48},{48,56},{56,32},{1,9},... | collective-permute-start | bytes 1572872 | tf_op jit(solution)/shard_map/ppermute | solution.py:231
  83.8 21.2 %collective-permute-start.15 = (bf16[1,128,2048]{2,1,0:T(8,128)(2,1)}, bf16[1,128,2048]{2,1,0:T(8,128)(2,1)}, u32[]{:S(2)}, u32[]{:S(2)}) collective-permute-start(bf16[1,128,2048]{2,1,0:T(8,128)(2,1)} %collective-permute-done.11.refs_2_), channel_id=1, source_target_pairs={{0,8},{8,16},{16,24},{24,0},{32,40},{40,48},{48,56},{56,32},{1,9},... | collective-permute-start | bytes 1572872 | tf_op jit(solution)/shard_map/ppermute | solution.py:231
  85.2 20.4 %collective-permute-start.16 = (bf16[1,128,2048]{2,1,0:T(8,128)(2,1)}, bf16[1,128,2048]{2,1,0:T(8,128)(2,1)}, u32[]{:S(2)}, u32[]{:S(2)}) collective-permute-start(bf16[1,128,2048]{2,1,0:T(8,128)(2,1)} %collective-permute-done.14.refs_5_), channel_id=1, source_target_pairs={{0,24},{8,0},{16,8},{24,16},{32,56},{40,32},{48,40},{56,48},{1,25}... | collective-permute-start | bytes 1572872 | tf_op jit(solution)/shard_map/ppermute | solution.py:231
  86.5 1.0 copy-start.1
  110.4 4.6 %collective-permute-start.17 = (bf16[4,256,256]{2,1,0:T(8,128)(2,1)S(1)}, bf16[4,256,256]{2,1,0:T(8,128)(2,1)S(1)}, u32[]{:S(2)}, u32[]{:S(2)}) collective-permute-start(bf16[4,256,256]{2,1,0:T(8,128)(2,1)S(1)} %dynamic-slice_bitcast_fusion), channel_id=1, source_target_pairs={{0,1},{1,0},{2,3},{3,2},{4,5},{5,4},{6,7},{7,6},{8,9},{9,8},{10,11... | collective-permute-start | bytes 1572872 | tf_op jit(solution)/shard_map/ppermute | solution.py:309
  115.2 6.1 %collective-permute-start.18 = (bf16[256,256]{1,0:T(8,128)(2,1)S(1)}, bf16[256,256]{1,0:T(8,128)(2,1)S(1)}, u32[]{:S(2)}, u32[]{:S(2)}) collective-permute-start(bf16[256,256]{1,0:T(8,128)(2,1)S(1)} %get-tuple-element.14), channel_id=1, source_target_pairs={{0,2},{2,4},{4,6},{6,0},{1,3},{3,5},{5,7},{7,1},{8,10},{10,12},{12... | collective-permute-start | bytes 393224 | tf_op jit(solution)/shard_map/ppermute | solution.py:314
  116.6 8.5 %collective-permute-start.19 = (bf16[256,256]{1,0:T(8,128)(2,1)S(1)}, bf16[256,256]{1,0:T(8,128)(2,1)S(1)}, u32[]{:S(2)}, u32[]{:S(2)}) collective-permute-start(bf16[256,256]{1,0:T(8,128)(2,1)S(1)} %get-tuple-element.16), channel_id=1, source_target_pairs={{0,4},{2,6},{4,0},{6,2},{1,5},{3,7},{5,1},{7,3},{8,12},{10,14},{12... | collective-permute-start | bytes 393224 | tf_op jit(solution)/shard_map/ppermute | solution.py:314
  119.1 6.0 %collective-permute-start.20 = (bf16[256,256]{1,0:T(8,128)(2,1)S(1)}, bf16[256,256]{1,0:T(8,128)(2,1)S(1)}, u32[]{:S(2)}, u32[]{:S(2)}) collective-permute-start(bf16[256,256]{1,0:T(8,128)(2,1)S(1)} %get-tuple-element.15), channel_id=1, source_target_pairs={{0,6},{2,0},{4,2},{6,4},{1,7},{3,1},{5,3},{7,5},{8,14},{10,8},{12,... | collective-permute-start | bytes 393224 | tf_op jit(solution)/shard_map/ppermute | solution.py:314
  125.2 4.4 %collective-permute-start.21 = (bf16[128,256]{1,0:T(8,128)(2,1)S(1)}, bf16[128,256]{1,0:T(8,128)(2,1)S(1)}, u32[]{:S(2)}, u32[]{:S(2)}) collective-permute-start(bf16[128,256]{1,0:T(8,128)(2,1)S(1)} %dynamic-slice_bitcast_fusion.4), channel_id=1, source_target_pairs={{0,96},{8,104},{16,112},{24,120},{32,64},{40,72},{48,80},{56,88},{... | collective-permute-start | bytes 196616 | tf_op jit(solution)/shard_map/ppermute | solution.py:320
  130.7 19.8 %all-to-all-start.2 = ((bf16[16,128,256]{2,1,0:T(8,128)(2,1)}), bf16[16,128,256]{2,1,0:T(8,128)(2,1)S(1)}, u32[]{:S(2)}, u32[]{:S(2)}) async-start(bf16[16,128,256]{2,1,0:T(8,128)(2,1)} %broadcast_in_dim.22), calls=%async_computation.2 | async-start | bytes 2097152 | tf_op jit(solution)/shard_map/all_to_all | solution.py:324
  135.6 23.7 %collective-permute-start.3 = (bf16[256,2048]{1,0:T(8,128)(2,1)}, bf16[256,2048]{1,0:T(8,128)(2,1)}, u32[]{:S(2)}, u32[]{:S(2)}) collective-permute-start(bf16[256,2048]{1,0:T(8,128)(2,1)} %refs_0_.2), channel_id=1, source_target_pairs={{0,2},{2,4},{4,6},{6,0},{1,3},{3,5},{5,7},{7,1},{8,10},{10,12},{12... | collective-permute-start | bytes 3145736 | tf_op jit(solution)/shard_map/ppermute | solution.py:238
  136.8 45.7 %collective-permute-start.4 = (bf16[256,2048]{1,0:T(8,128)(2,1)}, bf16[256,2048]{1,0:T(8,128)(2,1)}, u32[]{:S(2)}, u32[]{:S(2)}) collective-permute-start(bf16[256,2048]{1,0:T(8,128)(2,1)} %refs_0_.2), channel_id=1, source_target_pairs={{0,4},{2,6},{4,0},{6,2},{1,5},{3,7},{5,1},{7,3},{8,12},{10,14},{12... | collective-permute-start | bytes 3145736 | tf_op jit(solution)/shard_map/ppermute | solution.py:238
  139.0 46.9 %collective-permute-start.5 = (bf16[256,2048]{1,0:T(8,128)(2,1)}, bf16[256,2048]{1,0:T(8,128)(2,1)}, u32[]{:S(2)}, u32[]{:S(2)}) collective-permute-start(bf16[256,2048]{1,0:T(8,128)(2,1)} %refs_0_.2), channel_id=1, source_target_pairs={{0,6},{2,0},{4,2},{6,4},{1,7},{3,1},{5,3},{7,5},{8,14},{10,8},{12,... | collective-permute-start | bytes 3145736 | tf_op jit(solution)/shard_map/ppermute | solution.py:238
  150.5 39.5 %all-to-all-start.1 = ((bf16[8,128,1024]{2,1,0:T(8,128)(2,1)}), bf16[8,128,1024]{2,1,0:T(8,128)(2,1)S(1)}, u32[]{:S(2)}, u32[]{:S(2)}) async-start(bf16[8,128,1024]{2,1,0:T(8,128)(2,1)} %bitcast.53), calls=%async_computation.1 | async-start | bytes 4194304 | tf_op jit(solution)/shard_map/all_to_all | solution.py:275
  154.1 33.7 %collective-permute-start.6 = (bf16[256,2048]{1,0:T(8,128)(2,1)}, bf16[256,2048]{1,0:T(8,128)(2,1)}, u32[]{:S(2)}, u32[]{:S(2)}) collective-permute-start(bf16[256,2048]{1,0:T(8,128)(2,1)} %refs_0_.2), channel_id=1, source_target_pairs={{0,1},{1,0},{2,3},{3,2},{4,5},{5,4},{6,7},{7,6},{8,9},{9,8},{10,11... | collective-permute-start | bytes 3145736 | tf_op jit(solution)/shard_map/ppermute | solution.py:241
  159.3 28.6 %collective-permute-start.7 = (bf16[256,2048]{1,0:T(8,128)(2,1)}, bf16[256,2048]{1,0:T(8,128)(2,1)}, u32[]{:S(2)}, u32[]{:S(2)}) collective-permute-start(bf16[256,2048]{1,0:T(8,128)(2,1)} %collective-permute-done.3.refs_1_), channel_id=1, source_target_pairs={{0,1},{1,0},{2,3},{3,2},{4,5},{5,4},{6,7},{7,6},{8,9},{9,8},{10,11... | collective-permute-start | bytes 3145736 | tf_op jit(solution)/shard_map/ppermute | solution.py:241
  182.5 6.0 %collective-permute-start.8 = (bf16[256,2048]{1,0:T(8,128)(2,1)}, bf16[256,2048]{1,0:T(8,128)(2,1)}, u32[]{:S(2)}, u32[]{:S(2)}) collective-permute-start(bf16[256,2048]{1,0:T(8,128)(2,1)} %collective-permute-done.4.refs_2_), channel_id=1, source_target_pairs={{0,1},{1,0},{2,3},{3,2},{4,5},{5,4},{6,7},{7,6},{8,9},{9,8},{10,11... | collective-permute-start | bytes 3145736 | tf_op jit(solution)/shard_map/ppermute | solution.py:241
  185.9 4.1 %collective-permute-start.9 = (bf16[256,2048]{1,0:T(8,128)(2,1)}, bf16[256,2048]{1,0:T(8,128)(2,1)}, u32[]{:S(2)}, u32[]{:S(2)}) collective-permute-start(bf16[256,2048]{1,0:T(8,128)(2,1)} %collective-permute-done.5.refs_3_), channel_id=1, source_target_pairs={{0,1},{1,0},{2,3},{3,2},{4,5},{5,4},{6,7},{7,6},{8,9},{9,8},{10,11... | collective-permute-start | bytes 3145736 | tf_op jit(solution)/shard_map/ppermute | solution.py:241

commit v4 on v3

--- a/solution.py
+++ b/solution.py
@@ -25,7 +25,7 @@
 TN = ((0,), (0,))
 
 
-def decay_kernel(lam_ref, half_ref, rows_ref, tall_ref):
+def decay_kernel(lam_ref, half_ref, rows_ref, factors_ref):
     n = BLOCK
     row = lax.broadcasted_iota(jnp.int32, (n, n), 0)
     col = lax.broadcasted_iota(jnp.int32, (n, n), 1)
@@ -54,34 +54,43 @@
         key_sum.append(jnp.where(first, rem0[b] + later0, pre1[b] + early1))
         query_sum.append(jnp.where(first, suf1[b] + later1, loc0[b] + early0))
     rows_ref[...] = jnp.concatenate(loc0 + suf1 + rem0 + pre1 + tile0 + tile1, axis=0)
-    keys = jnp.exp(jnp.concatenate(key_sum, axis=0))
-    queries = jnp.exp(jnp.concatenate(query_sum, axis=0)) * 0.0625
-    stack = [jnp.concatenate(loc0 + suf1, axis=0), keys, queries, jnp.zeros((n - 32, n), F32)]
-    cols = jnp.transpose(jnp.concatenate(stack, axis=0))
-    for b in range(8):
-        picks = [cols[:, v * 8 + b : v * 8 + b + 1] for v in range(4)]
-        tall_ref[b * n : b * n + n, :] = jnp.concatenate(picks, axis=1)
+    tiles = []
+    for t in range(4):
+        pair = slice(2 * t, 2 * t + 2)
+        tiles += [jnp.exp(k) for k in key_sum[pair]]
+        tiles += [jnp.exp(q) * 0.0625 for q in query_sum[pair]]
+        tiles += loc0[pair] + suf1[pair]
+    factors_ref[...] = jnp.concatenate(tiles, axis=0)
+
+
+def upright(factors):
+    turned = jnp.transpose(factors)
+    pairs = [(turned[:, 2 * k : 2 * k + 1], turned[:, 2 * k + 1 : 2 * k + 2]) for k in range(4)]
+    return [jnp.concatenate(pair, axis=0) for pair in pairs]
 
 
 def wide(rows, base, t):
     return jnp.concatenate([rows[base + 2 * t : base + 2 * t + 1], rows[base + 2 * t + 1 : base + 2 * t + 2]], axis=1)
 
 
-def boundary_kernel(units_ref, tall_ref, state_ref):
-    keys = (units_ref[:, 256:512].astype(F32) * tall_ref[:, 2:3]).astype(BF16)
-    queries = (units_ref[:, 0:256].astype(F32) * tall_ref[:, 3:4]).astype(BF16)
+def boundary_kernel(units_ref, factors_ref, state_ref):
+    sides = [upright(factors_ref[8 * t : 8 * t + 8, :]) for t in range(4)]
+    to_end = jnp.concatenate([side[0] for side in sides], axis=0)
+    from_end = jnp.concatenate([side[1] for side in sides], axis=0)
+    keys = (units_ref[:, 256:512].astype(F32) * to_end).astype(BF16)
+    queries = (units_ref[:, 0:256].astype(F32) * from_end).astype(BF16)
     state_ref[0] = dot(keys, units_ref[:, 512:1024], TN).astype(BF16)
     state_ref[1] = dot(queries, units_ref[:, 1024:1536], TN).astype(BF16)
 
 
-def inside_kernel(units_ref, rows_ref, tall_ref, out_ref, s_ref, gs_ref):
+def inside_kernel(units_ref, rows_ref, factors_ref, out_ref, s_ref, gs_ref):
     rows = rows_ref[...]
     row = lax.broadcasted_iota(jnp.int32, (TILE, TILE), 0)
     col = lax.broadcasted_iota(jnp.int32, (TILE, TILE), 1)
     for i in range(4):
         at = pl.ds(i * TILE, TILE)
         query, grad = units_ref[at, 0:256], units_ref[at, 1024:1536]
-        loc0, suf1 = tall_ref[at, 0:1], tall_ref[at, 1:2]
+        loc0, suf1 = upright(factors_ref[8 * i : 8 * i + 8, :])[2:]
         for j in range(4):
             to = pl.ds(j * TILE, TILE)
             if i == j:
@@ -106,12 +115,13 @@
     out_ref[:, 512:1024] = dot(s_ref[...], units_ref[:, 1024:1536], TN).astype(BF16)
 
 
-def across_kernel(units_ref, tall_ref, state_ref, part_ref, out_ref):
+def across_kernel(units_ref, factors_ref, state_ref, part_ref, out_ref):
     memory, later = state_ref[0], state_ref[1]
-    keys = (units_ref[:, 256:512].astype(F32) * tall_ref[:, 2:3]).astype(BF16)
-    part = dot(units_ref[:, 512:1024], later, NT) * tall_ref[:, 2:3]
+    to_end, from_end = upright(factors_ref[...])[:2]
+    keys = (units_ref[:, 256:512].astype(F32) * to_end).astype(BF16)
+    part = dot(units_ref[:, 512:1024], later, NT) * to_end
     out_ref[:, 0:256] = (part_ref[:, 0:256].astype(F32) + part).astype(BF16)
-    part = dot(units_ref[:, 1024:1536], memory, NT) * tall_ref[:, 3:4]
+    part = dot(units_ref[:, 1024:1536], memory, NT) * from_end
     out_ref[:, 256:512] = (part_ref[:, 256:512].astype(F32) + part).astype(BF16)
     part = dot(keys, later, NN)
     out_ref[:, 512:1024] = (part_ref[:, 512:1024].astype(F32) + part).astype(BF16)
@@ -136,27 +146,59 @@
     return jax.ShapeDtypeStruct(dims, dtype)
 
 
-def pack_kernel(half_ref, query_ref, key_ref, value_ref, grad_ref, out_ref):
-    del half_ref
-    out_ref[0, :, 0:256] = query_ref[...]
-    out_ref[0, :, 256:512] = key_ref[...]
-    out_ref[0, :, 512:1024] = value_ref[...]
-    out_ref[0, :, 1024:1536] = grad_ref[...]
+PARTS = 4
+
+
+def pack_kernel(half_ref, *refs):
+    sources, (out_ref,), stages, packed_ref, in_sems, out_sems = (
+        refs[:4],
+        refs[4:5],
+        refs[5:9],
+        refs[9],
+        refs[10],
+        refs[11],
+    )
+    span = BLOCK // PARTS
+    loads, stores = [], []
+    for p in range(PARTS):
+        rows = pl.ds(p * span, span)
+        for k, (source, stage) in enumerate(zip(sources, stages, strict=True)):
+            loads.append(
+                pltpu.make_async_copy(source.at[rows, :], stage.at[rows, :], in_sems.at[p * 4 + k])
+            )
+        stores.append(
+            pltpu.make_async_copy(packed_ref.at[p], out_ref.at[:, rows, :], out_sems.at[p])
+        )
+    for load in loads:
+        load.start()
+    for p in range(PARTS):
+        rows = pl.ds(p * span, span)
+        for load in loads[4 * p : 4 * p + 4]:
+            load.wait()
+        for h in range(HEADS):
+            lane, at = (h + 4 * half_ref[0]) & 7, 0
+            for stage in stages:
+                width = stage.shape[1] // HEADS
+                packed_ref[p, lane, :, at : at + width] = stage[rows, h * width : h * width + width]
+                at += width
+        stores[p].start()
+    for store in stores:
+        store.wait()
 
 
 def pack(half, arrays):
-    def columns(width):
-        return pl.BlockSpec((BLOCK, width), lambda h, half: (0, (h + 4 * half[0]) & 7))
-
+    outside = pl.BlockSpec(memory_space=pltpu.HBM)
     return pl.pallas_call(
         pack_kernel,
         out_shape=pltpu.HBM((HEADS, BLOCK, 1536), BF16),
-        grid_spec=pltpu.PrefetchScalarGridSpec(
-            num_scalar_prefetch=1,
-            grid=(HEADS,),
-            in_specs=[columns(a.shape[1] // HEADS) for a in arrays],
-            out_specs=pl.BlockSpec((1, BLOCK, 1536), lambda h, half: (h, 0, 0)),
-        ),
+        in_specs=[pl.BlockSpec(memory_space=pltpu.SMEM)] + [outside] * 4,
+        out_specs=outside,
+        scratch_shapes=[
+            *[pltpu.VMEM(a.shape, BF16) for a in arrays],
+            pltpu.VMEM((PARTS, HEADS, BLOCK // PARTS, 1536), BF16),
+            pltpu.SemaphoreType.DMA((4 * PARTS,)),
+            pltpu.SemaphoreType.DMA((PARTS,)),
+        ],
         cost_estimate=pl.CostEstimate(flops=1 << 20, bytes_accessed=6 << 20, transcendentals=0),
         compiler_params=pltpu.CompilerParams(vmem_limit_bytes=16 << 20),
     )(half.reshape(1), *[in_hbm(a) for a in arrays])
@@ -169,16 +211,45 @@
 STEPS = ((0, 0), (1, 0), (0, 3), (0, 1), (1, 3), (1, 1), (0, 2), (1, 2))
 
 
-def term_kernel(lane_ref, grads_ref, *refs):
-    lane = lane_ref[0]
+def term_kernel(place_ref, grads_ref, *refs):
+    pieces, (mine_ref, *theirs), total_ref = refs[:8], refs[8:-1], refs[-1]
+    lane = place_ref[0]
     deep, y = lane // 4, lane % 4
     total = None
-    for piece, (other, step) in zip(refs[:-1], STEPS, strict=True):
+    for piece, (other, step) in zip(pieces, STEPS, strict=True):
         block = (deep ^ other) * 4 + (y + step) % 4
         grad = grads_ref[pl.ds(pl.multiple_of(block * BLOCK, BLOCK), BLOCK), :]
         part = dot(piece[0], grad, TN)
         total = part if total is None else total + part
+    slices = mine_ref.shape[0] * (1 + len(theirs))
+    total_ref[...] = total.reshape(slices, -1, total.shape[1])
+    for k in range(mine_ref.shape[0]):
+        if theirs:
+            mine_ref[k] = total_ref[2 * k + place_ref[1]]
+            theirs[0][k] = total_ref[2 * k + 1 - place_ref[1]].astype(BF16)
+        else:
+            mine_ref[k] = total_ref[k]
+
+
+def core_sum_kernel(turn_ref, mine_ref, theirs_ref, own_ref, *send_refs):
+    ring = mine_ref.shape[0]
+    for step, ref in enumerate((own_ref, *send_refs)):
+        at = (turn_ref[0] + step) & (ring - 1)
+        ref[...] = (mine_ref[at] + theirs_ref[at].astype(F32)).astype(ref.dtype)
+
+
+def ring_sum_kernel(*refs):
+    total = refs[0][...]
+    for ref in refs[1:-2]:
+        total = total + ref[...].astype(F32)
+    refs[-2][...] = total
     refs[-1][...] = total.astype(BF16)
+
+
+def half_sum_kernel(mine_ref, theirs_ref, out_ref):
+    total = (mine_ref[...] + theirs_ref[...].astype(F32)).astype(BF16)
+    for k in range(out_ref.shape[0]):
+        out_ref[k] = total
 
 
 def home_kernel(half_ref, owner_ref, home_ref, *refs):
@@ -194,11 +265,10 @@
         input_ref[:, pl.ds(at, span)] = dot(key_ref[...], weight[...], NT).astype(BF16)
 
 
-def widen_kernel(first_ref, second_ref, out_ref):
-    span = first_ref.shape[2]
-    for s, ref in enumerate((first_ref, second_ref)):
-        for h in range(2):
-            out_ref[s * span : s * span + span, h * 256 : h * 256 + 256] = ref[0, h].astype(F32)
+def widen_kernel(half_ref, in_ref, out_ref):
+    for k in range(HEADS):
+        at = pl.multiple_of(((k + 4 * half_ref[0]) & 7) * 256, 256)
+        out_ref[:, pl.ds(at, 256)] = in_ref[k].astype(F32)
 
 
 def shards(layer_input, queries, key_vectors, values, cotangent, log_decay, key_weight):
@@ -218,7 +288,7 @@
     far = lax.ppermute(far, SP, [(u, worker(1 - u % 2, u // 2)) for u in range(peers)])
     deep = lax.ppermute(layer_input, "lane", [(i, (i + 4) % 8) for i in range(8)])
     lam = jnp.where(half == 0, jnp.concatenate([near, far]), jnp.concatenate([far, near]))
-    rows, tall = kernel(decay_kernel, (shape((40, 128), F32), pltpu.HBM((1024, 4), F32)), 1 << 20)(
+    rows, factors = kernel(decay_kernel, (shape((40, 128), F32), shape((32, 128), F32)), 1 << 20)(
         lam, jnp.full((1, 128), half, jnp.int32)
     )
 
@@ -242,18 +312,19 @@
         owners += [o + 1 - 2 * core for o in owners]
 
     own = layer_input
+    own_last = lane_step(own, 2)
     own_before, own_after = lane_step(own, 1), lane_step(own, 3)
     deep_before, deep_after = lane_step(deep, 1), lane_step(deep, 3)
-    own_last, deep_last = lane_step(own_before, 1), lane_step(deep_after, 3)
-
-    state = kernel(boundary_kernel, pltpu.HBM((2, 256, 512), BF16), 540 << 20)(units, tall)
+    deep_last = lax.ppermute(own_last, "lane", [(i, (i + 4) % 8) for i in range(8)])
+
+    state = kernel(boundary_kernel, pltpu.HBM((2, 256, 512), BF16), 540 << 20)(units, factors)
     state = lax.ppermute(state, SP, [(u, u ^ 12) for u in range(peers)])
     part = kernel(
         inside_kernel,
         pltpu.HBM((1024, 1024), BF16),
         3760 << 20,
         (pltpu.VMEM((1024, 1024), BF16), pltpu.VMEM((1024, 1024), BF16)),
-    )(units, rows, tall)
+    )(units, rows, factors)
 
     def by_tile(width):
         return pl.BlockSpec((TILE, width), lambda i: (i, 0))
@@ -265,12 +336,12 @@
         grid=(4,),
         in_specs=[
             by_tile(1536),
-            by_tile(4),
+            pl.BlockSpec((8, 128), lambda i: (i, 0)),
             pl.BlockSpec((2, 256, 512), lambda i: (0, 0, 0)),
             by_tile(1024),
         ],
         out_specs=by_tile(1024),
-    )(units, tall, state, in_hbm(part))
+    )(units, factors, state, in_hbm(part))
 
     home = lax.all_to_all(grads.reshape(8, tokens, -1), "lane", 0, 0, tiled=True)
     grad_query, grad_value, grad_input = kernel(
@@ -282,15 +353,19 @@
         out_specs=(whole, whole, whole),
     )(half.reshape(1), jnp.stack(owners), home, *weights)
 
-    terms = kernel(
+    parts = [shape((ring, 2048 // ring // cores, 256), F32)]
+    if cores == 2:
+        parts.append(pltpu.HBM((ring, 2048 // ring // cores, 256), BF16))
+    terms, *theirs = kernel(
         term_kernel,
-        shape((2048, 256), BF16),
+        parts,
         1070 << 20,
+        (pltpu.VMEM((ring * cores, 2048 // ring // cores, 256), F32),),
         grid=(1,),
         in_specs=[scalars, pl.BlockSpec((1024, 256), lambda i: (0, 0))] + [whole] * 8,
-        out_specs=whole,
+        out_specs=[whole] * len(parts),
     )(
-        lane.reshape(1),
+        jnp.stack([lane, core]),
         in_hbm(grads),
         own,
         deep,
@@ -302,37 +377,33 @@
         deep_last,
     )
 
+    piece = terms.shape[1:]
+    sends = []
     if cores == 2:
-        terms = terms.reshape(ring, 2, -1, 256)
-        mine = lax.dynamic_index_in_dim(terms, core, 1, keepdims=False)
-        theirs = lax.dynamic_index_in_dim(terms, 1 - core, 1, keepdims=False)
-        theirs = lax.ppermute(theirs, "dp_1", [(0, 1), (1, 0)])
-        terms = (mine.astype(F32) + theirs.astype(F32)).astype(BF16)
-        total = lax.dynamic_index_in_dim(terms, turn, 0, keepdims=False).astype(F32)
+        theirs = lax.ppermute(theirs[0], "dp_1", [(0, 1), (1, 0)])
+        terms, *sends = kernel(
+            core_sum_kernel,
+            [shape(piece, F32)] + [shape(piece, BF16)] * (ring - 1),
+            1 << 20,
+            in_specs=[scalars] + [whole] * 2,
+            out_specs=[whole] * ring,
+        )(turn.reshape(1), terms, theirs)
         for step in range(1, ring):
-            piece = lax.dynamic_index_in_dim(terms, (turn + step) % ring, 0, keepdims=False)
-            piece = lax.ppermute(piece, "dp_0", [(i, (i + step) % ring) for i in range(ring)])
-            total = total + piece.astype(F32)
-        terms = total.astype(BF16)
-    terms = terms.reshape(2, -1, 256)
-    mine = lax.dynamic_index_in_dim(terms, half, 0, keepdims=False)
-    theirs = lax.dynamic_index_in_dim(terms, 1 - half, 0, keepdims=False)
+            moves = [(i, (i + step) % ring) for i in range(ring)]
+            sends[step - 1] = lax.ppermute(sends[step - 1], "dp_0", moves)
+    mine, theirs = kernel(ring_sum_kernel, (shape(piece, F32), shape(piece, BF16)), 1 << 20)(
+        terms.reshape(piece), *sends
+    )
     theirs = lax.ppermute(theirs, SP, [(u, u ^ 12) for u in range(peers)])
-    total = (mine.astype(F32) + theirs.astype(F32)).astype(BF16)
-    span = total.shape[0]
-    spread = jnp.broadcast_to(total[None], (peers, span, 256))
-    spread = lax.all_to_all(spread, SP, 0, 0, tiled=True)
+    spread = kernel(half_sum_kernel, pltpu.HBM((8, *piece), BF16), 1 << 20)(mine, theirs)
+    spread = lax.all_to_all(spread, "lane", 0, 0, tiled=True)
     grad_weight = kernel(
         widen_kernel,
-        shape((2 * span, 2048), F32),
+        pltpu.HBM((piece[0], 2048), F32),
         1 << 20,
-        grid=(4,),
-        in_specs=[
-            pl.BlockSpec((1, 2, span, 256), lambda h: (0, h, 0, 0)),
-            pl.BlockSpec((1, 2, span, 256), lambda h: (1, (h + 2) & 3, 0, 0)),
-        ],
-        out_specs=pl.BlockSpec((2 * span, 512), lambda h: (0, h)),
-    )(*[spread.reshape(2, 8, span, 256)] * 2)
+        in_specs=[scalars, whole],
+        out_specs=whole,
+    )(half.reshape(1), spread)
     return grad_query[None], grad_value[None], grad_input[None], grad_weight
 
 

time: 198 us -> 181 us (0.914)
  waiting for transfers between devices: 95 us -> 87.7 us
  starting transfers between devices: 63.8 us -> 60 us
  local copies, waits for them, and re-layouts: 3.34 us -> 0.1 us
  Pallas kernels: 34.5 us -> 31.5 us
    ppermute x1, waiting for transfers between devices: 43.9 us -> 0.01 us  [shards(): lax.ppermute(layer_input, 'lane', [(i, (i + 4) % 8) for i in range(8)])]
    ppermute x1, waiting for transfers between devices: 2.29 us -> 33.4 us  [shards(): lax.ppermute(far, SP, [(u, worker(1 - u % 2, u // 2)) for u in range(peer...]
    ppermute x4, starting transfers between devices: 12.9 us -> 8.11 us  [shards(): weights += [lax.ppermute(w, 'dp_1', [(0, 1), (1, 0)]) for w in weights]]
    ppermute x3, waiting for transfers between devices: 18.9 us -> 23.1 us  [shards(): weights.append(lax.ppermute(key_weight, 'dp_0', moves))]
    ppermute x1, starting transfers between devices: 5.58 us -> 9.4 us  [shards(): lax.ppermute(far, SP, [(u, worker(1 - u % 2, u // 2)) for u in range(peer...]
    pallas_call x1, Pallas kernels: 6.32 us -> 3.04 us  [pack(): pl.pallas_call(pack_kernel, out_shape=pltpu.HBM((HEADS, BLOCK, 1536), BF1...]
    ppermute x6 -> x5, starting transfers between devices: 12.3 us -> 9.17 us  [lane_step(): lax.ppermute(array, 'lane', [(i, i // 4 * 4 + (i + step) % 4) for i in ra...]
    unnamed x6 -> x2, local copies, waits for them, and re-layouts: 2.09 us -> 0.01 us
  transfers between devices with their start and end apart: 25 -> 25, of which waited for: 13 -> 14; matrix products, arithmetic and copies ran while one was open for 0% -> 0% of each run, Pallas kernels for 8% -> 8%
where the time goes in v4:
time: 181 us; the launch traced here: 180 us
  waiting for transfers between devices  87.7 us (48%)
  starting transfers between devices  60 us (33%)
  Pallas kernels  31.5 us (17%)
    ppermute x1, waiting for transfers between devices, shards(): lax.ppermute(far, SP, [(u, worker(1 - u % 2, u // 2)) for u in range(peer...  33.4 us
    ppermute x3, waiting for transfers between devices, shards(): weights.append(lax.ppermute(key_weight, 'dp_0', moves))  23.1 us
    all_to_all x1, waiting for transfers between devices, shards(): spread = lax.all_to_all(spread, 'lane', 0, 0, tiled=True)  11.6 us
    ppermute x1, starting transfers between devices, shards(): lax.ppermute(far, SP, [(u, worker(1 - u % 2, u // 2)) for u in range(peer...  9.4 us
    ppermute x5, starting transfers between devices, lane_step(): lax.ppermute(array, 'lane', [(i, i // 4 * 4 + (i + step) % 4) for i in ra...  9.17 us
    ppermute x4, starting transfers between devices, shards(): weights += [lax.ppermute(w, 'dp_1', [(0, 1), (1, 0)]) for w in weights]  8.11 us
    pallas_call x1, Pallas kernels, shards(): kernel(home_kernel, (shape((tokens, 2048), BF16), shape((tokens, 4096), B...  7.53 us
    ppermute x5, waiting for transfers between devices, lane_step(): lax.ppermute(array, 'lane', [(i, i // 4 * 4 + (i + step) % 4) for i in ra...  7.08 us
  transfers between devices with their start and end apart: 25, of which 14 were waited for; matrix products, arithmetic and copies ran while one was open for 0% of the time, Pallas kernels for 8%

profile of v4, /device:TPU:1, one launch (start us, length us, event | category | flops | bytes accessed | tf_op | source)
XLA Modules:
  0.0 180.2 jit_solution(16519856866654028704)
XLA Ops:
  0.6 3.0 %shard_map.102 = bf16[8,128,1536]{2,1,0:T(8,128)(2,1)} custom-call(s32[1]{0:T(128)} %bitcast.half_ref, bf16[128,2048]{1,0:T(8,128)(2,1)} %bitcast.32, bf16[128,2048]{1,0:T(8,128)(2,1)} %bitcast.33, bf16[128,4096]{1,0:T(8,128)(2,1)} %bitcast.30, bf16[128,4096]{1,0:T(8,128)(2,1)} %bitcast.31), custom_call_target="tpu_custom_call" | custom-call | flops 1048576 | bytes 6291456 | tf_op jit(solution)/shard_map/pallas_call | solution.py:191
  3.7 6.4 %all-to-all-start = ((bf16[8,128,1536]{2,1,0:T(8,128)(2,1)}), bf16[8,128,1536]{2,1,0:T(8,128)(2,1)S(1)}, u32[]{:S(2)}, u32[]{:S(2)}) async-start(bf16[8,128,1536]{2,1,0:T(8,128)(2,1)} %shard_map.102), calls=%async_computation | async-start | bytes 6291456 | tf_op jit(solution)/shard_map/all_to_all | solution.py:298
  10.1 0.7 collective-permute-start
  10.8 9.4 %collective-permute-start.1 = (f32[8,128]{1,0:T(8,128)S(1)}, f32[8,128]{1,0:T(8,128)S(1)}, u32[]{:S(2)}, u32[]{:S(2)}) collective-permute-start(f32[8,128]{1,0:T(8,128)S(1)} %get-tuple-element.31), channel_id=1, source_target_pairs={{0,96},{8,0},{16,104},{24,8},{32,112},{40,16},{48,120},{56,24},{64... | collective-permute-start | bytes 12296 | tf_op jit(solution)/shard_map/ppermute | solution.py:288
  20.2 1.3 collective-permute-start.10
  21.4 0.3 collective-permute-start.15
  21.7 33.4 %collective-permute-done.1 = f32[8,128]{1,0:T(8,128)S(1)} collective-permute-done((f32[8,128]{1,0:T(8,128)S(1)}, f32[8,128]{1,0:T(8,128)S(1)}, u32[]{:S(2)}, u32[]{:S(2)}) %collective-permute-start.1) | collective-permute-done | bytes 4128 | tf_op jit(solution)/shard_map/ppermute | solution.py:288
  55.1 0.4 shard_map.103
  55.5 2.4 %shard_map.104 = bf16[2,256,512]{2,1,0:T(8,128)(2,1)} custom-call(bf16[1024,1536]{1,0:T(8,128)(2,1)S(1)} %bitcast.26, f32[32,128]{1,0:T(8,128)S(1)} %get-tuple-element.17.factors_ref), custom_call_target="tpu_custom_call" | custom-call | flops 566231040 | bytes 4194304 | tf_op jit(solution)/shard_map/pallas_call | solution.py:320
  57.9 1.9 %collective-permute-start.2 = (bf16[2,256,512]{2,1,0:T(8,128)(2,1)}, bf16[2,256,512]{2,1,0:T(8,128)(2,1)}, u32[]{:S(2)}, u32[]{:S(2)}) collective-permute-start(bf16[2,256,512]{2,1,0:T(8,128)(2,1)} %shard_map.104), channel_id=1, source_target_pairs={{0,96},{8,104},{16,112},{24,120},{32,64},{40,72},{48,80},{56,88},{... | collective-permute-start | bytes 1572872 | tf_op jit(solution)/shard_map/ppermute | solution.py:321
  59.8 0.1 collective-permute-start.11
  59.9 3.0 %collective-permute-start.12 = (bf16[1,128,2048]{2,1,0:T(8,128)(2,1)}, bf16[1,128,2048]{2,1,0:T(8,128)(2,1)}, u32[]{:S(2)}, u32[]{:S(2)}) collective-permute-start(bf16[1,128,2048]{2,1,0:T(8,128)(2,1)} %refs_0_.3), channel_id=1, source_target_pairs={{0,24},{8,0},{16,8},{24,16},{32,56},{40,32},{48,40},{56,48},{1,25}... | collective-permute-start | bytes 1572872 | tf_op jit(solution)/shard_map/ppermute | solution.py:301
  62.9 0.1 collective-permute-done.15.refs_6_
  63.0 5.7 %collective-permute-start.14 = (bf16[1,128,2048]{2,1,0:T(8,128)(2,1)}, bf16[1,128,2048]{2,1,0:T(8,128)(2,1)S(1)}, u32[]{:S(2)}, u32[]{:S(2)}) collective-permute-start(bf16[1,128,2048]{2,1,0:T(8,128)(2,1)} %collective-permute-done.10.refs_1_), channel_id=1, source_target_pairs={{0,24},{8,0},{16,8},{24,16},{32,56},{40,32},{48,40},{56,48},{1,25}... | collective-permute-start | bytes 1572872 | tf_op jit(solution)/shard_map/ppermute | solution.py:301
  68.7 1.0 collective-permute-done.2.state_ref
  69.8 1.5 collective-permute-start.16
  71.3 5.6 %shard_map.105.part_ref = bf16[1024,1024]{1,0:T(8,128)(2,1)} custom-call(bf16[1024,1536]{1,0:T(8,128)(2,1)S(1)} %bitcast.27, f32[40,128]{1,0:T(8,128)S(1)} %get-tuple-element.18.rows_ref, f32[32,128]{1,0:T(8,128)S(1)} %get-tuple-element.17.factors_ref), custom_call_target="tpu_custom_call" | custom-call | flops 3942645760 | bytes 4194304 | tf_op jit(solution)/shard_map/pallas_call | solution.py:322
  76.9 4.8 %shard_map.106.grads_ref = bf16[1024,1024]{1,0:T(8,128)(2,1)} custom-call(bf16[1024,1536]{1,0:T(8,128)(2,1)S(1)} %bitcast.28, f32[32,128]{1,0:T(8,128)S(1)} %get-tuple-element.17.factors_ref, bf16[2,256,512]{2,1,0:T(8,128)(2,1)} %collective-permute-done.2.state_ref, bf16[1024,1024]{1,0:T(8,128)(2,1)} %shard_map.105.part_ref), custom_call_target="tpu_custom_call" | custom-call | flops 838860800 | bytes 4194304 | tf_op jit(solution)/shard_map/pallas_call | solution.py:332
  81.7 1.3 collective-permute-done.13.refs_4_
  83.1 5.6 %collective-permute-done.14.refs_5_ = bf16[1,128,2048]{2,1,0:T(8,128)(2,1)S(1)} collective-permute-done((bf16[1,128,2048]{2,1,0:T(8,128)(2,1)}, bf16[1,128,2048]{2,1,0:T(8,128)(2,1)S(1)}, u32[]{:S(2)}, u32[]{:S(2)}) %collective-permute-start.14) | collective-permute-done | bytes 524320 | tf_op jit(solution)/shard_map/ppermute | solution.py:301
  88.7 5.1 %shard_map.108 = (f32[4,256,256]{2,1,0:T(8,128)S(1)}, bf16[4,256,256]{2,1,0:T(8,128)(2,1)}) custom-call(s32[2]{0:T(128)S(1)} %pad_add_fusion.place_ref, bf16[1024,1024]{1,0:T(8,128)(2,1)} %shard_map.106.grads_ref, bf16[1,128,2048]{2,1,0:T(8,128)(2,1)} %refs_0_.3, bf16[1,128,2048]{2,1,0:T(8,128)(2,1)} %collective-permute-done.10.refs_1_, ...), custom_call_target="tpu_custom_call" | custom-call | flops 1121976320 | bytes 4194304 | tf_op jit(solution)/shard_map/pallas_call | solution.py:359
  93.8 1.8 %collective-permute-start.17 = (bf16[4,256,256]{2,1,0:T(8,128)(2,1)}, bf16[4,256,256]{2,1,0:T(8,128)(2,1)S(1)}, u32[]{:S(2)}, u32[]{:S(2)}) collective-permute-start(bf16[4,256,256]{2,1,0:T(8,128)(2,1)} %get-tuple-element.23), channel_id=1, source_target_pairs={{0,1},{1,0},{2,3},{3,2},{4,5},{5,4},{6,7},{7,6},{8,9},{9,8},{10,11... | collective-permute-start | bytes 1572872 | tf_op jit(solution)/shard_map/ppermute | solution.py:383
  95.7 1.7 collective-permute-done.17.theirs_ref
  97.4 0.1 shard_map.109
  97.5 1.5 collective-permute-start.18
  99.0 2.4 %collective-permute-start.19 = (bf16[256,256]{1,0:T(8,128)(2,1)S(1)}, bf16[256,256]{1,0:T(8,128)(2,1)S(1)}, u32[]{:S(2)}, u32[]{:S(2)}) collective-permute-start(bf16[256,256]{1,0:T(8,128)(2,1)S(1)} %get-tuple-element.26), channel_id=1, source_target_pairs={{0,4},{2,6},{4,0},{6,2},{1,5},{3,7},{5,1},{7,3},{8,12},{10,14},{12... | collective-permute-start | bytes 393224 | tf_op jit(solution)/shard_map/ppermute | solution.py:393
  101.4 1.2 collective-permute-start.20
  102.6 1.1 collective-permute-done.18.refs_1_
  103.6 3.8 %collective-permute-done.19.refs_2_ = bf16[256,256]{1,0:T(8,128)(2,1)S(1)} collective-permute-done((bf16[256,256]{1,0:T(8,128)(2,1)S(1)}, bf16[256,256]{1,0:T(8,128)(2,1)S(1)}, u32[]{:S(2)}, u32[]{:S(2)}) %collective-permute-start.19) | collective-permute-done | bytes 131104 | tf_op jit(solution)/shard_map/ppermute | solution.py:393
  107.5 3.3 %collective-permute-start.21 = (bf16[256,256]{1,0:T(8,128)(2,1)S(1)}, bf16[256,256]{1,0:T(8,128)(2,1)S(1)}, u32[]{:S(2)}, u32[]{:S(2)}) collective-permute-start(bf16[256,256]{1,0:T(8,128)(2,1)S(1)} %get-tuple-element.29), channel_id=1, source_target_pairs={{0,96},{8,104},{16,112},{24,120},{32,64},{40,72},{48,80},{56,88},{... | collective-permute-start | bytes 393224 | tf_op jit(solution)/shard_map/ppermute | solution.py:397
  110.8 2.4 %collective-permute-done.21.theirs_ref = bf16[256,256]{1,0:T(8,128)(2,1)S(1)} collective-permute-done((bf16[256,256]{1,0:T(8,128)(2,1)S(1)}, bf16[256,256]{1,0:T(8,128)(2,1)S(1)}, u32[]{:S(2)}, u32[]{:S(2)}) %collective-permute-start.21) | collective-permute-done | bytes 131104 | tf_op jit(solution)/shard_map/ppermute | solution.py:397
  113.2 1.0 shard_map.111
  114.2 3.6 %all-to-all-start.2 = ((bf16[8,256,256]{2,1,0:T(8,128)(2,1)}), bf16[8,256,256]{2,1,0:T(8,128)(2,1)S(1)}, u32[]{:S(2)}, u32[]{:S(2)}) async-start(bf16[8,256,256]{2,1,0:T(8,128)(2,1)} %shard_map.111), calls=%async_computation.2 | async-start | bytes 2097152 | tf_op jit(solution)/shard_map/all_to_all | solution.py:399
  117.9 1.5 collective-permute-start.3
  119.4 2.3 %collective-permute-start.4 = (bf16[256,2048]{1,0:T(8,128)(2,1)}, bf16[256,2048]{1,0:T(8,128)(2,1)}, u32[]{:S(2)}, u32[]{:S(2)}) collective-permute-start(bf16[256,2048]{1,0:T(8,128)(2,1)} %refs_0_.2), channel_id=1, source_target_pairs={{0,4},{2,6},{4,0},{6,2},{1,5},{3,7},{5,1},{7,3},{8,12},{10,14},{12... | collective-permute-start | bytes 3145736 | tf_op jit(solution)/shard_map/ppermute | solution.py:308
  121.7 0.5 collective-permute-start.5
  122.1 11.6 %all-to-all-done.2.in_ref = bf16[8,256,256]{2,1,0:T(8,128)(2,1)S(1)} async-done(((bf16[8,256,256]{2,1,0:T(8,128)(2,1)}), bf16[8,256,256]{2,1,0:T(8,128)(2,1)S(1)}, u32[]{:S(2)}, u32[]{:S(2)}) %all-to-all-start.2) | async-done | bytes 1048608 | tf_op jit(solution)/shard_map/all_to_all | solution.py:399
  133.7 3.6 %all-to-all-start.1 = ((bf16[8,128,1024]{2,1,0:T(8,128)(2,1)}), bf16[8,128,1024]{2,1,0:T(8,128)(2,1)S(1)}, u32[]{:S(2)}, u32[]{:S(2)}) async-start(bf16[8,128,1024]{2,1,0:T(8,128)(2,1)} %bitcast.29), calls=%async_computation.1 | async-start | bytes 4194304 | tf_op jit(solution)/shard_map/all_to_all | solution.py:346
  137.3 0.9 collective-permute-start.6
  138.2 3.6 %collective-permute-done.3.refs_1_ = bf16[256,2048]{1,0:T(8,128)(2,1)} collective-permute-done((bf16[256,2048]{1,0:T(8,128)(2,1)}, bf16[256,2048]{1,0:T(8,128)(2,1)}, u32[]{:S(2)}, u32[]{:S(2)}) %collective-permute-start.3) | collective-permute-done | bytes 1048608 | tf_op jit(solution)/shard_map/ppermute | solution.py:308
  141.8 4.5 %collective-permute-start.7 = (bf16[256,2048]{1,0:T(8,128)(2,1)}, bf16[256,2048]{1,0:T(8,128)(2,1)}, u32[]{:S(2)}, u32[]{:S(2)}) collective-permute-start(bf16[256,2048]{1,0:T(8,128)(2,1)} %collective-permute-done.3.refs_1_), channel_id=1, source_target_pairs={{0,1},{1,0},{2,3},{3,2},{4,5},{5,4},{6,7},{7,6},{8,9},{9,8},{10,11... | collective-permute-start | bytes 3145736 | tf_op jit(solution)/shard_map/ppermute | solution.py:311
  146.3 19.5 %collective-permute-done.4.refs_2_ = bf16[256,2048]{1,0:T(8,128)(2,1)} collective-permute-done((bf16[256,2048]{1,0:T(8,128)(2,1)}, bf16[256,2048]{1,0:T(8,128)(2,1)}, u32[]{:S(2)}, u32[]{:S(2)}) %collective-permute-start.4) | collective-permute-done | bytes 1048608 | tf_op jit(solution)/shard_map/ppermute | solution.py:308
  165.8 2.8 %collective-permute-start.8 = (bf16[256,2048]{1,0:T(8,128)(2,1)}, bf16[256,2048]{1,0:T(8,128)(2,1)}, u32[]{:S(2)}, u32[]{:S(2)}) collective-permute-start(bf16[256,2048]{1,0:T(8,128)(2,1)} %collective-permute-done.4.refs_2_), channel_id=1, source_target_pairs={{0,1},{1,0},{2,3},{3,2},{4,5},{5,4},{6,7},{7,6},{8,9},{9,8},{10,11... | collective-permute-start | bytes 3145736 | tf_op jit(solution)/shard_map/ppermute | solution.py:311
  168.6 0.1 stack.44.owner_ref
  168.6 1.5 shard_map.112
  170.1 1.1 collective-permute-done.8.refs_6_
  171.2 1.5 collective-permute-done.9.refs_7_
  172.7 7.5 %shard_map.107 = (bf16[128,2048]{1,0:T(8,128)(2,1)}, bf16[128,4096]{1,0:T(8,128)(2,1)}, bf16[128,2048]{1,0:T(8,128)(2,1)}) custom-call(s32[1]{0:T(128)} %bitcast.half_ref, s32[8]{0:T(128)S(1)} %stack.44.owner_ref, bf16[8,128,1024]{2,1,0:T(8,128)(2,1)S(1)} %all-to-all-done.1.home_ref, bf16[256,2048]{1,0:T(8,128)(2,1)} %refs_0_.2, ...), custom_call_target="tpu_custom_call" | custom-call | flops 1121976320 | bytes 4194304 | tf_op jit(solution)/shard_map/pallas_call | solution.py:347
  (20 shorter events, 0.2 us)
Async XLA Ops:
  3.7 6.4 %copy-start = (f32[1,1,2048]{2,1,0:T(1,128)S(1)}, f32[1,1,2048]{2,1,0:T(1,128)}, u32[]{:S(2)}) copy-start(f32[1,1,2048]{2,1,0:T(1,128)} %param.12) | copy-start | bytes 24580
  3.7 51.8 %all-to-all-start = ((bf16[8,128,1536]{2,1,0:T(8,128)(2,1)}), bf16[8,128,1536]{2,1,0:T(8,128)(2,1)S(1)}, u32[]{:S(2)}, u32[]{:S(2)}) async-start(bf16[8,128,1536]{2,1,0:T(8,128)(2,1)} %shard_map.102), calls=%async_computation | async-start | bytes 6291456 | tf_op jit(solution)/shard_map/all_to_all | solution.py:298
  10.1 11.6 %collective-permute-start = (f32[8,128]{1,0:T(8,128)S(1)}, f32[8,128]{1,0:T(8,128)S(1)}, u32[]{:S(2)}, u32[]{:S(2)}) collective-permute-start(f32[8,128]{1,0:T(8,128)S(1)} %get-tuple-element.30), channel_id=1, source_target_pairs={{0,0},{8,96},{16,8},{24,104},{32,16},{40,112},{48,24},{56,120},{64... | collective-permute-start | bytes 12296 | tf_op jit(solution)/shard_map/ppermute | solution.py:287
  10.8 44.3 %collective-permute-start.1 = (f32[8,128]{1,0:T(8,128)S(1)}, f32[8,128]{1,0:T(8,128)S(1)}, u32[]{:S(2)}, u32[]{:S(2)}) collective-permute-start(f32[8,128]{1,0:T(8,128)S(1)} %get-tuple-element.31), channel_id=1, source_target_pairs={{0,96},{8,0},{16,104},{24,8},{32,112},{40,16},{48,120},{56,24},{64... | collective-permute-start | bytes 12296 | tf_op jit(solution)/shard_map/ppermute | solution.py:288
  20.2 42.7 %collective-permute-start.10 = (bf16[1,128,2048]{2,1,0:T(8,128)(2,1)}, bf16[1,128,2048]{2,1,0:T(8,128)(2,1)}, u32[]{:S(2)}, u32[]{:S(2)}) collective-permute-start(bf16[1,128,2048]{2,1,0:T(8,128)(2,1)} %refs_0_.3), channel_id=1, source_target_pairs={{0,32},{8,40},{16,48},{24,56},{32,0},{40,8},{48,16},{56,24},{1,33}... | collective-permute-start | bytes 1572872 | tf_op jit(solution)/shard_map/ppermute | solution.py:289
  21.4 41.6 %collective-permute-start.15 = (bf16[1,128,2048]{2,1,0:T(8,128)(2,1)}, bf16[1,128,2048]{2,1,0:T(8,128)(2,1)}, u32[]{:S(2)}, u32[]{:S(2)}) collective-permute-start(bf16[1,128,2048]{2,1,0:T(8,128)(2,1)} %refs_0_.3), channel_id=1, source_target_pairs={{0,16},{8,24},{16,0},{24,8},{32,48},{40,56},{48,32},{56,40},{1,17}... | collective-permute-start | bytes 1572872 | tf_op jit(solution)/shard_map/ppermute | solution.py:301
  57.9 11.9 %collective-permute-start.2 = (bf16[2,256,512]{2,1,0:T(8,128)(2,1)}, bf16[2,256,512]{2,1,0:T(8,128)(2,1)}, u32[]{:S(2)}, u32[]{:S(2)}) collective-permute-start(bf16[2,256,512]{2,1,0:T(8,128)(2,1)} %shard_map.104), channel_id=1, source_target_pairs={{0,96},{8,104},{16,112},{24,120},{32,64},{40,72},{48,80},{56,88},{... | collective-permute-start | bytes 1572872 | tf_op jit(solution)/shard_map/ppermute | solution.py:321
  59.8 22.0 %collective-permute-start.11 = (bf16[1,128,2048]{2,1,0:T(8,128)(2,1)}, bf16[1,128,2048]{2,1,0:T(8,128)(2,1)}, u32[]{:S(2)}, u32[]{:S(2)}) collective-permute-start(bf16[1,128,2048]{2,1,0:T(8,128)(2,1)} %refs_0_.3), channel_id=1, source_target_pairs={{0,8},{8,16},{16,24},{24,0},{32,40},{40,48},{48,56},{56,32},{1,9},... | collective-permute-start | bytes 1572872 | tf_op jit(solution)/shard_map/ppermute | solution.py:301
  59.9 21.8 %collective-permute-start.12 = (bf16[1,128,2048]{2,1,0:T(8,128)(2,1)}, bf16[1,128,2048]{2,1,0:T(8,128)(2,1)}, u32[]{:S(2)}, u32[]{:S(2)}) collective-permute-start(bf16[1,128,2048]{2,1,0:T(8,128)(2,1)} %refs_0_.3), channel_id=1, source_target_pairs={{0,24},{8,0},{16,8},{24,16},{32,56},{40,32},{48,40},{56,48},{1,25}... | collective-permute-start | bytes 1572872 | tf_op jit(solution)/shard_map/ppermute | solution.py:301
  62.9 20.2 %collective-permute-start.13 = (bf16[1,128,2048]{2,1,0:T(8,128)(2,1)}, bf16[1,128,2048]{2,1,0:T(8,128)(2,1)S(1)}, u32[]{:S(2)}, u32[]{:S(2)}) collective-permute-start(bf16[1,128,2048]{2,1,0:T(8,128)(2,1)} %collective-permute-done.10.refs_1_), channel_id=1, source_target_pairs={{0,8},{8,16},{16,24},{24,0},{32,40},{40,48},{48,56},{56,32},{1,9},... | collective-permute-start | bytes 1572872 | tf_op jit(solution)/shard_map/ppermute | solution.py:301
  63.0 25.7 %collective-permute-start.14 = (bf16[1,128,2048]{2,1,0:T(8,128)(2,1)}, bf16[1,128,2048]{2,1,0:T(8,128)(2,1)S(1)}, u32[]{:S(2)}, u32[]{:S(2)}) collective-permute-start(bf16[1,128,2048]{2,1,0:T(8,128)(2,1)} %collective-permute-done.10.refs_1_), channel_id=1, source_target_pairs={{0,24},{8,0},{16,8},{24,16},{32,56},{40,32},{48,40},{56,48},{1,25}... | collective-permute-start | bytes 1572872 | tf_op jit(solution)/shard_map/ppermute | solution.py:301
  69.8 19.0 %collective-permute-start.16 = (bf16[1,128,2048]{2,1,0:T(8,128)(2,1)}, bf16[1,128,2048]{2,1,0:T(8,128)(2,1)S(1)}, u32[]{:S(2)}, u32[]{:S(2)}) collective-permute-start(bf16[1,128,2048]{2,1,0:T(8,128)(2,1)} %collective-permute-done.15.refs_6_), channel_id=1, source_target_pairs={{0,32},{8,40},{16,48},{24,56},{32,0},{40,8},{48,16},{56,24},{1,33}... | collective-permute-start | bytes 1572872 | tf_op jit(solution)/shard_map/ppermute | solution.py:318
  93.8 3.6 %collective-permute-start.17 = (bf16[4,256,256]{2,1,0:T(8,128)(2,1)}, bf16[4,256,256]{2,1,0:T(8,128)(2,1)S(1)}, u32[]{:S(2)}, u32[]{:S(2)}) collective-permute-start(bf16[4,256,256]{2,1,0:T(8,128)(2,1)} %get-tuple-element.23), channel_id=1, source_target_pairs={{0,1},{1,0},{2,3},{3,2},{4,5},{5,4},{6,7},{7,6},{8,9},{9,8},{10,11... | collective-permute-start | bytes 1572872 | tf_op jit(solution)/shard_map/ppermute | solution.py:383
  97.5 6.1 %collective-permute-start.18 = (bf16[256,256]{1,0:T(8,128)(2,1)S(1)}, bf16[256,256]{1,0:T(8,128)(2,1)S(1)}, u32[]{:S(2)}, u32[]{:S(2)}) collective-permute-start(bf16[256,256]{1,0:T(8,128)(2,1)S(1)} %get-tuple-element.25), channel_id=1, source_target_pairs={{0,2},{2,4},{4,6},{6,0},{1,3},{3,5},{5,7},{7,1},{8,10},{10,12},{12... | collective-permute-start | bytes 393224 | tf_op jit(solution)/shard_map/ppermute | solution.py:393
  99.0 8.5 %collective-permute-start.19 = (bf16[256,256]{1,0:T(8,128)(2,1)S(1)}, bf16[256,256]{1,0:T(8,128)(2,1)S(1)}, u32[]{:S(2)}, u32[]{:S(2)}) collective-permute-start(bf16[256,256]{1,0:T(8,128)(2,1)S(1)} %get-tuple-element.26), channel_id=1, source_target_pairs={{0,4},{2,6},{4,0},{6,2},{1,5},{3,7},{5,1},{7,3},{8,12},{10,14},{12... | collective-permute-start | bytes 393224 | tf_op jit(solution)/shard_map/ppermute | solution.py:393
  101.4 6.0 %collective-permute-start.20 = (bf16[256,256]{1,0:T(8,128)(2,1)S(1)}, bf16[256,256]{1,0:T(8,128)(2,1)S(1)}, u32[]{:S(2)}, u32[]{:S(2)}) collective-permute-start(bf16[256,256]{1,0:T(8,128)(2,1)S(1)} %get-tuple-element.27), channel_id=1, source_target_pairs={{0,6},{2,0},{4,2},{6,4},{1,7},{3,1},{5,3},{7,5},{8,14},{10,8},{12,... | collective-permute-start | bytes 393224 | tf_op jit(solution)/shard_map/ppermute | solution.py:393
  107.5 5.7 %collective-permute-start.21 = (bf16[256,256]{1,0:T(8,128)(2,1)S(1)}, bf16[256,256]{1,0:T(8,128)(2,1)S(1)}, u32[]{:S(2)}, u32[]{:S(2)}) collective-permute-start(bf16[256,256]{1,0:T(8,128)(2,1)S(1)} %get-tuple-element.29), channel_id=1, source_target_pairs={{0,96},{8,104},{16,112},{24,120},{32,64},{40,72},{48,80},{56,88},{... | collective-permute-start | bytes 393224 | tf_op jit(solution)/shard_map/ppermute | solution.py:397
  114.2 19.5 %all-to-all-start.2 = ((bf16[8,256,256]{2,1,0:T(8,128)(2,1)}), bf16[8,256,256]{2,1,0:T(8,128)(2,1)S(1)}, u32[]{:S(2)}, u32[]{:S(2)}) async-start(bf16[8,256,256]{2,1,0:T(8,128)(2,1)} %shard_map.111), calls=%async_computation.2 | async-start | bytes 2097152 | tf_op jit(solution)/shard_map/all_to_all | solution.py:399
  117.9 23.9 %collective-permute-start.3 = (bf16[256,2048]{1,0:T(8,128)(2,1)}, bf16[256,2048]{1,0:T(8,128)(2,1)}, u32[]{:S(2)}, u32[]{:S(2)}) collective-permute-start(bf16[256,2048]{1,0:T(8,128)(2,1)} %refs_0_.2), channel_id=1, source_target_pairs={{0,2},{2,4},{4,6},{6,0},{1,3},{3,5},{5,7},{7,1},{8,10},{10,12},{12... | collective-permute-start | bytes 3145736 | tf_op jit(solution)/shard_map/ppermute | solution.py:308
  119.4 46.4 %collective-permute-start.4 = (bf16[256,2048]{1,0:T(8,128)(2,1)}, bf16[256,2048]{1,0:T(8,128)(2,1)}, u32[]{:S(2)}, u32[]{:S(2)}) collective-permute-start(bf16[256,2048]{1,0:T(8,128)(2,1)} %refs_0_.2), channel_id=1, source_target_pairs={{0,4},{2,6},{4,0},{6,2},{1,5},{3,7},{5,1},{7,3},{8,12},{10,14},{12... | collective-permute-start | bytes 3145736 | tf_op jit(solution)/shard_map/ppermute | solution.py:308
  121.7 46.9 %collective-permute-start.5 = (bf16[256,2048]{1,0:T(8,128)(2,1)}, bf16[256,2048]{1,0:T(8,128)(2,1)}, u32[]{:S(2)}, u32[]{:S(2)}) collective-permute-start(bf16[256,2048]{1,0:T(8,128)(2,1)} %refs_0_.2), channel_id=1, source_target_pairs={{0,6},{2,0},{4,2},{6,4},{1,7},{3,1},{5,3},{7,5},{8,14},{10,8},{12,... | collective-permute-start | bytes 3145736 | tf_op jit(solution)/shard_map/ppermute | solution.py:308
  133.7 39.0 %all-to-all-start.1 = ((bf16[8,128,1024]{2,1,0:T(8,128)(2,1)}), bf16[8,128,1024]{2,1,0:T(8,128)(2,1)S(1)}, u32[]{:S(2)}, u32[]{:S(2)}) async-start(bf16[8,128,1024]{2,1,0:T(8,128)(2,1)} %bitcast.29), calls=%async_computation.1 | async-start | bytes 4194304 | tf_op jit(solution)/shard_map/all_to_all | solution.py:346
  137.3 32.8 %collective-permute-start.6 = (bf16[256,2048]{1,0:T(8,128)(2,1)}, bf16[256,2048]{1,0:T(8,128)(2,1)}, u32[]{:S(2)}, u32[]{:S(2)}) collective-permute-start(bf16[256,2048]{1,0:T(8,128)(2,1)} %refs_0_.2), channel_id=1, source_target_pairs={{0,1},{1,0},{2,3},{3,2},{4,5},{5,4},{6,7},{7,6},{8,9},{9,8},{10,11... | collective-permute-start | bytes 3145736 | tf_op jit(solution)/shard_map/ppermute | solution.py:311
  141.8 28.3 %collective-permute-start.7 = (bf16[256,2048]{1,0:T(8,128)(2,1)}, bf16[256,2048]{1,0:T(8,128)(2,1)}, u32[]{:S(2)}, u32[]{:S(2)}) collective-permute-start(bf16[256,2048]{1,0:T(8,128)(2,1)} %collective-permute-done.3.refs_1_), channel_id=1, source_target_pairs={{0,1},{1,0},{2,3},{3,2},{4,5},{5,4},{6,7},{7,6},{8,9},{9,8},{10,11... | collective-permute-start | bytes 3145736 | tf_op jit(solution)/shard_map/ppermute | solution.py:311
  165.8 5.4 %collective-permute-start.8 = (bf16[256,2048]{1,0:T(8,128)(2,1)}, bf16[256,2048]{1,0:T(8,128)(2,1)}, u32[]{:S(2)}, u32[]{:S(2)}) collective-permute-start(bf16[256,2048]{1,0:T(8,128)(2,1)} %collective-permute-done.4.refs_2_), channel_id=1, source_target_pairs={{0,1},{1,0},{2,3},{3,2},{4,5},{5,4},{6,7},{7,6},{8,9},{9,8},{10,11... | collective-permute-start | bytes 3145736 | tf_op jit(solution)/shard_map/ppermute | solution.py:311
  168.6 4.1 %collective-permute-start.9 = (bf16[256,2048]{1,0:T(8,128)(2,1)}, bf16[256,2048]{1,0:T(8,128)(2,1)}, u32[]{:S(2)}, u32[]{:S(2)}) collective-permute-start(bf16[256,2048]{1,0:T(8,128)(2,1)} %collective-permute-done.5.refs_3_), channel_id=1, source_target_pairs={{0,1},{1,0},{2,3},{3,2},{4,5},{5,4},{6,7},{7,6},{8,9},{9,8},{10,11... | collective-permute-start | bytes 3145736 | tf_op jit(solution)/shard_map/ppermute | solution.py:311

commit v5 on v4

--- a/solution.py
+++ b/solution.py
@@ -208,19 +208,27 @@
     return half * 8 + (head + 4 * half) % 8
 
 
-STEPS = ((0, 0), (1, 0), (0, 3), (0, 1), (1, 3), (1, 1), (0, 2), (1, 2))
-
-
-def term_kernel(place_ref, grads_ref, *refs):
-    pieces, (mine_ref, *theirs), total_ref = refs[:8], refs[8:-1], refs[-1]
-    lane = place_ref[0]
+EARLY = ((0, 0), (1, 0), (0, 3), (0, 1), (0, 2))
+LATE = ((1, 2), (1, 3), (1, 1))
+
+
+def term_sum(lane, grads_ref, pieces, steps, total):
     deep, y = lane // 4, lane % 4
-    total = None
-    for piece, (other, step) in zip(pieces, STEPS, strict=True):
+    for piece, (other, step) in zip(pieces, steps, strict=True):
         block = (deep ^ other) * 4 + (y + step) % 4
         grad = grads_ref[pl.ds(pl.multiple_of(block * BLOCK, BLOCK), BLOCK), :]
         part = dot(piece[0], grad, TN)
         total = part if total is None else total + part
+    return total
+
+
+def early_kernel(place_ref, grads_ref, *refs):
+    refs[-1][...] = term_sum(place_ref[0], grads_ref, refs[:-1], EARLY, None)
+
+
+def late_kernel(place_ref, grads_ref, early_ref, *refs):
+    pieces, (mine_ref, *theirs), total_ref = refs[: len(LATE)], refs[len(LATE) : -1], refs[-1]
+    total = term_sum(place_ref[0], grads_ref, pieces, LATE, early_ref[...])
     slices = mine_ref.shape[0] * (1 + len(theirs))
     total_ref[...] = total.reshape(slices, -1, total.shape[1])
     for k in range(mine_ref.shape[0]):
@@ -356,26 +364,25 @@
     parts = [shape((ring, 2048 // ring // cores, 256), F32)]
     if cores == 2:
         parts.append(pltpu.HBM((ring, 2048 // ring // cores, 256), BF16))
+    place = jnp.stack([lane, core])
+    first = pl.BlockSpec((1024, 256), lambda i: (0, 0))
+    early = kernel(
+        early_kernel,
+        shape((2048, 256), F32),
+        670 << 20,
+        grid=(1,),
+        in_specs=[scalars, first] + [whole] * len(EARLY),
+        out_specs=whole,
+    )(place, in_hbm(grads), own, deep, own_before, own_after, own_last)
     terms, *theirs = kernel(
-        term_kernel,
+        late_kernel,
         parts,
-        1070 << 20,
+        400 << 20,
         (pltpu.VMEM((ring * cores, 2048 // ring // cores, 256), F32),),
         grid=(1,),
-        in_specs=[scalars, pl.BlockSpec((1024, 256), lambda i: (0, 0))] + [whole] * 8,
+        in_specs=[scalars, first] + [whole] * (1 + len(LATE)),
         out_specs=[whole] * len(parts),
-    )(
-        jnp.stack([lane, core]),
-        in_hbm(grads),
-        own,
-        deep,
-        own_before,
-        own_after,
-        deep_before,
-        deep_after,
-        own_last,
-        deep_last,
-    )
+    )(place, in_hbm(grads), early, deep_last, deep_before, deep_after)
 
     piece = terms.shape[1:]
     sends = []

time: 181 us -> 179 us (0.989)
  waiting for transfers between devices: 87.7 us -> 84.3 us
    ppermute x5, waiting for transfers between devices: 7.08 us -> 3.65 us  [lane_step(): lax.ppermute(array, 'lane', [(i, i // 4 * 4 + (i + step) % 4) for i in ra...]
    pallas_call x1 -> x2, Pallas kernels: 5.14 us -> 6.4 us  [the longest x1 3.41 us: shards(): kernel(early_kernel, shape((2048, 256), F32), 670 << 20, grid=(1,), in_sp...]
  transfers between devices with their start and end apart: 25 -> 25, of which waited for: 14 -> 13; matrix products, arithmetic and copies ran while one was open for 0% -> 0% of each run, Pallas kernels for 8% -> 10%
where the time goes in v5:
time: 179 us; the launch traced here: 178 us
  waiting for transfers between devices  84.3 us (47%)
  starting transfers between devices  60.1 us (34%)
  Pallas kernels  32.8 us (18%)
    ppermute x1, waiting for transfers between devices, shards(): lax.ppermute(far, SP, [(u, worker(1 - u % 2, u // 2)) for u in range(peer...  33.4 us
    ppermute x3, waiting for transfers between devices, shards(): weights.append(lax.ppermute(key_weight, 'dp_0', moves))  23.1 us
    all_to_all x1, waiting for transfers between devices, shards(): spread = lax.all_to_all(spread, 'lane', 0, 0, tiled=True)  11.6 us
    ppermute x1, starting transfers between devices, shards(): lax.ppermute(far, SP, [(u, worker(1 - u % 2, u // 2)) for u in range(peer...  9.4 us
    ppermute x5, starting transfers between devices, lane_step(): lax.ppermute(array, 'lane', [(i, i // 4 * 4 + (i + step) % 4) for i in ra...  9.17 us
    ppermute x4, starting transfers between devices, shards(): weights += [lax.ppermute(w, 'dp_1', [(0, 1), (1, 0)]) for w in weights]  8.11 us
    pallas_call x1, Pallas kernels, shards(): kernel(home_kernel, (shape((tokens, 2048), BF16), shape((tokens, 4096), B...  7.53 us
    all_to_all x1, starting transfers between devices, shards(): lax.all_to_all(sent, 'lane', 0, 0, tiled=True).reshape(8 * tokens, -1)  6.37 us
  transfers between devices with their start and end apart: 25, of which 13 were waited for; matrix products, arithmetic and copies ran while one was open for 0% of the time, Pallas kernels for 10%

profile of v5, /device:TPU:1, one launch (start us, length us, event | category | flops | bytes accessed | tf_op | source)
XLA Modules:
  0.0 178.1 jit_solution(11960088435431620696)
XLA Ops:
  0.6 3.0 %shard_map.102 = bf16[8,128,1536]{2,1,0:T(8,128)(2,1)} custom-call(s32[1]{0:T(128)} %bitcast.half_ref, bf16[128,2048]{1,0:T(8,128)(2,1)} %bitcast.32, bf16[128,2048]{1,0:T(8,128)(2,1)} %bitcast.33, bf16[128,4096]{1,0:T(8,128)(2,1)} %bitcast.30, bf16[128,4096]{1,0:T(8,128)(2,1)} %bitcast.31), custom_call_target="tpu_custom_call" | custom-call | flops 1048576 | bytes 6291456 | tf_op jit(solution)/shard_map/pallas_call | solution.py:191
  3.7 6.4 %all-to-all-start = ((bf16[8,128,1536]{2,1,0:T(8,128)(2,1)}), bf16[8,128,1536]{2,1,0:T(8,128)(2,1)S(1)}, u32[]{:S(2)}, u32[]{:S(2)}) async-start(bf16[8,128,1536]{2,1,0:T(8,128)(2,1)} %shard_map.102), calls=%async_computation | async-start | bytes 6291456 | tf_op jit(solution)/shard_map/all_to_all | solution.py:306
  10.1 0.7 collective-permute-start
  10.8 9.4 %collective-permute-start.1 = (f32[8,128]{1,0:T(8,128)S(1)}, f32[8,128]{1,0:T(8,128)S(1)}, u32[]{:S(2)}, u32[]{:S(2)}) collective-permute-start(f32[8,128]{1,0:T(8,128)S(1)} %get-tuple-element.31), channel_id=1, source_target_pairs={{0,96},{8,0},{16,104},{24,8},{32,112},{40,16},{48,120},{56,24},{64... | collective-permute-start | bytes 12296 | tf_op jit(solution)/shard_map/ppermute | solution.py:296
  20.2 1.3 collective-permute-start.10
  21.4 0.3 collective-permute-start.13
  21.7 33.4 %collective-permute-done.1 = f32[8,128]{1,0:T(8,128)S(1)} collective-permute-done((f32[8,128]{1,0:T(8,128)S(1)}, f32[8,128]{1,0:T(8,128)S(1)}, u32[]{:S(2)}, u32[]{:S(2)}) %collective-permute-start.1) | collective-permute-done | bytes 4128 | tf_op jit(solution)/shard_map/ppermute | solution.py:296
  55.1 0.4 shard_map.103
  55.5 2.4 %shard_map.104 = bf16[2,256,512]{2,1,0:T(8,128)(2,1)} custom-call(bf16[1024,1536]{1,0:T(8,128)(2,1)S(1)} %bitcast.26, f32[32,128]{1,0:T(8,128)S(1)} %get-tuple-element.17.factors_ref), custom_call_target="tpu_custom_call" | custom-call | flops 566231040 | bytes 4194304 | tf_op jit(solution)/shard_map/pallas_call | solution.py:328
  57.9 1.9 %collective-permute-start.2 = (bf16[2,256,512]{2,1,0:T(8,128)(2,1)}, bf16[2,256,512]{2,1,0:T(8,128)(2,1)}, u32[]{:S(2)}, u32[]{:S(2)}) collective-permute-start(bf16[2,256,512]{2,1,0:T(8,128)(2,1)} %shard_map.104), channel_id=1, source_target_pairs={{0,96},{8,104},{16,112},{24,120},{32,64},{40,72},{48,80},{56,88},{... | collective-permute-start | bytes 1572872 | tf_op jit(solution)/shard_map/ppermute | solution.py:329
  59.8 0.1 collective-permute-start.11
  59.9 3.0 %collective-permute-start.12 = (bf16[1,128,2048]{2,1,0:T(8,128)(2,1)}, bf16[1,128,2048]{2,1,0:T(8,128)(2,1)}, u32[]{:S(2)}, u32[]{:S(2)}) collective-permute-start(bf16[1,128,2048]{2,1,0:T(8,128)(2,1)} %refs_0_.3), channel_id=1, source_target_pairs={{0,24},{8,0},{16,8},{24,16},{32,56},{40,32},{48,40},{56,48},{1,25}... | collective-permute-start | bytes 1572872 | tf_op jit(solution)/shard_map/ppermute | solution.py:309
  62.9 0.1 collective-permute-done.13.refs_4_
  63.0 5.7 %collective-permute-start.16 = (bf16[1,128,2048]{2,1,0:T(8,128)(2,1)}, bf16[1,128,2048]{2,1,0:T(8,128)(2,1)S(1)}, u32[]{:S(2)}, u32[]{:S(2)}) collective-permute-start(bf16[1,128,2048]{2,1,0:T(8,128)(2,1)} %collective-permute-done.10.refs_1_), channel_id=1, source_target_pairs={{0,24},{8,0},{16,8},{24,16},{32,56},{40,32},{48,40},{56,48},{1,25}... | collective-permute-start | bytes 1572872 | tf_op jit(solution)/shard_map/ppermute | solution.py:309
  68.7 1.0 collective-permute-done.2.state_ref
  69.8 1.5 collective-permute-start.14
  71.3 5.6 %shard_map.105.part_ref = bf16[1024,1024]{1,0:T(8,128)(2,1)} custom-call(bf16[1024,1536]{1,0:T(8,128)(2,1)S(1)} %bitcast.27, f32[40,128]{1,0:T(8,128)S(1)} %get-tuple-element.18.rows_ref, f32[32,128]{1,0:T(8,128)S(1)} %get-tuple-element.17.factors_ref), custom_call_target="tpu_custom_call" | custom-call | flops 3942645760 | bytes 4194304 | tf_op jit(solution)/shard_map/pallas_call | solution.py:330
  76.9 4.8 %shard_map.106.grads_ref = bf16[1024,1024]{1,0:T(8,128)(2,1)} custom-call(bf16[1024,1536]{1,0:T(8,128)(2,1)S(1)} %bitcast.28, f32[32,128]{1,0:T(8,128)S(1)} %get-tuple-element.17.factors_ref, bf16[2,256,512]{2,1,0:T(8,128)(2,1)} %collective-permute-done.2.state_ref, bf16[1024,1024]{1,0:T(8,128)(2,1)} %shard_map.105.part_ref), custom_call_target="tpu_custom_call" | custom-call | flops 838860800 | bytes 4194304 | tf_op jit(solution)/shard_map/pallas_call | solution.py:340
  81.7 3.4 %shard_map.108.early_ref = f32[2048,256]{1,0:T(8,128)S(1)} custom-call(s32[2]{0:T(128)S(1)} %pad_add_fusion.place_ref, bf16[1024,1024]{1,0:T(8,128)(2,1)} %shard_map.106.grads_ref, bf16[1,128,2048]{2,1,0:T(8,128)(2,1)} %refs_0_.3, bf16[1,128,2048]{2,1,0:T(8,128)(2,1)} %collective-permute-done.10.refs_1_, ...), custom_call_target="tpu_custom_call" | custom-call | flops 702545920 | bytes 4194304 | tf_op jit(solution)/shard_map/pallas_call | solution.py:369
  85.1 3.6 %collective-permute-done.16.refs_2_ = bf16[1,128,2048]{2,1,0:T(8,128)(2,1)S(1)} collective-permute-done((bf16[1,128,2048]{2,1,0:T(8,128)(2,1)}, bf16[1,128,2048]{2,1,0:T(8,128)(2,1)S(1)}, u32[]{:S(2)}, u32[]{:S(2)}) %collective-permute-start.16) | collective-permute-done | bytes 524320 | tf_op jit(solution)/shard_map/ppermute | solution.py:309
  88.7 3.0 %shard_map.109 = (f32[4,256,256]{2,1,0:T(8,128)S(1)}, bf16[4,256,256]{2,1,0:T(8,128)(2,1)}) custom-call(s32[2]{0:T(128)S(1)} %pad_add_fusion.place_ref, bf16[1024,1024]{1,0:T(8,128)(2,1)} %shard_map.106.grads_ref, f32[2048,256]{1,0:T(8,128)S(1)} %shard_map.108.early_ref, bf16[1,128,2048]{2,1,0:T(8,128)(2,1)S(1)} %collective-permute-done.14.refs_0_, ...), custom_call_target="tpu_custom_call" | custom-call | flops 419430400 | bytes 4194304 | tf_op jit(solution)/shard_map/pallas_call | solution.py:377
  91.7 1.8 %collective-permute-start.17 = (bf16[4,256,256]{2,1,0:T(8,128)(2,1)}, bf16[4,256,256]{2,1,0:T(8,128)(2,1)S(1)}, u32[]{:S(2)}, u32[]{:S(2)}) collective-permute-start(bf16[4,256,256]{2,1,0:T(8,128)(2,1)} %get-tuple-element.23), channel_id=1, source_target_pairs={{0,1},{1,0},{2,3},{3,2},{4,5},{5,4},{6,7},{7,6},{8,9},{9,8},{10,11... | collective-permute-start | bytes 1572872 | tf_op jit(solution)/shard_map/ppermute | solution.py:390
  93.5 1.7 collective-permute-done.17.theirs_ref
  95.3 0.1 shard_map.110
  95.3 1.5 collective-permute-start.18
  96.8 2.4 %collective-permute-start.19 = (bf16[256,256]{1,0:T(8,128)(2,1)S(1)}, bf16[256,256]{1,0:T(8,128)(2,1)S(1)}, u32[]{:S(2)}, u32[]{:S(2)}) collective-permute-start(bf16[256,256]{1,0:T(8,128)(2,1)S(1)} %get-tuple-element.26), channel_id=1, source_target_pairs={{0,4},{2,6},{4,0},{6,2},{1,5},{3,7},{5,1},{7,3},{8,12},{10,14},{12... | collective-permute-start | bytes 393224 | tf_op jit(solution)/shard_map/ppermute | solution.py:400
  99.3 1.2 collective-permute-start.20
  100.4 1.1 collective-permute-done.18.refs_1_
  101.5 3.8 %collective-permute-done.19.refs_2_ = bf16[256,256]{1,0:T(8,128)(2,1)S(1)} collective-permute-done((bf16[256,256]{1,0:T(8,128)(2,1)S(1)}, bf16[256,256]{1,0:T(8,128)(2,1)S(1)}, u32[]{:S(2)}, u32[]{:S(2)}) %collective-permute-start.19) | collective-permute-done | bytes 131104 | tf_op jit(solution)/shard_map/ppermute | solution.py:400
  105.4 3.3 %collective-permute-start.21 = (bf16[256,256]{1,0:T(8,128)(2,1)S(1)}, bf16[256,256]{1,0:T(8,128)(2,1)S(1)}, u32[]{:S(2)}, u32[]{:S(2)}) collective-permute-start(bf16[256,256]{1,0:T(8,128)(2,1)S(1)} %get-tuple-element.29), channel_id=1, source_target_pairs={{0,96},{8,104},{16,112},{24,120},{32,64},{40,72},{48,80},{56,88},{... | collective-permute-start | bytes 393224 | tf_op jit(solution)/shard_map/ppermute | solution.py:404
  108.7 2.4 %collective-permute-done.21.theirs_ref = bf16[256,256]{1,0:T(8,128)(2,1)S(1)} collective-permute-done((bf16[256,256]{1,0:T(8,128)(2,1)S(1)}, bf16[256,256]{1,0:T(8,128)(2,1)S(1)}, u32[]{:S(2)}, u32[]{:S(2)}) %collective-permute-start.21) | collective-permute-done | bytes 131104 | tf_op jit(solution)/shard_map/ppermute | solution.py:404
  111.0 1.0 shard_map.112
  112.1 3.6 %all-to-all-start.2 = ((bf16[8,256,256]{2,1,0:T(8,128)(2,1)}), bf16[8,256,256]{2,1,0:T(8,128)(2,1)S(1)}, u32[]{:S(2)}, u32[]{:S(2)}) async-start(bf16[8,256,256]{2,1,0:T(8,128)(2,1)} %shard_map.112), calls=%async_computation.2 | async-start | bytes 2097152 | tf_op jit(solution)/shard_map/all_to_all | solution.py:406
  115.7 1.5 collective-permute-start.3
  117.2 2.3 %collective-permute-start.4 = (bf16[256,2048]{1,0:T(8,128)(2,1)}, bf16[256,2048]{1,0:T(8,128)(2,1)}, u32[]{:S(2)}, u32[]{:S(2)}) collective-permute-start(bf16[256,2048]{1,0:T(8,128)(2,1)} %refs_0_.2), channel_id=1, source_target_pairs={{0,4},{2,6},{4,0},{6,2},{1,5},{3,7},{5,1},{7,3},{8,12},{10,14},{12... | collective-permute-start | bytes 3145736 | tf_op jit(solution)/shard_map/ppermute | solution.py:316
  119.5 0.5 collective-permute-start.5
  120.0 11.6 %all-to-all-done.2.in_ref = bf16[8,256,256]{2,1,0:T(8,128)(2,1)S(1)} async-done(((bf16[8,256,256]{2,1,0:T(8,128)(2,1)}), bf16[8,256,256]{2,1,0:T(8,128)(2,1)S(1)}, u32[]{:S(2)}, u32[]{:S(2)}) %all-to-all-start.2) | async-done | bytes 1048608 | tf_op jit(solution)/shard_map/all_to_all | solution.py:406
  131.6 3.6 %all-to-all-start.1 = ((bf16[8,128,1024]{2,1,0:T(8,128)(2,1)}), bf16[8,128,1024]{2,1,0:T(8,128)(2,1)S(1)}, u32[]{:S(2)}, u32[]{:S(2)}) async-start(bf16[8,128,1024]{2,1,0:T(8,128)(2,1)} %bitcast.29), calls=%async_computation.1 | async-start | bytes 4194304 | tf_op jit(solution)/shard_map/all_to_all | solution.py:354
  135.2 0.9 collective-permute-start.6
  136.1 3.6 %collective-permute-done.3.refs_1_ = bf16[256,2048]{1,0:T(8,128)(2,1)} collective-permute-done((bf16[256,2048]{1,0:T(8,128)(2,1)}, bf16[256,2048]{1,0:T(8,128)(2,1)}, u32[]{:S(2)}, u32[]{:S(2)}) %collective-permute-start.3) | collective-permute-done | bytes 1048608 | tf_op jit(solution)/shard_map/ppermute | solution.py:316
  139.7 4.5 %collective-permute-start.7 = (bf16[256,2048]{1,0:T(8,128)(2,1)}, bf16[256,2048]{1,0:T(8,128)(2,1)}, u32[]{:S(2)}, u32[]{:S(2)}) collective-permute-start(bf16[256,2048]{1,0:T(8,128)(2,1)} %collective-permute-done.3.refs_1_), channel_id=1, source_target_pairs={{0,1},{1,0},{2,3},{3,2},{4,5},{5,4},{6,7},{7,6},{8,9},{9,8},{10,11... | collective-permute-start | bytes 3145736 | tf_op jit(solution)/shard_map/ppermute | solution.py:319
  144.1 19.5 %collective-permute-done.4.refs_2_ = bf16[256,2048]{1,0:T(8,128)(2,1)} collective-permute-done((bf16[256,2048]{1,0:T(8,128)(2,1)}, bf16[256,2048]{1,0:T(8,128)(2,1)}, u32[]{:S(2)}, u32[]{:S(2)}) %collective-permute-start.4) | collective-permute-done | bytes 1048608 | tf_op jit(solution)/shard_map/ppermute | solution.py:316
  163.6 2.8 %collective-permute-start.8 = (bf16[256,2048]{1,0:T(8,128)(2,1)}, bf16[256,2048]{1,0:T(8,128)(2,1)}, u32[]{:S(2)}, u32[]{:S(2)}) collective-permute-start(bf16[256,2048]{1,0:T(8,128)(2,1)} %collective-permute-done.4.refs_2_), channel_id=1, source_target_pairs={{0,1},{1,0},{2,3},{3,2},{4,5},{5,4},{6,7},{7,6},{8,9},{9,8},{10,11... | collective-permute-start | bytes 3145736 | tf_op jit(solution)/shard_map/ppermute | solution.py:319
  166.4 0.1 stack.44.owner_ref
  166.5 1.5 shard_map.113
  168.0 1.1 collective-permute-done.8.refs_6_
  169.0 1.5 collective-permute-done.9.refs_7_
  170.5 7.5 %shard_map.107 = (bf16[128,2048]{1,0:T(8,128)(2,1)}, bf16[128,4096]{1,0:T(8,128)(2,1)}, bf16[128,2048]{1,0:T(8,128)(2,1)}) custom-call(s32[1]{0:T(128)} %bitcast.half_ref, s32[8]{0:T(128)S(1)} %stack.44.owner_ref, bf16[8,128,1024]{2,1,0:T(8,128)(2,1)S(1)} %all-to-all-done.1.home_ref, bf16[256,2048]{1,0:T(8,128)(2,1)} %refs_0_.2, ...), custom_call_target="tpu_custom_call" | custom-call | flops 1121976320 | bytes 4194304 | tf_op jit(solution)/shard_map/pallas_call | solution.py:355
  (21 shorter events, 0.2 us)
Async XLA Ops:
  3.7 6.4 %copy-start = (f32[1,1,2048]{2,1,0:T(1,128)S(1)}, f32[1,1,2048]{2,1,0:T(1,128)}, u32[]{:S(2)}) copy-start(f32[1,1,2048]{2,1,0:T(1,128)} %param.12) | copy-start | bytes 24580
  3.7 51.8 %all-to-all-start = ((bf16[8,128,1536]{2,1,0:T(8,128)(2,1)}), bf16[8,128,1536]{2,1,0:T(8,128)(2,1)S(1)}, u32[]{:S(2)}, u32[]{:S(2)}) async-start(bf16[8,128,1536]{2,1,0:T(8,128)(2,1)} %shard_map.102), calls=%async_computation | async-start | bytes 6291456 | tf_op jit(solution)/shard_map/all_to_all | solution.py:306
  10.1 11.6 %collective-permute-start = (f32[8,128]{1,0:T(8,128)S(1)}, f32[8,128]{1,0:T(8,128)S(1)}, u32[]{:S(2)}, u32[]{:S(2)}) collective-permute-start(f32[8,128]{1,0:T(8,128)S(1)} %get-tuple-element.30), channel_id=1, source_target_pairs={{0,0},{8,96},{16,8},{24,104},{32,16},{40,112},{48,24},{56,120},{64... | collective-permute-start | bytes 12296 | tf_op jit(solution)/shard_map/ppermute | solution.py:295
  10.8 44.3 %collective-permute-start.1 = (f32[8,128]{1,0:T(8,128)S(1)}, f32[8,128]{1,0:T(8,128)S(1)}, u32[]{:S(2)}, u32[]{:S(2)}) collective-permute-start(f32[8,128]{1,0:T(8,128)S(1)} %get-tuple-element.31), channel_id=1, source_target_pairs={{0,96},{8,0},{16,104},{24,8},{32,112},{40,16},{48,120},{56,24},{64... | collective-permute-start | bytes 12296 | tf_op jit(solution)/shard_map/ppermute | solution.py:296
  20.2 42.7 %collective-permute-start.10 = (bf16[1,128,2048]{2,1,0:T(8,128)(2,1)}, bf16[1,128,2048]{2,1,0:T(8,128)(2,1)}, u32[]{:S(2)}, u32[]{:S(2)}) collective-permute-start(bf16[1,128,2048]{2,1,0:T(8,128)(2,1)} %refs_0_.3), channel_id=1, source_target_pairs={{0,32},{8,40},{16,48},{24,56},{32,0},{40,8},{48,16},{56,24},{1,33}... | collective-permute-start | bytes 1572872 | tf_op jit(solution)/shard_map/ppermute | solution.py:297
  21.4 41.6 %collective-permute-start.13 = (bf16[1,128,2048]{2,1,0:T(8,128)(2,1)}, bf16[1,128,2048]{2,1,0:T(8,128)(2,1)}, u32[]{:S(2)}, u32[]{:S(2)}) collective-permute-start(bf16[1,128,2048]{2,1,0:T(8,128)(2,1)} %refs_0_.3), channel_id=1, source_target_pairs={{0,16},{8,24},{16,0},{24,8},{32,48},{40,56},{48,32},{56,40},{1,17}... | collective-permute-start | bytes 1572872 | tf_op jit(solution)/shard_map/ppermute | solution.py:309
  57.9 11.9 %collective-permute-start.2 = (bf16[2,256,512]{2,1,0:T(8,128)(2,1)}, bf16[2,256,512]{2,1,0:T(8,128)(2,1)}, u32[]{:S(2)}, u32[]{:S(2)}) collective-permute-start(bf16[2,256,512]{2,1,0:T(8,128)(2,1)} %shard_map.104), channel_id=1, source_target_pairs={{0,96},{8,104},{16,112},{24,120},{32,64},{40,72},{48,80},{56,88},{... | collective-permute-start | bytes 1572872 | tf_op jit(solution)/shard_map/ppermute | solution.py:329
  59.8 22.0 %collective-permute-start.11 = (bf16[1,128,2048]{2,1,0:T(8,128)(2,1)}, bf16[1,128,2048]{2,1,0:T(8,128)(2,1)}, u32[]{:S(2)}, u32[]{:S(2)}) collective-permute-start(bf16[1,128,2048]{2,1,0:T(8,128)(2,1)} %refs_0_.3), channel_id=1, source_target_pairs={{0,8},{8,16},{16,24},{24,0},{32,40},{40,48},{48,56},{56,32},{1,9},... | collective-permute-start | bytes 1572872 | tf_op jit(solution)/shard_map/ppermute | solution.py:309
  59.9 21.8 %collective-permute-start.12 = (bf16[1,128,2048]{2,1,0:T(8,128)(2,1)}, bf16[1,128,2048]{2,1,0:T(8,128)(2,1)}, u32[]{:S(2)}, u32[]{:S(2)}) collective-permute-start(bf16[1,128,2048]{2,1,0:T(8,128)(2,1)} %refs_0_.3), channel_id=1, source_target_pairs={{0,24},{8,0},{16,8},{24,16},{32,56},{40,32},{48,40},{56,48},{1,25}... | collective-permute-start | bytes 1572872 | tf_op jit(solution)/shard_map/ppermute | solution.py:309
  62.9 22.2 %collective-permute-start.15 = (bf16[1,128,2048]{2,1,0:T(8,128)(2,1)}, bf16[1,128,2048]{2,1,0:T(8,128)(2,1)S(1)}, u32[]{:S(2)}, u32[]{:S(2)}) collective-permute-start(bf16[1,128,2048]{2,1,0:T(8,128)(2,1)} %collective-permute-done.10.refs_1_), channel_id=1, source_target_pairs={{0,8},{8,16},{16,24},{24,0},{32,40},{40,48},{48,56},{56,32},{1,9},... | collective-permute-start | bytes 1572872 | tf_op jit(solution)/shard_map/ppermute | solution.py:309
  63.0 25.7 %collective-permute-start.16 = (bf16[1,128,2048]{2,1,0:T(8,128)(2,1)}, bf16[1,128,2048]{2,1,0:T(8,128)(2,1)S(1)}, u32[]{:S(2)}, u32[]{:S(2)}) collective-permute-start(bf16[1,128,2048]{2,1,0:T(8,128)(2,1)} %collective-permute-done.10.refs_1_), channel_id=1, source_target_pairs={{0,24},{8,0},{16,8},{24,16},{32,56},{40,32},{48,40},{56,48},{1,25}... | collective-permute-start | bytes 1572872 | tf_op jit(solution)/shard_map/ppermute | solution.py:309
  69.8 19.0 %collective-permute-start.14 = (bf16[1,128,2048]{2,1,0:T(8,128)(2,1)}, bf16[1,128,2048]{2,1,0:T(8,128)(2,1)S(1)}, u32[]{:S(2)}, u32[]{:S(2)}) collective-permute-start(bf16[1,128,2048]{2,1,0:T(8,128)(2,1)} %collective-permute-done.13.refs_4_), channel_id=1, source_target_pairs={{0,32},{8,40},{16,48},{24,56},{32,0},{40,8},{48,16},{56,24},{1,33}... | collective-permute-start | bytes 1572872 | tf_op jit(solution)/shard_map/ppermute | solution.py:326
  91.7 3.6 %collective-permute-start.17 = (bf16[4,256,256]{2,1,0:T(8,128)(2,1)}, bf16[4,256,256]{2,1,0:T(8,128)(2,1)S(1)}, u32[]{:S(2)}, u32[]{:S(2)}) collective-permute-start(bf16[4,256,256]{2,1,0:T(8,128)(2,1)} %get-tuple-element.23), channel_id=1, source_target_pairs={{0,1},{1,0},{2,3},{3,2},{4,5},{5,4},{6,7},{7,6},{8,9},{9,8},{10,11... | collective-permute-start | bytes 1572872 | tf_op jit(solution)/shard_map/ppermute | solution.py:390
  95.3 6.1 %collective-permute-start.18 = (bf16[256,256]{1,0:T(8,128)(2,1)S(1)}, bf16[256,256]{1,0:T(8,128)(2,1)S(1)}, u32[]{:S(2)}, u32[]{:S(2)}) collective-permute-start(bf16[256,256]{1,0:T(8,128)(2,1)S(1)} %get-tuple-element.25), channel_id=1, source_target_pairs={{0,2},{2,4},{4,6},{6,0},{1,3},{3,5},{5,7},{7,1},{8,10},{10,12},{12... | collective-permute-start | bytes 393224 | tf_op jit(solution)/shard_map/ppermute | solution.py:400
  96.8 8.5 %collective-permute-start.19 = (bf16[256,256]{1,0:T(8,128)(2,1)S(1)}, bf16[256,256]{1,0:T(8,128)(2,1)S(1)}, u32[]{:S(2)}, u32[]{:S(2)}) collective-permute-start(bf16[256,256]{1,0:T(8,128)(2,1)S(1)} %get-tuple-element.26), channel_id=1, source_target_pairs={{0,4},{2,6},{4,0},{6,2},{1,5},{3,7},{5,1},{7,3},{8,12},{10,14},{12... | collective-permute-start | bytes 393224 | tf_op jit(solution)/shard_map/ppermute | solution.py:400
  99.3 6.0 %collective-permute-start.20 = (bf16[256,256]{1,0:T(8,128)(2,1)S(1)}, bf16[256,256]{1,0:T(8,128)(2,1)S(1)}, u32[]{:S(2)}, u32[]{:S(2)}) collective-permute-start(bf16[256,256]{1,0:T(8,128)(2,1)S(1)} %get-tuple-element.27), channel_id=1, source_target_pairs={{0,6},{2,0},{4,2},{6,4},{1,7},{3,1},{5,3},{7,5},{8,14},{10,8},{12,... | collective-permute-start | bytes 393224 | tf_op jit(solution)/shard_map/ppermute | solution.py:400
  105.4 5.7 %collective-permute-start.21 = (bf16[256,256]{1,0:T(8,128)(2,1)S(1)}, bf16[256,256]{1,0:T(8,128)(2,1)S(1)}, u32[]{:S(2)}, u32[]{:S(2)}) collective-permute-start(bf16[256,256]{1,0:T(8,128)(2,1)S(1)} %get-tuple-element.29), channel_id=1, source_target_pairs={{0,96},{8,104},{16,112},{24,120},{32,64},{40,72},{48,80},{56,88},{... | collective-permute-start | bytes 393224 | tf_op jit(solution)/shard_map/ppermute | solution.py:404
  112.1 19.5 %all-to-all-start.2 = ((bf16[8,256,256]{2,1,0:T(8,128)(2,1)}), bf16[8,256,256]{2,1,0:T(8,128)(2,1)S(1)}, u32[]{:S(2)}, u32[]{:S(2)}) async-start(bf16[8,256,256]{2,1,0:T(8,128)(2,1)} %shard_map.112), calls=%async_computation.2 | async-start | bytes 2097152 | tf_op jit(solution)/shard_map/all_to_all | solution.py:406
  115.7 23.9 %collective-permute-start.3 = (bf16[256,2048]{1,0:T(8,128)(2,1)}, bf16[256,2048]{1,0:T(8,128)(2,1)}, u32[]{:S(2)}, u32[]{:S(2)}) collective-permute-start(bf16[256,2048]{1,0:T(8,128)(2,1)} %refs_0_.2), channel_id=1, source_target_pairs={{0,2},{2,4},{4,6},{6,0},{1,3},{3,5},{5,7},{7,1},{8,10},{10,12},{12... | collective-permute-start | bytes 3145736 | tf_op jit(solution)/shard_map/ppermute | solution.py:316
  117.2 46.4 %collective-permute-start.4 = (bf16[256,2048]{1,0:T(8,128)(2,1)}, bf16[256,2048]{1,0:T(8,128)(2,1)}, u32[]{:S(2)}, u32[]{:S(2)}) collective-permute-start(bf16[256,2048]{1,0:T(8,128)(2,1)} %refs_0_.2), channel_id=1, source_target_pairs={{0,4},{2,6},{4,0},{6,2},{1,5},{3,7},{5,1},{7,3},{8,12},{10,14},{12... | collective-permute-start | bytes 3145736 | tf_op jit(solution)/shard_map/ppermute | solution.py:316
  119.5 46.9 %collective-permute-start.5 = (bf16[256,2048]{1,0:T(8,128)(2,1)}, bf16[256,2048]{1,0:T(8,128)(2,1)}, u32[]{:S(2)}, u32[]{:S(2)}) collective-permute-start(bf16[256,2048]{1,0:T(8,128)(2,1)} %refs_0_.2), channel_id=1, source_target_pairs={{0,6},{2,0},{4,2},{6,4},{1,7},{3,1},{5,3},{7,5},{8,14},{10,8},{12,... | collective-permute-start | bytes 3145736 | tf_op jit(solution)/shard_map/ppermute | solution.py:316
  131.6 38.9 %all-to-all-start.1 = ((bf16[8,128,1024]{2,1,0:T(8,128)(2,1)}), bf16[8,128,1024]{2,1,0:T(8,128)(2,1)S(1)}, u32[]{:S(2)}, u32[]{:S(2)}) async-start(bf16[8,128,1024]{2,1,0:T(8,128)(2,1)} %bitcast.29), calls=%async_computation.1 | async-start | bytes 4194304 | tf_op jit(solution)/shard_map/all_to_all | solution.py:354
  135.2 32.8 %collective-permute-start.6 = (bf16[256,2048]{1,0:T(8,128)(2,1)}, bf16[256,2048]{1,0:T(8,128)(2,1)}, u32[]{:S(2)}, u32[]{:S(2)}) collective-permute-start(bf16[256,2048]{1,0:T(8,128)(2,1)} %refs_0_.2), channel_id=1, source_target_pairs={{0,1},{1,0},{2,3},{3,2},{4,5},{5,4},{6,7},{7,6},{8,9},{9,8},{10,11... | collective-permute-start | bytes 3145736 | tf_op jit(solution)/shard_map/ppermute | solution.py:319
  139.7 28.3 %collective-permute-start.7 = (bf16[256,2048]{1,0:T(8,128)(2,1)}, bf16[256,2048]{1,0:T(8,128)(2,1)}, u32[]{:S(2)}, u32[]{:S(2)}) collective-permute-start(bf16[256,2048]{1,0:T(8,128)(2,1)} %collective-permute-done.3.refs_1_), channel_id=1, source_target_pairs={{0,1},{1,0},{2,3},{3,2},{4,5},{5,4},{6,7},{7,6},{8,9},{9,8},{10,11... | collective-permute-start | bytes 3145736 | tf_op jit(solution)/shard_map/ppermute | solution.py:319
  163.6 5.4 %collective-permute-start.8 = (bf16[256,2048]{1,0:T(8,128)(2,1)}, bf16[256,2048]{1,0:T(8,128)(2,1)}, u32[]{:S(2)}, u32[]{:S(2)}) collective-permute-start(bf16[256,2048]{1,0:T(8,128)(2,1)} %collective-permute-done.4.refs_2_), channel_id=1, source_target_pairs={{0,1},{1,0},{2,3},{3,2},{4,5},{5,4},{6,7},{7,6},{8,9},{9,8},{10,11... | collective-permute-start | bytes 3145736 | tf_op jit(solution)/shard_map/ppermute | solution.py:319
  166.4 4.1 %collective-permute-start.9 = (bf16[256,2048]{1,0:T(8,128)(2,1)}, bf16[256,2048]{1,0:T(8,128)(2,1)}, u32[]{:S(2)}, u32[]{:S(2)}) collective-permute-start(bf16[256,2048]{1,0:T(8,128)(2,1)} %collective-permute-done.5.refs_3_), channel_id=1, source_target_pairs={{0,1},{1,0},{2,3},{3,2},{4,5},{5,4},{6,7},{7,6},{8,9},{9,8},{10,11... | collective-permute-start | bytes 3145736 | tf_op jit(solution)/shard_map/ppermute | solution.py:319

commit v6 on v5

--- a/solution.py
+++ b/solution.py
@@ -1,3 +1,5 @@
+import functools
+
 import jax
 import jax.numpy as jnp
 from jax import lax
@@ -226,17 +228,23 @@
     refs[-1][...] = term_sum(place_ref[0], grads_ref, refs[:-1], EARLY, None)
 
 
-def late_kernel(place_ref, grads_ref, early_ref, *refs):
-    pieces, (mine_ref, *theirs), total_ref = refs[: len(LATE)], refs[len(LATE) : -1], refs[-1]
-    total = term_sum(place_ref[0], grads_ref, pieces, LATE, early_ref[...])
-    slices = mine_ref.shape[0] * (1 + len(theirs))
-    total_ref[...] = total.reshape(slices, -1, total.shape[1])
-    for k in range(mine_ref.shape[0]):
-        if theirs:
-            mine_ref[k] = total_ref[2 * k + place_ref[1]]
-            theirs[0][k] = total_ref[2 * k + 1 - place_ref[1]].astype(BF16)
-        else:
-            mine_ref[k] = total_ref[k]
+def late_kernel(side, place_ref, grads_ref, early_ref, *refs):
+    pieces, out_ref = refs[:-1], refs[-1]
+    ring, span, _ = out_ref.shape
+    cores = early_ref.shape[0] // (ring * span)
+    lane = place_ref[0]
+    deep, y = lane // 4, lane % 4
+    grads = []
+    for other, step in LATE:
+        block = (deep ^ other) * 4 + (y + step) % 4
+        grads.append(grads_ref[pl.ds(pl.multiple_of(block * BLOCK, BLOCK), BLOCK), :])
+    for k in range(ring):
+        owner = cores * k + (place_ref[1] if side == 0 else 1 - place_ref[1])
+        at = pl.multiple_of(owner * span, span)
+        total = early_ref[pl.ds(at, span), :]
+        for piece, grad in zip(pieces, grads, strict=True):
+            total = total + dot(piece[0, :, pl.ds(at, span)], grad, TN)
+        out_ref[k] = total.astype(out_ref.dtype)
 
 
 def core_sum_kernel(turn_ref, mine_ref, theirs_ref, own_ref, *send_refs):
@@ -361,9 +369,6 @@
         out_specs=(whole, whole, whole),
     )(half.reshape(1), jnp.stack(owners), home, *weights)
 
-    parts = [shape((ring, 2048 // ring // cores, 256), F32)]
-    if cores == 2:
-        parts.append(pltpu.HBM((ring, 2048 // ring // cores, 256), BF16))
     place = jnp.stack([lane, core])
     first = pl.BlockSpec((1024, 256), lambda i: (0, 0))
     early = kernel(
@@ -374,20 +379,24 @@
         in_specs=[scalars, first] + [whole] * len(EARLY),
         out_specs=whole,
     )(place, in_hbm(grads), own, deep, own_before, own_after, own_last)
-    terms, *theirs = kernel(
-        late_kernel,
-        parts,
-        400 << 20,
-        (pltpu.VMEM((ring * cores, 2048 // ring // cores, 256), F32),),
-        grid=(1,),
-        in_specs=[scalars, first] + [whole] * (1 + len(LATE)),
-        out_specs=[whole] * len(parts),
-    )(place, in_hbm(grads), early, deep_last, deep_before, deep_after)
-
-    piece = terms.shape[1:]
+
+    def late(side, out_shape):
+        return kernel(
+            functools.partial(late_kernel, side),
+            out_shape,
+            200 << 20,
+            grid=(1,),
+            in_specs=[scalars, first] + [whole] * (1 + len(LATE)),
+            out_specs=whole,
+        )(place, in_hbm(grads), early, deep_last, deep_before, deep_after)
+
+    piece = (2048 // ring // cores, 256)
     sends = []
     if cores == 2:
-        theirs = lax.ppermute(theirs[0], "dp_1", [(0, 1), (1, 0)])
+        theirs = late(1, pltpu.HBM((ring, *piece), BF16))
+        theirs = lax.ppermute(theirs, "dp_1", [(0, 1), (1, 0)])
+    terms = late(0, shape((ring, *piece), F32))
+    if cores == 2:
         terms, *sends = kernel(
             core_sum_kernel,
             [shape(piece, F32)] + [shape(piece, BF16)] * (ring - 1),

time: 179 us -> 182 us (1.017)
  local copies, waits for them, and re-layouts: 0.1 us -> 3.24 us
    unnamed x2 -> x14, local copies, waits for them, and re-layouts: 0.01 us -> 3.14 us
    pallas_call x1 -> x2, Pallas kernels: 2.99 us -> 4.49 us  [late(): kernel(functools.partial(late_kernel, side), out_shape, 200 << 20, grid=(...]
  transfers between devices with their start and end apart: 25 -> 25, of which waited for: 13 -> 12; matrix products, arithmetic and copies ran while one was open for 0% -> 0% of each run, Pallas kernels for 10% -> 11%
where the time goes in v6:
time: 182 us
  waiting for transfers between devices  84.1 us (46%)
  starting transfers between devices  59.1 us (32%)
  Pallas kernels  34.3 us (19%)
  local copies, waits for them, and re-layouts  3.24 us (2%)
    ppermute x1, waiting for transfers between devices, shards(): lax.ppermute(far, SP, [(u, worker(1 - u % 2, u // 2)) for u in range(peer...  33.4 us
    ppermute x3, waiting for transfers between devices, shards(): weights.append(lax.ppermute(key_weight, 'dp_0', moves))  23.4 us
    all_to_all x1, waiting for transfers between devices, shards(): spread = lax.all_to_all(spread, 'lane', 0, 0, tiled=True)  11.9 us
    ppermute x1, starting transfers between devices, shards(): lax.ppermute(far, SP, [(u, worker(1 - u % 2, u // 2)) for u in range(peer...  9.4 us
    ppermute x5, starting transfers between devices, lane_step(): lax.ppermute(array, 'lane', [(i, i // 4 * 4 + (i + step) % 4) for i in ra...  9.16 us
    pallas_call x1, Pallas kernels, shards(): kernel(home_kernel, (shape((tokens, 2048), BF16), shape((tokens, 4096), B...  7.53 us
    ppermute x4, starting transfers between devices, shards(): weights += [lax.ppermute(w, 'dp_1', [(0, 1), (1, 0)]) for w in weights]  7.36 us
    all_to_all x1, starting transfers between devices, shards(): lax.all_to_all(sent, 'lane', 0, 0, tiled=True).reshape(8 * tokens, -1)  6.37 us
  transfers between devices with their start and end apart: 25, of which 12 were waited for; matrix products, arithmetic and copies ran while one was open for 0% of the time, Pallas kernels for 11%

profile of v6, /device:TPU:1, one launch (start us, length us, event | category | flops | bytes accessed | tf_op | source)
XLA Modules:
  0.0 181.6 jit_solution(8569887702865289880)
XLA Ops:
  0.6 3.1 %shard_map.102 = bf16[8,128,1536]{2,1,0:T(8,128)(2,1)} custom-call(s32[1]{0:T(128)} %bitcast.half_ref, bf16[128,2048]{1,0:T(8,128)(2,1)} %bitcast.32, bf16[128,2048]{1,0:T(8,128)(2,1)} %bitcast.33, bf16[128,4096]{1,0:T(8,128)(2,1)} %bitcast.30, bf16[128,4096]{1,0:T(8,128)(2,1)} %bitcast.31), custom_call_target="tpu_custom_call" | custom-call | flops 1048576 | bytes 6291456 | tf_op jit(solution)/shard_map/pallas_call | solution.py:193
  3.7 6.4 %all-to-all-start = ((bf16[8,128,1536]{2,1,0:T(8,128)(2,1)}), bf16[8,128,1536]{2,1,0:T(8,128)(2,1)S(1)}, u32[]{:S(2)}, u32[]{:S(2)}) async-start(bf16[8,128,1536]{2,1,0:T(8,128)(2,1)} %shard_map.102), calls=%async_computation | async-start | bytes 6291456 | tf_op jit(solution)/shard_map/all_to_all | solution.py:314
  10.1 0.7 collective-permute-start
  10.8 9.4 %collective-permute-start.1 = (f32[8,128]{1,0:T(8,128)S(1)}, f32[8,128]{1,0:T(8,128)S(1)}, u32[]{:S(2)}, u32[]{:S(2)}) collective-permute-start(f32[8,128]{1,0:T(8,128)S(1)} %get-tuple-element.27), channel_id=1, source_target_pairs={{0,96},{8,0},{16,104},{24,8},{32,112},{40,16},{48,120},{56,24},{64... | collective-permute-start | bytes 12296 | tf_op jit(solution)/shard_map/ppermute | solution.py:304
  20.2 1.3 collective-permute-start.10
  21.4 0.3 collective-permute-start.13
  21.7 33.4 %collective-permute-done.1 = f32[8,128]{1,0:T(8,128)S(1)} collective-permute-done((f32[8,128]{1,0:T(8,128)S(1)}, f32[8,128]{1,0:T(8,128)S(1)}, u32[]{:S(2)}, u32[]{:S(2)}) %collective-permute-start.1) | collective-permute-done | bytes 4128 | tf_op jit(solution)/shard_map/ppermute | solution.py:304
  55.1 0.4 shard_map.103
  55.5 2.4 %shard_map.104 = bf16[2,256,512]{2,1,0:T(8,128)(2,1)} custom-call(bf16[1024,1536]{1,0:T(8,128)(2,1)S(1)} %bitcast.26, f32[32,128]{1,0:T(8,128)S(1)} %get-tuple-element.15.factors_ref), custom_call_target="tpu_custom_call" | custom-call | flops 566231040 | bytes 4194304 | tf_op jit(solution)/shard_map/pallas_call | solution.py:336
  57.9 1.9 %collective-permute-start.2 = (bf16[2,256,512]{2,1,0:T(8,128)(2,1)}, bf16[2,256,512]{2,1,0:T(8,128)(2,1)}, u32[]{:S(2)}, u32[]{:S(2)}) collective-permute-start(bf16[2,256,512]{2,1,0:T(8,128)(2,1)} %shard_map.104), channel_id=1, source_target_pairs={{0,96},{8,104},{16,112},{24,120},{32,64},{40,72},{48,80},{56,88},{... | collective-permute-start | bytes 1572872 | tf_op jit(solution)/shard_map/ppermute | solution.py:337
  59.8 0.1 collective-permute-start.11
  59.9 3.0 %collective-permute-start.12 = (bf16[1,128,2048]{2,1,0:T(8,128)(2,1)}, bf16[1,128,2048]{2,1,0:T(8,128)(2,1)}, u32[]{:S(2)}, u32[]{:S(2)}) collective-permute-start(bf16[1,128,2048]{2,1,0:T(8,128)(2,1)} %refs_0_.3), channel_id=1, source_target_pairs={{0,24},{8,0},{16,8},{24,16},{32,56},{40,32},{48,40},{56,48},{1,25}... | collective-permute-start | bytes 1572872 | tf_op jit(solution)/shard_map/ppermute | solution.py:317
  63.0 5.7 %collective-permute-start.16 = (bf16[1,128,2048]{2,1,0:T(8,128)(2,1)}, bf16[1,128,2048]{2,1,0:T(8,128)(2,1)S(1)}, u32[]{:S(2)}, u32[]{:S(2)}) collective-permute-start(bf16[1,128,2048]{2,1,0:T(8,128)(2,1)} %collective-permute-done.10.refs_1_), channel_id=1, source_target_pairs={{0,24},{8,0},{16,8},{24,16},{32,56},{40,32},{48,40},{56,48},{1,25}... | collective-permute-start | bytes 1572872 | tf_op jit(solution)/shard_map/ppermute | solution.py:317
  68.7 1.0 collective-permute-done.2.state_ref
  69.7 1.5 collective-permute-start.14
  71.3 5.6 %shard_map.105.part_ref = bf16[1024,1024]{1,0:T(8,128)(2,1)} custom-call(bf16[1024,1536]{1,0:T(8,128)(2,1)S(1)} %bitcast.27, f32[40,128]{1,0:T(8,128)S(1)} %get-tuple-element.16.rows_ref, f32[32,128]{1,0:T(8,128)S(1)} %get-tuple-element.15.factors_ref), custom_call_target="tpu_custom_call" | custom-call | flops 3942645760 | bytes 4194304 | tf_op jit(solution)/shard_map/pallas_call | solution.py:338
  77.0 4.8 %shard_map.106.grads_ref = bf16[1024,1024]{1,0:T(8,128)(2,1)} custom-call(bf16[1024,1536]{1,0:T(8,128)(2,1)S(1)} %bitcast.28, f32[32,128]{1,0:T(8,128)S(1)} %get-tuple-element.15.factors_ref, bf16[2,256,512]{2,1,0:T(8,128)(2,1)} %collective-permute-done.2.state_ref, bf16[1024,1024]{1,0:T(8,128)(2,1)} %shard_map.105.part_ref), custom_call_target="tpu_custom_call" | custom-call | flops 838860800 | bytes 4194304 | tf_op jit(solution)/shard_map/pallas_call | solution.py:348
  81.7 3.4 %shard_map.108.early_ref = f32[2048,256]{1,0:T(8,128)S(1)} custom-call(s32[2]{0:T(128)S(1)} %pad_add_fusion.place_ref, bf16[1024,1024]{1,0:T(8,128)(2,1)} %shard_map.106.grads_ref, bf16[1,128,2048]{2,1,0:T(8,128)(2,1)} %refs_0_.3, bf16[1,128,2048]{2,1,0:T(8,128)(2,1)} %collective-permute-done.10.refs_1_, ...), custom_call_target="tpu_custom_call" | custom-call | flops 702545920 | bytes 4194304 | tf_op jit(solution)/shard_map/pallas_call | solution.py:374
  85.2 3.5 %collective-permute-done.16.refs_2_ = bf16[1,128,2048]{2,1,0:T(8,128)(2,1)S(1)} collective-permute-done((bf16[1,128,2048]{2,1,0:T(8,128)(2,1)}, bf16[1,128,2048]{2,1,0:T(8,128)(2,1)S(1)}, u32[]{:S(2)}, u32[]{:S(2)}) %collective-permute-start.16) | collective-permute-done | bytes 524320 | tf_op jit(solution)/shard_map/ppermute | solution.py:317
  88.7 2.8 %shard_map.110 = bf16[4,256,256]{2,1,0:T(8,128)(2,1)} custom-call(s32[2]{0:T(128)S(1)} %pad_add_fusion.place_ref, bf16[1024,1024]{1,0:T(8,128)(2,1)} %shard_map.106.grads_ref, f32[2048,256]{1,0:T(8,128)S(1)} %shard_map.108.early_ref, bf16[1,128,2048]{2,1,0:T(8,128)(2,1)S(1)} %collective-permute-done.14.refs_0_, ...), custom_call_target="tpu_custom_call" | custom-call | flops 209715200 | bytes 4194304 | tf_op jit(solution)/shard_map/pallas_call | solution.py:384
  91.6 1.9 %collective-permute-start.17 = (bf16[4,256,256]{2,1,0:T(8,128)(2,1)}, bf16[4,256,256]{2,1,0:T(8,128)(2,1)S(1)}, u32[]{:S(2)}, u32[]{:S(2)}) collective-permute-start(bf16[4,256,256]{2,1,0:T(8,128)(2,1)} %shard_map.110), channel_id=1, source_target_pairs={{0,1},{1,0},{2,3},{3,2},{4,5},{5,4},{6,7},{7,6},{8,9},{9,8},{10,11... | collective-permute-start | bytes 1572872 | tf_op jit(solution)/shard_map/ppermute | solution.py:397
  93.5 1.0 copy-done.1
  94.5 1.0 copy-done.3
  95.5 1.0 copy-done.5
  96.6 1.7 shard_map.109.mine_ref
  98.4 1.5 collective-permute-start.18
  99.8 2.5 %collective-permute-start.19 = (bf16[256,256]{1,0:T(8,128)(2,1)S(1)}, bf16[256,256]{1,0:T(8,128)(2,1)S(1)}, u32[]{:S(2)}, u32[]{:S(2)}) collective-permute-start(bf16[256,256]{1,0:T(8,128)(2,1)S(1)} %get-tuple-element.22), channel_id=1, source_target_pairs={{0,4},{2,6},{4,0},{6,2},{1,5},{3,7},{5,1},{7,3},{8,12},{10,14},{12... | collective-permute-start | bytes 393224 | tf_op jit(solution)/shard_map/ppermute | solution.py:409
  102.3 1.1 collective-permute-start.20
  103.4 1.4 collective-permute-done.18.refs_1_
  104.9 3.8 %collective-permute-done.19.refs_2_ = bf16[256,256]{1,0:T(8,128)(2,1)S(1)} collective-permute-done((bf16[256,256]{1,0:T(8,128)(2,1)S(1)}, bf16[256,256]{1,0:T(8,128)(2,1)S(1)}, u32[]{:S(2)}, u32[]{:S(2)}) %collective-permute-start.19) | collective-permute-done | bytes 131104 | tf_op jit(solution)/shard_map/ppermute | solution.py:409
  108.7 3.3 %collective-permute-start.21 = (bf16[256,256]{1,0:T(8,128)(2,1)S(1)}, bf16[256,256]{1,0:T(8,128)(2,1)S(1)}, u32[]{:S(2)}, u32[]{:S(2)}) collective-permute-start(bf16[256,256]{1,0:T(8,128)(2,1)S(1)} %get-tuple-element.25), channel_id=1, source_target_pairs={{0,96},{8,104},{16,112},{24,120},{32,64},{40,72},{48,80},{56,88},{... | collective-permute-start | bytes 393224 | tf_op jit(solution)/shard_map/ppermute | solution.py:413
  112.0 3.0 %collective-permute-done.21.theirs_ref = bf16[256,256]{1,0:T(8,128)(2,1)S(1)} collective-permute-done((bf16[256,256]{1,0:T(8,128)(2,1)S(1)}, bf16[256,256]{1,0:T(8,128)(2,1)S(1)}, u32[]{:S(2)}, u32[]{:S(2)}) %collective-permute-start.21) | collective-permute-done | bytes 131104 | tf_op jit(solution)/shard_map/ppermute | solution.py:413
  115.0 1.0 shard_map.113
  116.1 3.6 %all-to-all-start.2 = ((bf16[8,256,256]{2,1,0:T(8,128)(2,1)}), bf16[8,256,256]{2,1,0:T(8,128)(2,1)S(1)}, u32[]{:S(2)}, u32[]{:S(2)}) async-start(bf16[8,256,256]{2,1,0:T(8,128)(2,1)} %shard_map.113), calls=%async_computation.2 | async-start | bytes 2097152 | tf_op jit(solution)/shard_map/all_to_all | solution.py:415
  119.7 0.5 collective-permute-start.3
  120.2 2.8 %collective-permute-start.4 = (bf16[256,2048]{1,0:T(8,128)(2,1)}, bf16[256,2048]{1,0:T(8,128)(2,1)}, u32[]{:S(2)}, u32[]{:S(2)}) collective-permute-start(bf16[256,2048]{1,0:T(8,128)(2,1)} %refs_0_.2), channel_id=1, source_target_pairs={{0,4},{2,6},{4,0},{6,2},{1,5},{3,7},{5,1},{7,3},{8,12},{10,14},{12... | collective-permute-start | bytes 3145736 | tf_op jit(solution)/shard_map/ppermute | solution.py:324
  123.0 0.6 collective-permute-start.5
  123.6 11.9 %all-to-all-done.2.in_ref = bf16[8,256,256]{2,1,0:T(8,128)(2,1)S(1)} async-done(((bf16[8,256,256]{2,1,0:T(8,128)(2,1)}), bf16[8,256,256]{2,1,0:T(8,128)(2,1)S(1)}, u32[]{:S(2)}, u32[]{:S(2)}) %all-to-all-start.2) | async-done | bytes 1048608 | tf_op jit(solution)/shard_map/all_to_all | solution.py:415
  135.6 3.6 %all-to-all-start.1 = ((bf16[8,128,1024]{2,1,0:T(8,128)(2,1)}), bf16[8,128,1024]{2,1,0:T(8,128)(2,1)S(1)}, u32[]{:S(2)}, u32[]{:S(2)}) async-start(bf16[8,128,1024]{2,1,0:T(8,128)(2,1)} %bitcast.29), calls=%async_computation.1 | async-start | bytes 4194304 | tf_op jit(solution)/shard_map/all_to_all | solution.py:362
  139.2 0.9 collective-permute-start.6
  140.0 4.3 %collective-permute-done.3.refs_1_ = bf16[256,2048]{1,0:T(8,128)(2,1)} collective-permute-done((bf16[256,2048]{1,0:T(8,128)(2,1)}, bf16[256,2048]{1,0:T(8,128)(2,1)}, u32[]{:S(2)}, u32[]{:S(2)}) %collective-permute-start.3) | collective-permute-done | bytes 1048608 | tf_op jit(solution)/shard_map/ppermute | solution.py:324
  144.3 4.0 %collective-permute-start.7 = (bf16[256,2048]{1,0:T(8,128)(2,1)}, bf16[256,2048]{1,0:T(8,128)(2,1)}, u32[]{:S(2)}, u32[]{:S(2)}) collective-permute-start(bf16[256,2048]{1,0:T(8,128)(2,1)} %collective-permute-done.3.refs_1_), channel_id=1, source_target_pairs={{0,1},{1,0},{2,3},{3,2},{4,5},{5,4},{6,7},{7,6},{8,9},{9,8},{10,11... | collective-permute-start | bytes 3145736 | tf_op jit(solution)/shard_map/ppermute | solution.py:327
  148.3 19.2 %collective-permute-done.4.refs_2_ = bf16[256,2048]{1,0:T(8,128)(2,1)} collective-permute-done((bf16[256,2048]{1,0:T(8,128)(2,1)}, bf16[256,2048]{1,0:T(8,128)(2,1)}, u32[]{:S(2)}, u32[]{:S(2)}) %collective-permute-start.4) | collective-permute-done | bytes 1048608 | tf_op jit(solution)/shard_map/ppermute | solution.py:324
  167.5 2.5 %collective-permute-start.8 = (bf16[256,2048]{1,0:T(8,128)(2,1)}, bf16[256,2048]{1,0:T(8,128)(2,1)}, u32[]{:S(2)}, u32[]{:S(2)}) collective-permute-start(bf16[256,2048]{1,0:T(8,128)(2,1)} %collective-permute-done.4.refs_2_), channel_id=1, source_target_pairs={{0,1},{1,0},{2,3},{3,2},{4,5},{5,4},{6,7},{7,6},{8,9},{9,8},{10,11... | collective-permute-start | bytes 3145736 | tf_op jit(solution)/shard_map/ppermute | solution.py:327
  170.0 1.5 shard_map.114
  171.5 1.1 collective-permute-done.8.refs_6_
  172.6 1.5 collective-permute-done.9.refs_7_
  174.1 7.5 %shard_map.107 = (bf16[128,2048]{1,0:T(8,128)(2,1)}, bf16[128,4096]{1,0:T(8,128)(2,1)}, bf16[128,2048]{1,0:T(8,128)(2,1)}) custom-call(s32[1]{0:T(128)} %bitcast.half_ref, s32[8]{0:T(128)S(1)} %stack.44.owner_ref, bf16[8,128,1024]{2,1,0:T(8,128)(2,1)S(1)} %all-to-all-done.1.home_ref, bf16[256,2048]{1,0:T(8,128)(2,1)} %refs_0_.2, ...), custom_call_target="tpu_custom_call" | custom-call | flops 1121976320 | bytes 4194304 | tf_op jit(solution)/shard_map/pallas_call | solution.py:363
  (34 shorter events, 0.5 us)
Async XLA Ops:
  3.7 6.4 %copy-start.6 = (f32[1,1,2048]{2,1,0:T(1,128)S(1)}, f32[1,1,2048]{2,1,0:T(1,128)}, u32[]{:S(2)}) copy-start(f32[1,1,2048]{2,1,0:T(1,128)} %param.12) | copy-start | bytes 24580
  3.7 51.8 %all-to-all-start = ((bf16[8,128,1536]{2,1,0:T(8,128)(2,1)}), bf16[8,128,1536]{2,1,0:T(8,128)(2,1)S(1)}, u32[]{:S(2)}, u32[]{:S(2)}) async-start(bf16[8,128,1536]{2,1,0:T(8,128)(2,1)} %shard_map.102), calls=%async_computation | async-start | bytes 6291456 | tf_op jit(solution)/shard_map/all_to_all | solution.py:314
  10.1 11.6 %collective-permute-start = (f32[8,128]{1,0:T(8,128)S(1)}, f32[8,128]{1,0:T(8,128)S(1)}, u32[]{:S(2)}, u32[]{:S(2)}) collective-permute-start(f32[8,128]{1,0:T(8,128)S(1)} %get-tuple-element.26), channel_id=1, source_target_pairs={{0,0},{8,96},{16,8},{24,104},{32,16},{40,112},{48,24},{56,120},{64... | collective-permute-start | bytes 12296 | tf_op jit(solution)/shard_map/ppermute | solution.py:303
  10.8 44.3 %collective-permute-start.1 = (f32[8,128]{1,0:T(8,128)S(1)}, f32[8,128]{1,0:T(8,128)S(1)}, u32[]{:S(2)}, u32[]{:S(2)}) collective-permute-start(f32[8,128]{1,0:T(8,128)S(1)} %get-tuple-element.27), channel_id=1, source_target_pairs={{0,96},{8,0},{16,104},{24,8},{32,112},{40,16},{48,120},{56,24},{64... | collective-permute-start | bytes 12296 | tf_op jit(solution)/shard_map/ppermute | solution.py:304
  20.2 42.7 %collective-permute-start.10 = (bf16[1,128,2048]{2,1,0:T(8,128)(2,1)}, bf16[1,128,2048]{2,1,0:T(8,128)(2,1)}, u32[]{:S(2)}, u32[]{:S(2)}) collective-permute-start(bf16[1,128,2048]{2,1,0:T(8,128)(2,1)} %refs_0_.3), channel_id=1, source_target_pairs={{0,32},{8,40},{16,48},{24,56},{32,0},{40,8},{48,16},{56,24},{1,33}... | collective-permute-start | bytes 1572872 | tf_op jit(solution)/shard_map/ppermute | solution.py:305
  21.4 41.6 %collective-permute-start.13 = (bf16[1,128,2048]{2,1,0:T(8,128)(2,1)}, bf16[1,128,2048]{2,1,0:T(8,128)(2,1)}, u32[]{:S(2)}, u32[]{:S(2)}) collective-permute-start(bf16[1,128,2048]{2,1,0:T(8,128)(2,1)} %refs_0_.3), channel_id=1, source_target_pairs={{0,16},{8,24},{16,0},{24,8},{32,48},{40,56},{48,32},{56,40},{1,17}... | collective-permute-start | bytes 1572872 | tf_op jit(solution)/shard_map/ppermute | solution.py:317
  57.9 11.9 %collective-permute-start.2 = (bf16[2,256,512]{2,1,0:T(8,128)(2,1)}, bf16[2,256,512]{2,1,0:T(8,128)(2,1)}, u32[]{:S(2)}, u32[]{:S(2)}) collective-permute-start(bf16[2,256,512]{2,1,0:T(8,128)(2,1)} %shard_map.104), channel_id=1, source_target_pairs={{0,96},{8,104},{16,112},{24,120},{32,64},{40,72},{48,80},{56,88},{... | collective-permute-start | bytes 1572872 | tf_op jit(solution)/shard_map/ppermute | solution.py:337
  59.8 22.0 %collective-permute-start.11 = (bf16[1,128,2048]{2,1,0:T(8,128)(2,1)}, bf16[1,128,2048]{2,1,0:T(8,128)(2,1)}, u32[]{:S(2)}, u32[]{:S(2)}) collective-permute-start(bf16[1,128,2048]{2,1,0:T(8,128)(2,1)} %refs_0_.3), channel_id=1, source_target_pairs={{0,8},{8,16},{16,24},{24,0},{32,40},{40,48},{48,56},{56,32},{1,9},... | collective-permute-start | bytes 1572872 | tf_op jit(solution)/shard_map/ppermute | solution.py:317
  59.9 21.8 %collective-permute-start.12 = (bf16[1,128,2048]{2,1,0:T(8,128)(2,1)}, bf16[1,128,2048]{2,1,0:T(8,128)(2,1)}, u32[]{:S(2)}, u32[]{:S(2)}) collective-permute-start(bf16[1,128,2048]{2,1,0:T(8,128)(2,1)} %refs_0_.3), channel_id=1, source_target_pairs={{0,24},{8,0},{16,8},{24,16},{32,56},{40,32},{48,40},{56,48},{1,25}... | collective-permute-start | bytes 1572872 | tf_op jit(solution)/shard_map/ppermute | solution.py:317
  62.9 22.2 %collective-permute-start.15 = (bf16[1,128,2048]{2,1,0:T(8,128)(2,1)}, bf16[1,128,2048]{2,1,0:T(8,128)(2,1)S(1)}, u32[]{:S(2)}, u32[]{:S(2)}) collective-permute-start(bf16[1,128,2048]{2,1,0:T(8,128)(2,1)} %collective-permute-done.10.refs_1_), channel_id=1, source_target_pairs={{0,8},{8,16},{16,24},{24,0},{32,40},{40,48},{48,56},{56,32},{1,9},... | collective-permute-start | bytes 1572872 | tf_op jit(solution)/shard_map/ppermute | solution.py:317
  63.0 25.7 %collective-permute-start.16 = (bf16[1,128,2048]{2,1,0:T(8,128)(2,1)}, bf16[1,128,2048]{2,1,0:T(8,128)(2,1)S(1)}, u32[]{:S(2)}, u32[]{:S(2)}) collective-permute-start(bf16[1,128,2048]{2,1,0:T(8,128)(2,1)} %collective-permute-done.10.refs_1_), channel_id=1, source_target_pairs={{0,24},{8,0},{16,8},{24,16},{32,56},{40,32},{48,40},{56,48},{1,25}... | collective-permute-start | bytes 1572872 | tf_op jit(solution)/shard_map/ppermute | solution.py:317
  69.7 19.0 %collective-permute-start.14 = (bf16[1,128,2048]{2,1,0:T(8,128)(2,1)}, bf16[1,128,2048]{2,1,0:T(8,128)(2,1)S(1)}, u32[]{:S(2)}, u32[]{:S(2)}) collective-permute-start(bf16[1,128,2048]{2,1,0:T(8,128)(2,1)} %collective-permute-done.13.refs_4_), channel_id=1, source_target_pairs={{0,32},{8,40},{16,48},{24,56},{32,0},{40,8},{48,16},{56,24},{1,33}... | collective-permute-start | bytes 1572872 | tf_op jit(solution)/shard_map/ppermute | solution.py:334
  85.2 6.4 %copy-start = (bf16[1,128,2048]{2,1,0:T(8,128)(2,1)}, bf16[1,128,2048]{2,1,0:T(8,128)(2,1)S(1)}, u32[]{:S(2)}) copy-start(bf16[1,128,2048]{2,1,0:T(8,128)(2,1)S(1)} %collective-permute-done.15.refs_1_) | copy-start | bytes 1572868
  88.7 2.9 %copy-start.2 = (bf16[1,128,2048]{2,1,0:T(8,128)(2,1)}, bf16[1,128,2048]{2,1,0:T(8,128)(2,1)S(1)}, u32[]{:S(2)}) copy-start(bf16[1,128,2048]{2,1,0:T(8,128)(2,1)S(1)} %collective-permute-done.16.refs_2_) | copy-start | bytes 1572868
  88.7 2.8 %copy-start.4 = (bf16[1,128,2048]{2,1,0:T(8,128)(2,1)}, bf16[1,128,2048]{2,1,0:T(8,128)(2,1)S(1)}, u32[]{:S(2)}) copy-start(bf16[1,128,2048]{2,1,0:T(8,128)(2,1)S(1)} %collective-permute-done.14.refs_0_) | copy-start | bytes 1572868
  91.6 6.7 %collective-permute-start.17 = (bf16[4,256,256]{2,1,0:T(8,128)(2,1)}, bf16[4,256,256]{2,1,0:T(8,128)(2,1)S(1)}, u32[]{:S(2)}, u32[]{:S(2)}) collective-permute-start(bf16[4,256,256]{2,1,0:T(8,128)(2,1)} %shard_map.110), channel_id=1, source_target_pairs={{0,1},{1,0},{2,3},{3,2},{4,5},{5,4},{6,7},{7,6},{8,9},{9,8},{10,11... | collective-permute-start | bytes 1572872 | tf_op jit(solution)/shard_map/ppermute | solution.py:397
  93.5 1.0 copy-start.1
  94.5 1.0 copy-start.3
  95.5 1.0 copy-start.5
  98.4 6.5 %collective-permute-start.18 = (bf16[256,256]{1,0:T(8,128)(2,1)S(1)}, bf16[256,256]{1,0:T(8,128)(2,1)S(1)}, u32[]{:S(2)}, u32[]{:S(2)}) collective-permute-start(bf16[256,256]{1,0:T(8,128)(2,1)S(1)} %get-tuple-element.21), channel_id=1, source_target_pairs={{0,2},{2,4},{4,6},{6,0},{1,3},{3,5},{5,7},{7,1},{8,10},{10,12},{12... | collective-permute-start | bytes 393224 | tf_op jit(solution)/shard_map/ppermute | solution.py:409
  99.8 8.8 %collective-permute-start.19 = (bf16[256,256]{1,0:T(8,128)(2,1)S(1)}, bf16[256,256]{1,0:T(8,128)(2,1)S(1)}, u32[]{:S(2)}, u32[]{:S(2)}) collective-permute-start(bf16[256,256]{1,0:T(8,128)(2,1)S(1)} %get-tuple-element.22), channel_id=1, source_target_pairs={{0,4},{2,6},{4,0},{6,2},{1,5},{3,7},{5,1},{7,3},{8,12},{10,14},{12... | collective-permute-start | bytes 393224 | tf_op jit(solution)/shard_map/ppermute | solution.py:409
  102.3 6.4 %collective-permute-start.20 = (bf16[256,256]{1,0:T(8,128)(2,1)S(1)}, bf16[256,256]{1,0:T(8,128)(2,1)S(1)}, u32[]{:S(2)}, u32[]{:S(2)}) collective-permute-start(bf16[256,256]{1,0:T(8,128)(2,1)S(1)} %get-tuple-element.23), channel_id=1, source_target_pairs={{0,6},{2,0},{4,2},{6,4},{1,7},{3,1},{5,3},{7,5},{8,14},{10,8},{12,... | collective-permute-start | bytes 393224 | tf_op jit(solution)/shard_map/ppermute | solution.py:409
  108.7 6.3 %collective-permute-start.21 = (bf16[256,256]{1,0:T(8,128)(2,1)S(1)}, bf16[256,256]{1,0:T(8,128)(2,1)S(1)}, u32[]{:S(2)}, u32[]{:S(2)}) collective-permute-start(bf16[256,256]{1,0:T(8,128)(2,1)S(1)} %get-tuple-element.25), channel_id=1, source_target_pairs={{0,96},{8,104},{16,112},{24,120},{32,64},{40,72},{48,80},{56,88},{... | collective-permute-start | bytes 393224 | tf_op jit(solution)/shard_map/ppermute | solution.py:413
  116.1 19.5 %all-to-all-start.2 = ((bf16[8,256,256]{2,1,0:T(8,128)(2,1)}), bf16[8,256,256]{2,1,0:T(8,128)(2,1)S(1)}, u32[]{:S(2)}, u32[]{:S(2)}) async-start(bf16[8,256,256]{2,1,0:T(8,128)(2,1)} %shard_map.113), calls=%async_computation.2 | async-start | bytes 2097152 | tf_op jit(solution)/shard_map/all_to_all | solution.py:415
  119.7 24.6 %collective-permute-start.3 = (bf16[256,2048]{1,0:T(8,128)(2,1)}, bf16[256,2048]{1,0:T(8,128)(2,1)}, u32[]{:S(2)}, u32[]{:S(2)}) collective-permute-start(bf16[256,2048]{1,0:T(8,128)(2,1)} %refs_0_.2), channel_id=1, source_target_pairs={{0,2},{2,4},{4,6},{6,0},{1,3},{3,5},{5,7},{7,1},{8,10},{10,12},{12... | collective-permute-start | bytes 3145736 | tf_op jit(solution)/shard_map/ppermute | solution.py:324
  120.2 47.2 %collective-permute-start.4 = (bf16[256,2048]{1,0:T(8,128)(2,1)}, bf16[256,2048]{1,0:T(8,128)(2,1)}, u32[]{:S(2)}, u32[]{:S(2)}) collective-permute-start(bf16[256,2048]{1,0:T(8,128)(2,1)} %refs_0_.2), channel_id=1, source_target_pairs={{0,4},{2,6},{4,0},{6,2},{1,5},{3,7},{5,1},{7,3},{8,12},{10,14},{12... | collective-permute-start | bytes 3145736 | tf_op jit(solution)/shard_map/ppermute | solution.py:324
  123.0 46.9 %collective-permute-start.5 = (bf16[256,2048]{1,0:T(8,128)(2,1)}, bf16[256,2048]{1,0:T(8,128)(2,1)}, u32[]{:S(2)}, u32[]{:S(2)}) collective-permute-start(bf16[256,2048]{1,0:T(8,128)(2,1)} %refs_0_.2), channel_id=1, source_target_pairs={{0,6},{2,0},{4,2},{6,4},{1,7},{3,1},{5,3},{7,5},{8,14},{10,8},{12,... | collective-permute-start | bytes 3145736 | tf_op jit(solution)/shard_map/ppermute | solution.py:324
  135.6 38.5 %all-to-all-start.1 = ((bf16[8,128,1024]{2,1,0:T(8,128)(2,1)}), bf16[8,128,1024]{2,1,0:T(8,128)(2,1)S(1)}, u32[]{:S(2)}, u32[]{:S(2)}) async-start(bf16[8,128,1024]{2,1,0:T(8,128)(2,1)} %bitcast.29), calls=%async_computation.1 | async-start | bytes 4194304 | tf_op jit(solution)/shard_map/all_to_all | solution.py:362
  139.2 32.3 %collective-permute-start.6 = (bf16[256,2048]{1,0:T(8,128)(2,1)}, bf16[256,2048]{1,0:T(8,128)(2,1)}, u32[]{:S(2)}, u32[]{:S(2)}) collective-permute-start(bf16[256,2048]{1,0:T(8,128)(2,1)} %refs_0_.2), channel_id=1, source_target_pairs={{0,1},{1,0},{2,3},{3,2},{4,5},{5,4},{6,7},{7,6},{8,9},{9,8},{10,11... | collective-permute-start | bytes 3145736 | tf_op jit(solution)/shard_map/ppermute | solution.py:327
  144.3 27.2 %collective-permute-start.7 = (bf16[256,2048]{1,0:T(8,128)(2,1)}, bf16[256,2048]{1,0:T(8,128)(2,1)}, u32[]{:S(2)}, u32[]{:S(2)}) collective-permute-start(bf16[256,2048]{1,0:T(8,128)(2,1)} %collective-permute-done.3.refs_1_), channel_id=1, source_target_pairs={{0,1},{1,0},{2,3},{3,2},{4,5},{5,4},{6,7},{7,6},{8,9},{9,8},{10,11... | collective-permute-start | bytes 3145736 | tf_op jit(solution)/shard_map/ppermute | solution.py:327
  167.5 5.1 %collective-permute-start.8 = (bf16[256,2048]{1,0:T(8,128)(2,1)}, bf16[256,2048]{1,0:T(8,128)(2,1)}, u32[]{:S(2)}, u32[]{:S(2)}) collective-permute-start(bf16[256,2048]{1,0:T(8,128)(2,1)} %collective-permute-done.4.refs_2_), channel_id=1, source_target_pairs={{0,1},{1,0},{2,3},{3,2},{4,5},{5,4},{6,7},{7,6},{8,9},{9,8},{10,11... | collective-permute-start | bytes 3145736 | tf_op jit(solution)/shard_map/ppermute | solution.py:327
  169.9 4.1 %collective-permute-start.9 = (bf16[256,2048]{1,0:T(8,128)(2,1)}, bf16[256,2048]{1,0:T(8,128)(2,1)}, u32[]{:S(2)}, u32[]{:S(2)}) collective-permute-start(bf16[256,2048]{1,0:T(8,128)(2,1)} %collective-permute-done.5.refs_3_), channel_id=1, source_target_pairs={{0,1},{1,0},{2,3},{3,2},{4,5},{5,4},{6,7},{7,6},{8,9},{9,8},{10,11... | collective-permute-start | bytes 3145736 | tf_op jit(solution)/shard_map/ppermute | solution.py:327

commit v7 on v6

--- a/solution.py
+++ b/solution.py
@@ -210,8 +210,8 @@
     return half * 8 + (head + 4 * half) % 8
 
 
-EARLY = ((0, 0), (1, 0), (0, 3), (0, 1), (0, 2))
-LATE = ((1, 2), (1, 3), (1, 1))
+EARLY = ((0, 0), (1, 0), (0, 3), (0, 1), (0, 2), (1, 2))
+LATE = ((1, 3), (1, 1))
 
 
 def term_sum(lane, grads_ref, pieces, steps, total):
@@ -378,7 +378,7 @@
         grid=(1,),
         in_specs=[scalars, first] + [whole] * len(EARLY),
         out_specs=whole,
-    )(place, in_hbm(grads), own, deep, own_before, own_after, own_last)
+    )(place, in_hbm(grads), own, deep, own_before, own_after, own_last, deep_last)
 
     def late(side, out_shape):
         return kernel(
@@ -388,7 +388,7 @@
             grid=(1,),
             in_specs=[scalars, first] + [whole] * (1 + len(LATE)),
             out_specs=whole,
-        )(place, in_hbm(grads), early, deep_last, deep_before, deep_after)
+        )(place, in_hbm(grads), early, deep_before, deep_after)
 
     piece = (2048 // ring // cores, 256)
     sends = []

time: 182 us -> 181 us (level)
  no operation moved by 1% of the time
where the time goes in v7:
time: 181 us; the launch traced here: 180 us
  waiting for transfers between devices  83.9 us (46%)
  starting transfers between devices  59 us (33%)
  Pallas kernels  34 us (19%)
  local copies, waits for them, and re-layouts  2.19 us (1%)
    ppermute x1, waiting for transfers between devices, shards(): lax.ppermute(far, SP, [(u, worker(1 - u % 2, u // 2)) for u in range(peer...  33.4 us
    ppermute x3, waiting for transfers between devices, shards(): weights.append(lax.ppermute(key_weight, 'dp_0', moves))  23.4 us
    all_to_all x1, waiting for transfers between devices, shards(): spread = lax.all_to_all(spread, 'lane', 0, 0, tiled=True)  11.9 us
    ppermute x1, starting transfers between devices, shards(): lax.ppermute(far, SP, [(u, worker(1 - u % 2, u // 2)) for u in range(peer...  9.4 us
    ppermute x5, starting transfers between devices, lane_step(): lax.ppermute(array, 'lane', [(i, i // 4 * 4 + (i + step) % 4) for i in ra...  9.17 us
    pallas_call x1, Pallas kernels, shards(): kernel(home_kernel, (shape((tokens, 2048), BF16), shape((tokens, 4096), B...  7.54 us
    ppermute x4, starting transfers between devices, shards(): weights += [lax.ppermute(w, 'dp_1', [(0, 1), (1, 0)]) for w in weights]  7.37 us
    all_to_all x1, starting transfers between devices, shards(): lax.all_to_all(sent, 'lane', 0, 0, tiled=True).reshape(8 * tokens, -1)  6.37 us
  transfers between devices with their start and end apart: 25, of which 12 were waited for; matrix products, arithmetic and copies ran while one was open for 0% of the time, Pallas kernels for 11%

profile of v7, /device:TPU:1, one launch (start us, length us, event | category | flops | bytes accessed | tf_op | source)
XLA Modules:
  0.0 180.0 jit_solution(3310360049613383004)
XLA Ops:
  0.6 3.0 %shard_map.102 = bf16[8,128,1536]{2,1,0:T(8,128)(2,1)} custom-call(s32[1]{0:T(128)} %bitcast.half_ref, bf16[128,2048]{1,0:T(8,128)(2,1)} %bitcast.32, bf16[128,2048]{1,0:T(8,128)(2,1)} %bitcast.33, bf16[128,4096]{1,0:T(8,128)(2,1)} %bitcast.30, bf16[128,4096]{1,0:T(8,128)(2,1)} %bitcast.31), custom_call_target="tpu_custom_call" | custom-call | flops 1048576 | bytes 6291456 | tf_op jit(solution)/shard_map/pallas_call | solution.py:193
  3.7 6.4 %all-to-all-start = ((bf16[8,128,1536]{2,1,0:T(8,128)(2,1)}), bf16[8,128,1536]{2,1,0:T(8,128)(2,1)S(1)}, u32[]{:S(2)}, u32[]{:S(2)}) async-start(bf16[8,128,1536]{2,1,0:T(8,128)(2,1)} %shard_map.102), calls=%async_computation | async-start | bytes 6291456 | tf_op jit(solution)/shard_map/all_to_all | solution.py:314
  10.1 0.7 collective-permute-start
  10.7 9.4 %collective-permute-start.1 = (f32[8,128]{1,0:T(8,128)S(1)}, f32[8,128]{1,0:T(8,128)S(1)}, u32[]{:S(2)}, u32[]{:S(2)}) collective-permute-start(f32[8,128]{1,0:T(8,128)S(1)} %get-tuple-element.27), channel_id=1, source_target_pairs={{0,96},{8,0},{16,104},{24,8},{32,112},{40,16},{48,120},{56,24},{64... | collective-permute-start | bytes 12296 | tf_op jit(solution)/shard_map/ppermute | solution.py:304
  20.2 1.3 collective-permute-start.10
  21.4 0.3 collective-permute-start.13
  21.7 33.4 %collective-permute-done.1 = f32[8,128]{1,0:T(8,128)S(1)} collective-permute-done((f32[8,128]{1,0:T(8,128)S(1)}, f32[8,128]{1,0:T(8,128)S(1)}, u32[]{:S(2)}, u32[]{:S(2)}) %collective-permute-start.1) | collective-permute-done | bytes 4128 | tf_op jit(solution)/shard_map/ppermute | solution.py:304
  55.1 0.4 shard_map.103
  55.4 2.4 %shard_map.104 = bf16[2,256,512]{2,1,0:T(8,128)(2,1)} custom-call(bf16[1024,1536]{1,0:T(8,128)(2,1)S(1)} %bitcast.26, f32[32,128]{1,0:T(8,128)S(1)} %get-tuple-element.15.factors_ref), custom_call_target="tpu_custom_call" | custom-call | flops 566231040 | bytes 4194304 | tf_op jit(solution)/shard_map/pallas_call | solution.py:336
  57.8 1.9 %collective-permute-start.2 = (bf16[2,256,512]{2,1,0:T(8,128)(2,1)}, bf16[2,256,512]{2,1,0:T(8,128)(2,1)}, u32[]{:S(2)}, u32[]{:S(2)}) collective-permute-start(bf16[2,256,512]{2,1,0:T(8,128)(2,1)} %shard_map.104), channel_id=1, source_target_pairs={{0,96},{8,104},{16,112},{24,120},{32,64},{40,72},{48,80},{56,88},{... | collective-permute-start | bytes 1572872 | tf_op jit(solution)/shard_map/ppermute | solution.py:337
  59.7 0.1 collective-permute-start.11
  59.9 3.0 %collective-permute-start.12 = (bf16[1,128,2048]{2,1,0:T(8,128)(2,1)}, bf16[1,128,2048]{2,1,0:T(8,128)(2,1)}, u32[]{:S(2)}, u32[]{:S(2)}) collective-permute-start(bf16[1,128,2048]{2,1,0:T(8,128)(2,1)} %refs_0_.3), channel_id=1, source_target_pairs={{0,24},{8,0},{16,8},{24,16},{32,56},{40,32},{48,40},{56,48},{1,25}... | collective-permute-start | bytes 1572872 | tf_op jit(solution)/shard_map/ppermute | solution.py:317
  63.0 5.7 %collective-permute-start.16 = (bf16[1,128,2048]{2,1,0:T(8,128)(2,1)}, bf16[1,128,2048]{2,1,0:T(8,128)(2,1)S(1)}, u32[]{:S(2)}, u32[]{:S(2)}) collective-permute-start(bf16[1,128,2048]{2,1,0:T(8,128)(2,1)} %collective-permute-done.10.refs_1_), channel_id=1, source_target_pairs={{0,24},{8,0},{16,8},{24,16},{32,56},{40,32},{48,40},{56,48},{1,25}... | collective-permute-start | bytes 1572872 | tf_op jit(solution)/shard_map/ppermute | solution.py:317
  68.7 1.0 collective-permute-done.2.state_ref
  69.7 1.5 collective-permute-start.14
  71.3 5.6 %shard_map.105.part_ref = bf16[1024,1024]{1,0:T(8,128)(2,1)} custom-call(bf16[1024,1536]{1,0:T(8,128)(2,1)S(1)} %bitcast.27, f32[40,128]{1,0:T(8,128)S(1)} %get-tuple-element.16.rows_ref, f32[32,128]{1,0:T(8,128)S(1)} %get-tuple-element.15.factors_ref), custom_call_target="tpu_custom_call" | custom-call | flops 3942645760 | bytes 4194304 | tf_op jit(solution)/shard_map/pallas_call | solution.py:338
  76.9 4.8 %shard_map.106.grads_ref = bf16[1024,1024]{1,0:T(8,128)(2,1)} custom-call(bf16[1024,1536]{1,0:T(8,128)(2,1)S(1)} %bitcast.28, f32[32,128]{1,0:T(8,128)S(1)} %get-tuple-element.15.factors_ref, bf16[2,256,512]{2,1,0:T(8,128)(2,1)} %collective-permute-done.2.state_ref, bf16[1024,1024]{1,0:T(8,128)(2,1)} %shard_map.105.part_ref), custom_call_target="tpu_custom_call" | custom-call | flops 838860800 | bytes 4194304 | tf_op jit(solution)/shard_map/pallas_call | solution.py:348
  81.7 3.7 %shard_map.108.early_ref = f32[2048,256]{1,0:T(8,128)S(1)} custom-call(s32[2]{0:T(128)S(1)} %pad_add_fusion.place_ref, bf16[1024,1024]{1,0:T(8,128)(2,1)} %shard_map.106.grads_ref, bf16[1,128,2048]{2,1,0:T(8,128)(2,1)} %refs_0_.3, bf16[1,128,2048]{2,1,0:T(8,128)(2,1)} %collective-permute-done.10.refs_1_, ...), custom_call_target="tpu_custom_call" | custom-call | flops 702545920 | bytes 4194304 | tf_op jit(solution)/shard_map/pallas_call | solution.py:374
  85.4 3.3 %collective-permute-done.16.refs_1_ = bf16[1,128,2048]{2,1,0:T(8,128)(2,1)S(1)} collective-permute-done((bf16[1,128,2048]{2,1,0:T(8,128)(2,1)}, bf16[1,128,2048]{2,1,0:T(8,128)(2,1)S(1)}, u32[]{:S(2)}, u32[]{:S(2)}) %collective-permute-start.16) | collective-permute-done | bytes 524320 | tf_op jit(solution)/shard_map/ppermute | solution.py:317
  88.7 2.5 %shard_map.110 = bf16[4,256,256]{2,1,0:T(8,128)(2,1)} custom-call(s32[2]{0:T(128)S(1)} %pad_add_fusion.place_ref, bf16[1024,1024]{1,0:T(8,128)(2,1)} %shard_map.106.grads_ref, f32[2048,256]{1,0:T(8,128)S(1)} %shard_map.108.early_ref, bf16[1,128,2048]{2,1,0:T(8,128)(2,1)S(1)} %collective-permute-done.15.refs_0_, ...), custom_call_target="tpu_custom_call" | custom-call | flops 209715200 | bytes 4194304 | tf_op jit(solution)/shard_map/pallas_call | solution.py:384
  91.2 1.8 %collective-permute-start.17 = (bf16[4,256,256]{2,1,0:T(8,128)(2,1)}, bf16[4,256,256]{2,1,0:T(8,128)(2,1)S(1)}, u32[]{:S(2)}, u32[]{:S(2)}) collective-permute-start(bf16[4,256,256]{2,1,0:T(8,128)(2,1)} %shard_map.110), channel_id=1, source_target_pairs={{0,1},{1,0},{2,3},{3,2},{4,5},{5,4},{6,7},{7,6},{8,9},{9,8},{10,11... | collective-permute-start | bytes 1572872 | tf_op jit(solution)/shard_map/ppermute | solution.py:397
  93.0 1.0 copy-done.1
  94.0 1.0 copy-done.3
  95.1 1.5 shard_map.109.mine_ref
  96.6 0.1 shard_map.111
  96.7 1.5 collective-permute-start.18
  98.2 2.5 %collective-permute-start.19 = (bf16[256,256]{1,0:T(8,128)(2,1)S(1)}, bf16[256,256]{1,0:T(8,128)(2,1)S(1)}, u32[]{:S(2)}, u32[]{:S(2)}) collective-permute-start(bf16[256,256]{1,0:T(8,128)(2,1)S(1)} %get-tuple-element.22), channel_id=1, source_target_pairs={{0,4},{2,6},{4,0},{6,2},{1,5},{3,7},{5,1},{7,3},{8,12},{10,14},{12... | collective-permute-start | bytes 393224 | tf_op jit(solution)/shard_map/ppermute | solution.py:409
  100.6 1.1 collective-permute-start.20
  101.8 1.4 collective-permute-done.18.refs_1_
  103.2 3.8 %collective-permute-done.19.refs_2_ = bf16[256,256]{1,0:T(8,128)(2,1)S(1)} collective-permute-done((bf16[256,256]{1,0:T(8,128)(2,1)S(1)}, bf16[256,256]{1,0:T(8,128)(2,1)S(1)}, u32[]{:S(2)}, u32[]{:S(2)}) %collective-permute-start.19) | collective-permute-done | bytes 131104 | tf_op jit(solution)/shard_map/ppermute | solution.py:409
  107.1 3.3 %collective-permute-start.21 = (bf16[256,256]{1,0:T(8,128)(2,1)S(1)}, bf16[256,256]{1,0:T(8,128)(2,1)S(1)}, u32[]{:S(2)}, u32[]{:S(2)}) collective-permute-start(bf16[256,256]{1,0:T(8,128)(2,1)S(1)} %get-tuple-element.25), channel_id=1, source_target_pairs={{0,96},{8,104},{16,112},{24,120},{32,64},{40,72},{48,80},{56,88},{... | collective-permute-start | bytes 393224 | tf_op jit(solution)/shard_map/ppermute | solution.py:413
  110.4 3.0 %collective-permute-done.21.theirs_ref = bf16[256,256]{1,0:T(8,128)(2,1)S(1)} collective-permute-done((bf16[256,256]{1,0:T(8,128)(2,1)S(1)}, bf16[256,256]{1,0:T(8,128)(2,1)S(1)}, u32[]{:S(2)}, u32[]{:S(2)}) %collective-permute-start.21) | collective-permute-done | bytes 131104 | tf_op jit(solution)/shard_map/ppermute | solution.py:413
  113.4 1.0 shard_map.113
  114.5 3.6 %all-to-all-start.2 = ((bf16[8,256,256]{2,1,0:T(8,128)(2,1)}), bf16[8,256,256]{2,1,0:T(8,128)(2,1)S(1)}, u32[]{:S(2)}, u32[]{:S(2)}) async-start(bf16[8,256,256]{2,1,0:T(8,128)(2,1)} %shard_map.113), calls=%async_computation.2 | async-start | bytes 2097152 | tf_op jit(solution)/shard_map/all_to_all | solution.py:415
  118.1 0.5 collective-permute-start.3
  118.6 2.8 %collective-permute-start.4 = (bf16[256,2048]{1,0:T(8,128)(2,1)}, bf16[256,2048]{1,0:T(8,128)(2,1)}, u32[]{:S(2)}, u32[]{:S(2)}) collective-permute-start(bf16[256,2048]{1,0:T(8,128)(2,1)} %refs_0_.2), channel_id=1, source_target_pairs={{0,4},{2,6},{4,0},{6,2},{1,5},{3,7},{5,1},{7,3},{8,12},{10,14},{12... | collective-permute-start | bytes 3145736 | tf_op jit(solution)/shard_map/ppermute | solution.py:324
  121.4 0.6 collective-permute-start.5
  122.0 11.9 %all-to-all-done.2.in_ref = bf16[8,256,256]{2,1,0:T(8,128)(2,1)S(1)} async-done(((bf16[8,256,256]{2,1,0:T(8,128)(2,1)}), bf16[8,256,256]{2,1,0:T(8,128)(2,1)S(1)}, u32[]{:S(2)}, u32[]{:S(2)}) %all-to-all-start.2) | async-done | bytes 1048608 | tf_op jit(solution)/shard_map/all_to_all | solution.py:415
  134.0 3.6 %all-to-all-start.1 = ((bf16[8,128,1024]{2,1,0:T(8,128)(2,1)}), bf16[8,128,1024]{2,1,0:T(8,128)(2,1)S(1)}, u32[]{:S(2)}, u32[]{:S(2)}) async-start(bf16[8,128,1024]{2,1,0:T(8,128)(2,1)} %bitcast.29), calls=%async_computation.1 | async-start | bytes 4194304 | tf_op jit(solution)/shard_map/all_to_all | solution.py:362
  137.6 0.9 collective-permute-start.6
  138.4 4.2 %collective-permute-done.3.refs_1_ = bf16[256,2048]{1,0:T(8,128)(2,1)} collective-permute-done((bf16[256,2048]{1,0:T(8,128)(2,1)}, bf16[256,2048]{1,0:T(8,128)(2,1)}, u32[]{:S(2)}, u32[]{:S(2)}) %collective-permute-start.3) | collective-permute-done | bytes 1048608 | tf_op jit(solution)/shard_map/ppermute | solution.py:324
  142.7 4.0 %collective-permute-start.7 = (bf16[256,2048]{1,0:T(8,128)(2,1)}, bf16[256,2048]{1,0:T(8,128)(2,1)}, u32[]{:S(2)}, u32[]{:S(2)}) collective-permute-start(bf16[256,2048]{1,0:T(8,128)(2,1)} %collective-permute-done.3.refs_1_), channel_id=1, source_target_pairs={{0,1},{1,0},{2,3},{3,2},{4,5},{5,4},{6,7},{7,6},{8,9},{9,8},{10,11... | collective-permute-start | bytes 3145736 | tf_op jit(solution)/shard_map/ppermute | solution.py:327
  146.7 19.1 %collective-permute-done.4.refs_2_ = bf16[256,2048]{1,0:T(8,128)(2,1)} collective-permute-done((bf16[256,2048]{1,0:T(8,128)(2,1)}, bf16[256,2048]{1,0:T(8,128)(2,1)}, u32[]{:S(2)}, u32[]{:S(2)}) %collective-permute-start.4) | collective-permute-done | bytes 1048608 | tf_op jit(solution)/shard_map/ppermute | solution.py:324
  165.8 2.5 %collective-permute-start.8 = (bf16[256,2048]{1,0:T(8,128)(2,1)}, bf16[256,2048]{1,0:T(8,128)(2,1)}, u32[]{:S(2)}, u32[]{:S(2)}) collective-permute-start(bf16[256,2048]{1,0:T(8,128)(2,1)} %collective-permute-done.4.refs_2_), channel_id=1, source_target_pairs={{0,1},{1,0},{2,3},{3,2},{4,5},{5,4},{6,7},{7,6},{8,9},{9,8},{10,11... | collective-permute-start | bytes 3145736 | tf_op jit(solution)/shard_map/ppermute | solution.py:327
  168.4 1.5 shard_map.114
  169.9 1.1 collective-permute-done.8.refs_6_
  170.9 1.5 collective-permute-done.9.refs_7_
  172.4 7.5 %shard_map.107 = (bf16[128,2048]{1,0:T(8,128)(2,1)}, bf16[128,4096]{1,0:T(8,128)(2,1)}, bf16[128,2048]{1,0:T(8,128)(2,1)}) custom-call(s32[1]{0:T(128)} %bitcast.half_ref, s32[8]{0:T(128)S(1)} %stack.44.owner_ref, bf16[8,128,1024]{2,1,0:T(8,128)(2,1)S(1)} %all-to-all-done.1.home_ref, bf16[256,2048]{1,0:T(8,128)(2,1)} %refs_0_.2, ...), custom_call_target="tpu_custom_call" | custom-call | flops 1121976320 | bytes 4194304 | tf_op jit(solution)/shard_map/pallas_call | solution.py:363
  (30 shorter events, 0.4 us)
Async XLA Ops:
  3.7 6.4 %copy-start.4 = (f32[1,1,2048]{2,1,0:T(1,128)S(1)}, f32[1,1,2048]{2,1,0:T(1,128)}, u32[]{:S(2)}) copy-start(f32[1,1,2048]{2,1,0:T(1,128)} %param.12) | copy-start | bytes 24580
  3.7 51.8 %all-to-all-start = ((bf16[8,128,1536]{2,1,0:T(8,128)(2,1)}), bf16[8,128,1536]{2,1,0:T(8,128)(2,1)S(1)}, u32[]{:S(2)}, u32[]{:S(2)}) async-start(bf16[8,128,1536]{2,1,0:T(8,128)(2,1)} %shard_map.102), calls=%async_computation | async-start | bytes 6291456 | tf_op jit(solution)/shard_map/all_to_all | solution.py:314
  10.1 11.6 %collective-permute-start = (f32[8,128]{1,0:T(8,128)S(1)}, f32[8,128]{1,0:T(8,128)S(1)}, u32[]{:S(2)}, u32[]{:S(2)}) collective-permute-start(f32[8,128]{1,0:T(8,128)S(1)} %get-tuple-element.26), channel_id=1, source_target_pairs={{0,0},{8,96},{16,8},{24,104},{32,16},{40,112},{48,24},{56,120},{64... | collective-permute-start | bytes 12296 | tf_op jit(solution)/shard_map/ppermute | solution.py:303
  10.7 44.3 %collective-permute-start.1 = (f32[8,128]{1,0:T(8,128)S(1)}, f32[8,128]{1,0:T(8,128)S(1)}, u32[]{:S(2)}, u32[]{:S(2)}) collective-permute-start(f32[8,128]{1,0:T(8,128)S(1)} %get-tuple-element.27), channel_id=1, source_target_pairs={{0,96},{8,0},{16,104},{24,8},{32,112},{40,16},{48,120},{56,24},{64... | collective-permute-start | bytes 12296 | tf_op jit(solution)/shard_map/ppermute | solution.py:304
  20.2 42.7 %collective-permute-start.10 = (bf16[1,128,2048]{2,1,0:T(8,128)(2,1)}, bf16[1,128,2048]{2,1,0:T(8,128)(2,1)}, u32[]{:S(2)}, u32[]{:S(2)}) collective-permute-start(bf16[1,128,2048]{2,1,0:T(8,128)(2,1)} %refs_0_.3), channel_id=1, source_target_pairs={{0,32},{8,40},{16,48},{24,56},{32,0},{40,8},{48,16},{56,24},{1,33}... | collective-permute-start | bytes 1572872 | tf_op jit(solution)/shard_map/ppermute | solution.py:305
  21.4 41.6 %collective-permute-start.13 = (bf16[1,128,2048]{2,1,0:T(8,128)(2,1)}, bf16[1,128,2048]{2,1,0:T(8,128)(2,1)}, u32[]{:S(2)}, u32[]{:S(2)}) collective-permute-start(bf16[1,128,2048]{2,1,0:T(8,128)(2,1)} %refs_0_.3), channel_id=1, source_target_pairs={{0,16},{8,24},{16,0},{24,8},{32,48},{40,56},{48,32},{56,40},{1,17}... | collective-permute-start | bytes 1572872 | tf_op jit(solution)/shard_map/ppermute | solution.py:317
  57.8 11.9 %collective-permute-start.2 = (bf16[2,256,512]{2,1,0:T(8,128)(2,1)}, bf16[2,256,512]{2,1,0:T(8,128)(2,1)}, u32[]{:S(2)}, u32[]{:S(2)}) collective-permute-start(bf16[2,256,512]{2,1,0:T(8,128)(2,1)} %shard_map.104), channel_id=1, source_target_pairs={{0,96},{8,104},{16,112},{24,120},{32,64},{40,72},{48,80},{56,88},{... | collective-permute-start | bytes 1572872 | tf_op jit(solution)/shard_map/ppermute | solution.py:337
  59.7 22.0 %collective-permute-start.11 = (bf16[1,128,2048]{2,1,0:T(8,128)(2,1)}, bf16[1,128,2048]{2,1,0:T(8,128)(2,1)}, u32[]{:S(2)}, u32[]{:S(2)}) collective-permute-start(bf16[1,128,2048]{2,1,0:T(8,128)(2,1)} %refs_0_.3), channel_id=1, source_target_pairs={{0,8},{8,16},{16,24},{24,0},{32,40},{40,48},{48,56},{56,32},{1,9},... | collective-permute-start | bytes 1572872 | tf_op jit(solution)/shard_map/ppermute | solution.py:317
  59.9 21.8 %collective-permute-start.12 = (bf16[1,128,2048]{2,1,0:T(8,128)(2,1)}, bf16[1,128,2048]{2,1,0:T(8,128)(2,1)}, u32[]{:S(2)}, u32[]{:S(2)}) collective-permute-start(bf16[1,128,2048]{2,1,0:T(8,128)(2,1)} %refs_0_.3), channel_id=1, source_target_pairs={{0,24},{8,0},{16,8},{24,16},{32,56},{40,32},{48,40},{56,48},{1,25}... | collective-permute-start | bytes 1572872 | tf_op jit(solution)/shard_map/ppermute | solution.py:317
  62.9 22.5 %collective-permute-start.15 = (bf16[1,128,2048]{2,1,0:T(8,128)(2,1)}, bf16[1,128,2048]{2,1,0:T(8,128)(2,1)S(1)}, u32[]{:S(2)}, u32[]{:S(2)}) collective-permute-start(bf16[1,128,2048]{2,1,0:T(8,128)(2,1)} %collective-permute-done.10.refs_1_), channel_id=1, source_target_pairs={{0,8},{8,16},{16,24},{24,0},{32,40},{40,48},{48,56},{56,32},{1,9},... | collective-permute-start | bytes 1572872 | tf_op jit(solution)/shard_map/ppermute | solution.py:317
  63.0 25.7 %collective-permute-start.16 = (bf16[1,128,2048]{2,1,0:T(8,128)(2,1)}, bf16[1,128,2048]{2,1,0:T(8,128)(2,1)S(1)}, u32[]{:S(2)}, u32[]{:S(2)}) collective-permute-start(bf16[1,128,2048]{2,1,0:T(8,128)(2,1)} %collective-permute-done.10.refs_1_), channel_id=1, source_target_pairs={{0,24},{8,0},{16,8},{24,16},{32,56},{40,32},{48,40},{56,48},{1,25}... | collective-permute-start | bytes 1572872 | tf_op jit(solution)/shard_map/ppermute | solution.py:317
  69.7 12.0 %collective-permute-start.14 = (bf16[1,128,2048]{2,1,0:T(8,128)(2,1)}, bf16[1,128,2048]{2,1,0:T(8,128)(2,1)S(1)}, u32[]{:S(2)}, u32[]{:S(2)}) collective-permute-start(bf16[1,128,2048]{2,1,0:T(8,128)(2,1)} %collective-permute-done.13.refs_4_), channel_id=1, source_target_pairs={{0,32},{8,40},{16,48},{24,56},{32,0},{40,8},{48,16},{56,24},{1,33}... | collective-permute-start | bytes 1572872 | tf_op jit(solution)/shard_map/ppermute | solution.py:334
  85.4 5.8 %copy-start = (bf16[1,128,2048]{2,1,0:T(8,128)(2,1)}, bf16[1,128,2048]{2,1,0:T(8,128)(2,1)S(1)}, u32[]{:S(2)}) copy-start(bf16[1,128,2048]{2,1,0:T(8,128)(2,1)S(1)} %collective-permute-done.15.refs_0_) | copy-start | bytes 1572868
  88.7 2.5 %copy-start.2 = (bf16[1,128,2048]{2,1,0:T(8,128)(2,1)}, bf16[1,128,2048]{2,1,0:T(8,128)(2,1)S(1)}, u32[]{:S(2)}) copy-start(bf16[1,128,2048]{2,1,0:T(8,128)(2,1)S(1)} %collective-permute-done.16.refs_1_) | copy-start | bytes 1572868
  91.2 5.4 %collective-permute-start.17 = (bf16[4,256,256]{2,1,0:T(8,128)(2,1)}, bf16[4,256,256]{2,1,0:T(8,128)(2,1)S(1)}, u32[]{:S(2)}, u32[]{:S(2)}) collective-permute-start(bf16[4,256,256]{2,1,0:T(8,128)(2,1)} %shard_map.110), channel_id=1, source_target_pairs={{0,1},{1,0},{2,3},{3,2},{4,5},{5,4},{6,7},{7,6},{8,9},{9,8},{10,11... | collective-permute-start | bytes 1572872 | tf_op jit(solution)/shard_map/ppermute | solution.py:397
  93.0 1.0 copy-start.1
  94.0 1.0 copy-start.3
  96.7 6.5 %collective-permute-start.18 = (bf16[256,256]{1,0:T(8,128)(2,1)S(1)}, bf16[256,256]{1,0:T(8,128)(2,1)S(1)}, u32[]{:S(2)}, u32[]{:S(2)}) collective-permute-start(bf16[256,256]{1,0:T(8,128)(2,1)S(1)} %get-tuple-element.21), channel_id=1, source_target_pairs={{0,2},{2,4},{4,6},{6,0},{1,3},{3,5},{5,7},{7,1},{8,10},{10,12},{12... | collective-permute-start | bytes 393224 | tf_op jit(solution)/shard_map/ppermute | solution.py:409
  98.2 8.8 %collective-permute-start.19 = (bf16[256,256]{1,0:T(8,128)(2,1)S(1)}, bf16[256,256]{1,0:T(8,128)(2,1)S(1)}, u32[]{:S(2)}, u32[]{:S(2)}) collective-permute-start(bf16[256,256]{1,0:T(8,128)(2,1)S(1)} %get-tuple-element.22), channel_id=1, source_target_pairs={{0,4},{2,6},{4,0},{6,2},{1,5},{3,7},{5,1},{7,3},{8,12},{10,14},{12... | collective-permute-start | bytes 393224 | tf_op jit(solution)/shard_map/ppermute | solution.py:409
  100.6 6.4 %collective-permute-start.20 = (bf16[256,256]{1,0:T(8,128)(2,1)S(1)}, bf16[256,256]{1,0:T(8,128)(2,1)S(1)}, u32[]{:S(2)}, u32[]{:S(2)}) collective-permute-start(bf16[256,256]{1,0:T(8,128)(2,1)S(1)} %get-tuple-element.23), channel_id=1, source_target_pairs={{0,6},{2,0},{4,2},{6,4},{1,7},{3,1},{5,3},{7,5},{8,14},{10,8},{12,... | collective-permute-start | bytes 393224 | tf_op jit(solution)/shard_map/ppermute | solution.py:409
  107.1 6.3 %collective-permute-start.21 = (bf16[256,256]{1,0:T(8,128)(2,1)S(1)}, bf16[256,256]{1,0:T(8,128)(2,1)S(1)}, u32[]{:S(2)}, u32[]{:S(2)}) collective-permute-start(bf16[256,256]{1,0:T(8,128)(2,1)S(1)} %get-tuple-element.25), channel_id=1, source_target_pairs={{0,96},{8,104},{16,112},{24,120},{32,64},{40,72},{48,80},{56,88},{... | collective-permute-start | bytes 393224 | tf_op jit(solution)/shard_map/ppermute | solution.py:413
  114.5 19.5 %all-to-all-start.2 = ((bf16[8,256,256]{2,1,0:T(8,128)(2,1)}), bf16[8,256,256]{2,1,0:T(8,128)(2,1)S(1)}, u32[]{:S(2)}, u32[]{:S(2)}) async-start(bf16[8,256,256]{2,1,0:T(8,128)(2,1)} %shard_map.113), calls=%async_computation.2 | async-start | bytes 2097152 | tf_op jit(solution)/shard_map/all_to_all | solution.py:415
  118.1 24.6 %collective-permute-start.3 = (bf16[256,2048]{1,0:T(8,128)(2,1)}, bf16[256,2048]{1,0:T(8,128)(2,1)}, u32[]{:S(2)}, u32[]{:S(2)}) collective-permute-start(bf16[256,2048]{1,0:T(8,128)(2,1)} %refs_0_.2), channel_id=1, source_target_pairs={{0,2},{2,4},{4,6},{6,0},{1,3},{3,5},{5,7},{7,1},{8,10},{10,12},{12... | collective-permute-start | bytes 3145736 | tf_op jit(solution)/shard_map/ppermute | solution.py:324
  118.6 47.2 %collective-permute-start.4 = (bf16[256,2048]{1,0:T(8,128)(2,1)}, bf16[256,2048]{1,0:T(8,128)(2,1)}, u32[]{:S(2)}, u32[]{:S(2)}) collective-permute-start(bf16[256,2048]{1,0:T(8,128)(2,1)} %refs_0_.2), channel_id=1, source_target_pairs={{0,4},{2,6},{4,0},{6,2},{1,5},{3,7},{5,1},{7,3},{8,12},{10,14},{12... | collective-permute-start | bytes 3145736 | tf_op jit(solution)/shard_map/ppermute | solution.py:324
  121.4 46.9 %collective-permute-start.5 = (bf16[256,2048]{1,0:T(8,128)(2,1)}, bf16[256,2048]{1,0:T(8,128)(2,1)}, u32[]{:S(2)}, u32[]{:S(2)}) collective-permute-start(bf16[256,2048]{1,0:T(8,128)(2,1)} %refs_0_.2), channel_id=1, source_target_pairs={{0,6},{2,0},{4,2},{6,4},{1,7},{3,1},{5,3},{7,5},{8,14},{10,8},{12,... | collective-permute-start | bytes 3145736 | tf_op jit(solution)/shard_map/ppermute | solution.py:324
  134.0 38.5 %all-to-all-start.1 = ((bf16[8,128,1024]{2,1,0:T(8,128)(2,1)}), bf16[8,128,1024]{2,1,0:T(8,128)(2,1)S(1)}, u32[]{:S(2)}, u32[]{:S(2)}) async-start(bf16[8,128,1024]{2,1,0:T(8,128)(2,1)} %bitcast.29), calls=%async_computation.1 | async-start | bytes 4194304 | tf_op jit(solution)/shard_map/all_to_all | solution.py:362
  137.6 32.3 %collective-permute-start.6 = (bf16[256,2048]{1,0:T(8,128)(2,1)}, bf16[256,2048]{1,0:T(8,128)(2,1)}, u32[]{:S(2)}, u32[]{:S(2)}) collective-permute-start(bf16[256,2048]{1,0:T(8,128)(2,1)} %refs_0_.2), channel_id=1, source_target_pairs={{0,1},{1,0},{2,3},{3,2},{4,5},{5,4},{6,7},{7,6},{8,9},{9,8},{10,11... | collective-permute-start | bytes 3145736 | tf_op jit(solution)/shard_map/ppermute | solution.py:327
  142.7 27.2 %collective-permute-start.7 = (bf16[256,2048]{1,0:T(8,128)(2,1)}, bf16[256,2048]{1,0:T(8,128)(2,1)}, u32[]{:S(2)}, u32[]{:S(2)}) collective-permute-start(bf16[256,2048]{1,0:T(8,128)(2,1)} %collective-permute-done.3.refs_1_), channel_id=1, source_target_pairs={{0,1},{1,0},{2,3},{3,2},{4,5},{5,4},{6,7},{7,6},{8,9},{9,8},{10,11... | collective-permute-start | bytes 3145736 | tf_op jit(solution)/shard_map/ppermute | solution.py:327
  165.8 5.1 %collective-permute-start.8 = (bf16[256,2048]{1,0:T(8,128)(2,1)}, bf16[256,2048]{1,0:T(8,128)(2,1)}, u32[]{:S(2)}, u32[]{:S(2)}) collective-permute-start(bf16[256,2048]{1,0:T(8,128)(2,1)} %collective-permute-done.4.refs_2_), channel_id=1, source_target_pairs={{0,1},{1,0},{2,3},{3,2},{4,5},{5,4},{6,7},{7,6},{8,9},{9,8},{10,11... | collective-permute-start | bytes 3145736 | tf_op jit(solution)/shard_map/ppermute | solution.py:327
  168.3 4.1 %collective-permute-start.9 = (bf16[256,2048]{1,0:T(8,128)(2,1)}, bf16[256,2048]{1,0:T(8,128)(2,1)}, u32[]{:S(2)}, u32[]{:S(2)}) collective-permute-start(bf16[256,2048]{1,0:T(8,128)(2,1)} %collective-permute-done.5.refs_3_), channel_id=1, source_target_pairs={{0,1},{1,0},{2,3},{3,2},{4,5},{5,4},{6,7},{7,6},{8,9},{9,8},{10,11... | collective-permute-start | bytes 3145736 | tf_op jit(solution)/shard_map/ppermute | solution.py:327

commit v8 on v7

--- a/solution.py
+++ b/solution.py
@@ -225,19 +225,19 @@
 
 
 def early_kernel(place_ref, grads_ref, *refs):
-    refs[-1][...] = term_sum(place_ref[0], grads_ref, refs[:-1], EARLY, None)
+    pieces, out_ref, late_ref = refs[:-2], refs[-2], refs[-1]
+    lane = place_ref[0]
+    for k, (other, step) in enumerate(LATE):
+        block = (lane // 4 ^ other) * 4 + (lane % 4 + step) % 4
+        late_ref[k] = grads_ref[pl.ds(pl.multiple_of(block * BLOCK, BLOCK), BLOCK), :]
+    out_ref[...] = term_sum(lane, grads_ref, pieces, EARLY, None)
 
 
 def late_kernel(side, place_ref, grads_ref, early_ref, *refs):
     pieces, out_ref = refs[:-1], refs[-1]
     ring, span, _ = out_ref.shape
     cores = early_ref.shape[0] // (ring * span)
-    lane = place_ref[0]
-    deep, y = lane // 4, lane % 4
-    grads = []
-    for other, step in LATE:
-        block = (deep ^ other) * 4 + (y + step) % 4
-        grads.append(grads_ref[pl.ds(pl.multiple_of(block * BLOCK, BLOCK), BLOCK), :])
+    grads = [grads_ref[k] for k in range(len(LATE))]
     for k in range(ring):
         owner = cores * k + (place_ref[1] if side == 0 else 1 - place_ref[1])
         at = pl.multiple_of(owner * span, span)
@@ -371,13 +371,13 @@
 
     place = jnp.stack([lane, core])
     first = pl.BlockSpec((1024, 256), lambda i: (0, 0))
-    early = kernel(
+    early, late_grads = kernel(
         early_kernel,
-        shape((2048, 256), F32),
+        (shape((2048, 256), F32), shape((len(LATE), BLOCK, 256), BF16)),
         670 << 20,
         grid=(1,),
         in_specs=[scalars, first] + [whole] * len(EARLY),
-        out_specs=whole,
+        out_specs=(whole, whole),
     )(place, in_hbm(grads), own, deep, own_before, own_after, own_last, deep_last)
 
     def late(side, out_shape):
@@ -386,9 +386,9 @@
             out_shape,
             200 << 20,
             grid=(1,),
-            in_specs=[scalars, first] + [whole] * (1 + len(LATE)),
+            in_specs=[scalars] + [whole] * (2 + len(LATE)),
             out_specs=whole,
-        )(place, in_hbm(grads), early, deep_before, deep_after)
+        )(place, late_grads, early, deep_before, deep_after)
 
     piece = (2048 // ring // cores, 256)
     sends = []

time: 181 us -> 180 us (level)
  no operation moved by 1% of the time
where the time goes in v8:
time: 180 us
  waiting for transfers between devices  83.9 us (47%)
  starting transfers between devices  59 us (33%)
  Pallas kernels  32.9 us (18%)
  local copies, waits for them, and re-layouts  2.98 us (2%)
    ppermute x1, waiting for transfers between devices, shards(): lax.ppermute(far, SP, [(u, worker(1 - u % 2, u // 2)) for u in range(peer...  33.4 us
    ppermute x3, waiting for transfers between devices, shards(): weights.append(lax.ppermute(key_weight, 'dp_0', moves))  23.4 us
    all_to_all x1, waiting for transfers between devices, shards(): spread = lax.all_to_all(spread, 'lane', 0, 0, tiled=True)  11.9 us
    ppermute x1, starting transfers between devices, shards(): lax.ppermute(far, SP, [(u, worker(1 - u % 2, u // 2)) for u in range(peer...  9.4 us
    ppermute x5, starting transfers between devices, lane_step(): lax.ppermute(array, 'lane', [(i, i // 4 * 4 + (i + step) % 4) for i in ra...  9.17 us
    pallas_call x1, Pallas kernels, shards(): kernel(home_kernel, (shape((tokens, 2048), BF16), shape((tokens, 4096), B...  7.54 us
    ppermute x4, starting transfers between devices, shards(): weights += [lax.ppermute(w, 'dp_1', [(0, 1), (1, 0)]) for w in weights]  7.34 us
    all_to_all x1, starting transfers between devices, shards(): lax.all_to_all(sent, 'lane', 0, 0, tiled=True).reshape(8 * tokens, -1)  6.37 us
  transfers between devices with their start and end apart: 25, of which 12 were waited for; matrix products, arithmetic and copies ran while one was open for 0% of the time, Pallas kernels for 11%

profile of v8, /device:TPU:1, one launch (start us, length us, event | category | flops | bytes accessed | tf_op | source)
XLA Modules:
  0.0 179.6 jit_solution(4089803237714344102)
XLA Ops:
  0.6 3.0 %shard_map.102 = bf16[8,128,1536]{2,1,0:T(8,128)(2,1)} custom-call(s32[1]{0:T(128)} %bitcast.half_ref, bf16[128,2048]{1,0:T(8,128)(2,1)} %bitcast.32, bf16[128,2048]{1,0:T(8,128)(2,1)} %bitcast.33, bf16[128,4096]{1,0:T(8,128)(2,1)} %bitcast.30, bf16[128,4096]{1,0:T(8,128)(2,1)} %bitcast.31), custom_call_target="tpu_custom_call" | custom-call | flops 1048576 | bytes 6291456 | tf_op jit(solution)/shard_map/pallas_call | solution.py:193
  3.7 6.4 %all-to-all-start = ((bf16[8,128,1536]{2,1,0:T(8,128)(2,1)}), bf16[8,128,1536]{2,1,0:T(8,128)(2,1)S(1)}, u32[]{:S(2)}, u32[]{:S(2)}) async-start(bf16[8,128,1536]{2,1,0:T(8,128)(2,1)} %shard_map.102), calls=%async_computation | async-start | bytes 6291456 | tf_op jit(solution)/shard_map/all_to_all | solution.py:314
  10.1 0.7 collective-permute-start
  10.8 9.4 %collective-permute-start.1 = (f32[8,128]{1,0:T(8,128)S(1)}, f32[8,128]{1,0:T(8,128)S(1)}, u32[]{:S(2)}, u32[]{:S(2)}) collective-permute-start(f32[8,128]{1,0:T(8,128)S(1)} %get-tuple-element.31), channel_id=1, source_target_pairs={{0,96},{8,0},{16,104},{24,8},{32,112},{40,16},{48,120},{56,24},{64... | collective-permute-start | bytes 12296 | tf_op jit(solution)/shard_map/ppermute | solution.py:304
  20.2 1.3 collective-permute-start.10
  21.4 0.3 collective-permute-start.13
  21.7 33.4 %collective-permute-done.1 = f32[8,128]{1,0:T(8,128)S(1)} collective-permute-done((f32[8,128]{1,0:T(8,128)S(1)}, f32[8,128]{1,0:T(8,128)S(1)}, u32[]{:S(2)}, u32[]{:S(2)}) %collective-permute-start.1) | collective-permute-done | bytes 4128 | tf_op jit(solution)/shard_map/ppermute | solution.py:304
  55.1 0.4 shard_map.103
  55.5 2.4 %shard_map.104 = bf16[2,256,512]{2,1,0:T(8,128)(2,1)} custom-call(bf16[1024,1536]{1,0:T(8,128)(2,1)S(1)} %bitcast.26, f32[32,128]{1,0:T(8,128)S(1)} %get-tuple-element.17.factors_ref), custom_call_target="tpu_custom_call" | custom-call | flops 566231040 | bytes 4194304 | tf_op jit(solution)/shard_map/pallas_call | solution.py:336
  57.8 1.9 %collective-permute-start.2 = (bf16[2,256,512]{2,1,0:T(8,128)(2,1)}, bf16[2,256,512]{2,1,0:T(8,128)(2,1)}, u32[]{:S(2)}, u32[]{:S(2)}) collective-permute-start(bf16[2,256,512]{2,1,0:T(8,128)(2,1)} %shard_map.104), channel_id=1, source_target_pairs={{0,96},{8,104},{16,112},{24,120},{32,64},{40,72},{48,80},{56,88},{... | collective-permute-start | bytes 1572872 | tf_op jit(solution)/shard_map/ppermute | solution.py:337
  59.7 0.1 collective-permute-start.11
  59.9 3.0 %collective-permute-start.12 = (bf16[1,128,2048]{2,1,0:T(8,128)(2,1)}, bf16[1,128,2048]{2,1,0:T(8,128)(2,1)}, u32[]{:S(2)}, u32[]{:S(2)}) collective-permute-start(bf16[1,128,2048]{2,1,0:T(8,128)(2,1)} %refs_0_.3), channel_id=1, source_target_pairs={{0,24},{8,0},{16,8},{24,16},{32,56},{40,32},{48,40},{56,48},{1,25}... | collective-permute-start | bytes 1572872 | tf_op jit(solution)/shard_map/ppermute | solution.py:317
  63.0 5.7 %collective-permute-start.16 = (bf16[1,128,2048]{2,1,0:T(8,128)(2,1)}, bf16[1,128,2048]{2,1,0:T(8,128)(2,1)S(1)}, u32[]{:S(2)}, u32[]{:S(2)}) collective-permute-start(bf16[1,128,2048]{2,1,0:T(8,128)(2,1)} %collective-permute-done.10.refs_1_), channel_id=1, source_target_pairs={{0,24},{8,0},{16,8},{24,16},{32,56},{40,32},{48,40},{56,48},{1,25}... | collective-permute-start | bytes 1572872 | tf_op jit(solution)/shard_map/ppermute | solution.py:317
  68.7 1.0 collective-permute-done.2.state_ref
  69.7 1.5 collective-permute-start.14
  71.3 5.6 %shard_map.105.part_ref = bf16[1024,1024]{1,0:T(8,128)(2,1)} custom-call(bf16[1024,1536]{1,0:T(8,128)(2,1)S(1)} %bitcast.27, f32[40,128]{1,0:T(8,128)S(1)} %get-tuple-element.18.rows_ref, f32[32,128]{1,0:T(8,128)S(1)} %get-tuple-element.17.factors_ref), custom_call_target="tpu_custom_call" | custom-call | flops 3942645760 | bytes 4194304 | tf_op jit(solution)/shard_map/pallas_call | solution.py:338
  77.0 4.8 %shard_map.106.grads_ref = bf16[1024,1024]{1,0:T(8,128)(2,1)} custom-call(bf16[1024,1536]{1,0:T(8,128)(2,1)S(1)} %bitcast.28, f32[32,128]{1,0:T(8,128)S(1)} %get-tuple-element.17.factors_ref, bf16[2,256,512]{2,1,0:T(8,128)(2,1)} %collective-permute-done.2.state_ref, bf16[1024,1024]{1,0:T(8,128)(2,1)} %shard_map.105.part_ref), custom_call_target="tpu_custom_call" | custom-call | flops 838860800 | bytes 4194304 | tf_op jit(solution)/shard_map/pallas_call | solution.py:348
  81.8 3.7 %shard_map.108 = (f32[2048,256]{1,0:T(8,128)S(1)}, bf16[2,128,256]{2,1,0:T(8,128)(2,1)S(1)}) custom-call(s32[2]{0:T(128)S(1)} %pad_add_fusion.place_ref, bf16[1024,1024]{1,0:T(8,128)(2,1)} %shard_map.106.grads_ref, bf16[1,128,2048]{2,1,0:T(8,128)(2,1)} %refs_0_.3, bf16[1,128,2048]{2,1,0:T(8,128)(2,1)} %collective-permute-done.10.refs_1_, ...), custom_call_target="tpu_custom_call" | custom-call | flops 702545920 | bytes 4194304 | tf_op jit(solution)/shard_map/pallas_call | solution.py:374
  85.5 3.2 %collective-permute-done.16.refs_1_ = bf16[1,128,2048]{2,1,0:T(8,128)(2,1)S(1)} collective-permute-done((bf16[1,128,2048]{2,1,0:T(8,128)(2,1)}, bf16[1,128,2048]{2,1,0:T(8,128)(2,1)S(1)}, u32[]{:S(2)}, u32[]{:S(2)}) %collective-permute-start.16) | collective-permute-done | bytes 524320 | tf_op jit(solution)/shard_map/ppermute | solution.py:317
  88.7 1.8 %shard_map.110 = bf16[4,256,256]{2,1,0:T(8,128)(2,1)} custom-call(s32[2]{0:T(128)S(1)} %pad_add_fusion.place_ref, bf16[2,128,256]{2,1,0:T(8,128)(2,1)S(1)} %get-tuple-element.22.grads_ref, f32[2048,256]{1,0:T(8,128)S(1)} %get-tuple-element.23.early_ref, bf16[1,128,2048]{2,1,0:T(8,128)(2,1)S(1)} %collective-permute-done.15.refs_0_, ...), custom_call_target="tpu_custom_call" | custom-call | flops 209715200 | bytes 4194304 | tf_op jit(solution)/shard_map/pallas_call | solution.py:384
  90.5 0.8 copy-done
  91.3 1.8 %collective-permute-start.17 = (bf16[4,256,256]{2,1,0:T(8,128)(2,1)}, bf16[4,256,256]{2,1,0:T(8,128)(2,1)S(1)}, u32[]{:S(2)}, u32[]{:S(2)}) collective-permute-start(bf16[4,256,256]{2,1,0:T(8,128)(2,1)} %shard_map.110), channel_id=1, source_target_pairs={{0,1},{1,0},{2,3},{3,2},{4,5},{5,4},{6,7},{7,6},{8,9},{9,8},{10,11... | collective-permute-start | bytes 1572872 | tf_op jit(solution)/shard_map/ppermute | solution.py:397
  93.1 1.0 copy-done.1
  94.2 1.0 copy-done.3
  95.2 1.0 shard_map.109.mine_ref
  96.3 1.5 collective-permute-start.18
  97.8 2.5 %collective-permute-start.19 = (bf16[256,256]{1,0:T(8,128)(2,1)S(1)}, bf16[256,256]{1,0:T(8,128)(2,1)S(1)}, u32[]{:S(2)}, u32[]{:S(2)}) collective-permute-start(bf16[256,256]{1,0:T(8,128)(2,1)S(1)} %get-tuple-element.26), channel_id=1, source_target_pairs={{0,4},{2,6},{4,0},{6,2},{1,5},{3,7},{5,1},{7,3},{8,12},{10,14},{12... | collective-permute-start | bytes 393224 | tf_op jit(solution)/shard_map/ppermute | solution.py:409
  100.2 1.1 collective-permute-start.20
  101.4 1.5 collective-permute-done.18.refs_1_
  102.8 3.8 %collective-permute-done.19.refs_2_ = bf16[256,256]{1,0:T(8,128)(2,1)S(1)} collective-permute-done((bf16[256,256]{1,0:T(8,128)(2,1)S(1)}, bf16[256,256]{1,0:T(8,128)(2,1)S(1)}, u32[]{:S(2)}, u32[]{:S(2)}) %collective-permute-start.19) | collective-permute-done | bytes 131104 | tf_op jit(solution)/shard_map/ppermute | solution.py:409
  106.7 3.3 %collective-permute-start.21 = (bf16[256,256]{1,0:T(8,128)(2,1)S(1)}, bf16[256,256]{1,0:T(8,128)(2,1)S(1)}, u32[]{:S(2)}, u32[]{:S(2)}) collective-permute-start(bf16[256,256]{1,0:T(8,128)(2,1)S(1)} %get-tuple-element.29), channel_id=1, source_target_pairs={{0,96},{8,104},{16,112},{24,120},{32,64},{40,72},{48,80},{56,88},{... | collective-permute-start | bytes 393224 | tf_op jit(solution)/shard_map/ppermute | solution.py:413
  110.0 3.0 %collective-permute-done.21.theirs_ref = bf16[256,256]{1,0:T(8,128)(2,1)S(1)} collective-permute-done((bf16[256,256]{1,0:T(8,128)(2,1)S(1)}, bf16[256,256]{1,0:T(8,128)(2,1)S(1)}, u32[]{:S(2)}, u32[]{:S(2)}) %collective-permute-start.21) | collective-permute-done | bytes 131104 | tf_op jit(solution)/shard_map/ppermute | solution.py:413
  113.0 1.0 shard_map.113
  114.1 3.6 %all-to-all-start.2 = ((bf16[8,256,256]{2,1,0:T(8,128)(2,1)}), bf16[8,256,256]{2,1,0:T(8,128)(2,1)S(1)}, u32[]{:S(2)}, u32[]{:S(2)}) async-start(bf16[8,256,256]{2,1,0:T(8,128)(2,1)} %shard_map.113), calls=%async_computation.2 | async-start | bytes 2097152 | tf_op jit(solution)/shard_map/all_to_all | solution.py:415
  117.7 0.5 collective-permute-start.3
  118.2 2.8 %collective-permute-start.4 = (bf16[256,2048]{1,0:T(8,128)(2,1)}, bf16[256,2048]{1,0:T(8,128)(2,1)}, u32[]{:S(2)}, u32[]{:S(2)}) collective-permute-start(bf16[256,2048]{1,0:T(8,128)(2,1)} %refs_0_.2), channel_id=1, source_target_pairs={{0,4},{2,6},{4,0},{6,2},{1,5},{3,7},{5,1},{7,3},{8,12},{10,14},{12... | collective-permute-start | bytes 3145736 | tf_op jit(solution)/shard_map/ppermute | solution.py:324
  121.0 0.6 collective-permute-start.5
  121.6 11.9 %all-to-all-done.2.in_ref = bf16[8,256,256]{2,1,0:T(8,128)(2,1)S(1)} async-done(((bf16[8,256,256]{2,1,0:T(8,128)(2,1)}), bf16[8,256,256]{2,1,0:T(8,128)(2,1)S(1)}, u32[]{:S(2)}, u32[]{:S(2)}) %all-to-all-start.2) | async-done | bytes 1048608 | tf_op jit(solution)/shard_map/all_to_all | solution.py:415
  133.6 3.6 %all-to-all-start.1 = ((bf16[8,128,1024]{2,1,0:T(8,128)(2,1)}), bf16[8,128,1024]{2,1,0:T(8,128)(2,1)S(1)}, u32[]{:S(2)}, u32[]{:S(2)}) async-start(bf16[8,128,1024]{2,1,0:T(8,128)(2,1)} %bitcast.29), calls=%async_computation.1 | async-start | bytes 4194304 | tf_op jit(solution)/shard_map/all_to_all | solution.py:362
  137.2 0.9 collective-permute-start.6
  138.0 4.2 %collective-permute-done.3.refs_1_ = bf16[256,2048]{1,0:T(8,128)(2,1)} collective-permute-done((bf16[256,2048]{1,0:T(8,128)(2,1)}, bf16[256,2048]{1,0:T(8,128)(2,1)}, u32[]{:S(2)}, u32[]{:S(2)}) %collective-permute-start.3) | collective-permute-done | bytes 1048608 | tf_op jit(solution)/shard_map/ppermute | solution.py:324
  142.3 4.0 %collective-permute-start.7 = (bf16[256,2048]{1,0:T(8,128)(2,1)}, bf16[256,2048]{1,0:T(8,128)(2,1)}, u32[]{:S(2)}, u32[]{:S(2)}) collective-permute-start(bf16[256,2048]{1,0:T(8,128)(2,1)} %collective-permute-done.3.refs_1_), channel_id=1, source_target_pairs={{0,1},{1,0},{2,3},{3,2},{4,5},{5,4},{6,7},{7,6},{8,9},{9,8},{10,11... | collective-permute-start | bytes 3145736 | tf_op jit(solution)/shard_map/ppermute | solution.py:327
  146.3 19.2 %collective-permute-done.4.refs_2_ = bf16[256,2048]{1,0:T(8,128)(2,1)} collective-permute-done((bf16[256,2048]{1,0:T(8,128)(2,1)}, bf16[256,2048]{1,0:T(8,128)(2,1)}, u32[]{:S(2)}, u32[]{:S(2)}) %collective-permute-start.4) | collective-permute-done | bytes 1048608 | tf_op jit(solution)/shard_map/ppermute | solution.py:324
  165.5 2.5 %collective-permute-start.8 = (bf16[256,2048]{1,0:T(8,128)(2,1)}, bf16[256,2048]{1,0:T(8,128)(2,1)}, u32[]{:S(2)}, u32[]{:S(2)}) collective-permute-start(bf16[256,2048]{1,0:T(8,128)(2,1)} %collective-permute-done.4.refs_2_), channel_id=1, source_target_pairs={{0,1},{1,0},{2,3},{3,2},{4,5},{5,4},{6,7},{7,6},{8,9},{9,8},{10,11... | collective-permute-start | bytes 3145736 | tf_op jit(solution)/shard_map/ppermute | solution.py:327
  168.0 1.5 shard_map.114
  169.5 1.1 collective-permute-done.8.refs_6_
  170.6 1.5 collective-permute-done.9.refs_7_
  172.1 7.5 %shard_map.107 = (bf16[128,2048]{1,0:T(8,128)(2,1)}, bf16[128,4096]{1,0:T(8,128)(2,1)}, bf16[128,2048]{1,0:T(8,128)(2,1)}) custom-call(s32[1]{0:T(128)} %bitcast.half_ref, s32[8]{0:T(128)S(1)} %stack.44.owner_ref, bf16[8,128,1024]{2,1,0:T(8,128)(2,1)S(1)} %all-to-all-done.1.home_ref, bf16[256,2048]{1,0:T(8,128)(2,1)} %refs_0_.2, ...), custom_call_target="tpu_custom_call" | custom-call | flops 1121976320 | bytes 4194304 | tf_op jit(solution)/shard_map/pallas_call | solution.py:363
  (30 shorter events, 0.5 us)
Async XLA Ops:
  3.7 6.4 %copy-start.4 = (f32[1,1,2048]{2,1,0:T(1,128)S(1)}, f32[1,1,2048]{2,1,0:T(1,128)}, u32[]{:S(2)}) copy-start(f32[1,1,2048]{2,1,0:T(1,128)} %param.12) | copy-start | bytes 24580
  3.7 51.8 %all-to-all-start = ((bf16[8,128,1536]{2,1,0:T(8,128)(2,1)}), bf16[8,128,1536]{2,1,0:T(8,128)(2,1)S(1)}, u32[]{:S(2)}, u32[]{:S(2)}) async-start(bf16[8,128,1536]{2,1,0:T(8,128)(2,1)} %shard_map.102), calls=%async_computation | async-start | bytes 6291456 | tf_op jit(solution)/shard_map/all_to_all | solution.py:314
  10.1 11.6 %collective-permute-start = (f32[8,128]{1,0:T(8,128)S(1)}, f32[8,128]{1,0:T(8,128)S(1)}, u32[]{:S(2)}, u32[]{:S(2)}) collective-permute-start(f32[8,128]{1,0:T(8,128)S(1)} %get-tuple-element.30), channel_id=1, source_target_pairs={{0,0},{8,96},{16,8},{24,104},{32,16},{40,112},{48,24},{56,120},{64... | collective-permute-start | bytes 12296 | tf_op jit(solution)/shard_map/ppermute | solution.py:303
  10.8 44.3 %collective-permute-start.1 = (f32[8,128]{1,0:T(8,128)S(1)}, f32[8,128]{1,0:T(8,128)S(1)}, u32[]{:S(2)}, u32[]{:S(2)}) collective-permute-start(f32[8,128]{1,0:T(8,128)S(1)} %get-tuple-element.31), channel_id=1, source_target_pairs={{0,96},{8,0},{16,104},{24,8},{32,112},{40,16},{48,120},{56,24},{64... | collective-permute-start | bytes 12296 | tf_op jit(solution)/shard_map/ppermute | solution.py:304
  20.2 42.7 %collective-permute-start.10 = (bf16[1,128,2048]{2,1,0:T(8,128)(2,1)}, bf16[1,128,2048]{2,1,0:T(8,128)(2,1)}, u32[]{:S(2)}, u32[]{:S(2)}) collective-permute-start(bf16[1,128,2048]{2,1,0:T(8,128)(2,1)} %refs_0_.3), channel_id=1, source_target_pairs={{0,32},{8,40},{16,48},{24,56},{32,0},{40,8},{48,16},{56,24},{1,33}... | collective-permute-start | bytes 1572872 | tf_op jit(solution)/shard_map/ppermute | solution.py:305
  21.4 41.6 %collective-permute-start.13 = (bf16[1,128,2048]{2,1,0:T(8,128)(2,1)}, bf16[1,128,2048]{2,1,0:T(8,128)(2,1)}, u32[]{:S(2)}, u32[]{:S(2)}) collective-permute-start(bf16[1,128,2048]{2,1,0:T(8,128)(2,1)} %refs_0_.3), channel_id=1, source_target_pairs={{0,16},{8,24},{16,0},{24,8},{32,48},{40,56},{48,32},{56,40},{1,17}... | collective-permute-start | bytes 1572872 | tf_op jit(solution)/shard_map/ppermute | solution.py:317
  57.8 11.9 %collective-permute-start.2 = (bf16[2,256,512]{2,1,0:T(8,128)(2,1)}, bf16[2,256,512]{2,1,0:T(8,128)(2,1)}, u32[]{:S(2)}, u32[]{:S(2)}) collective-permute-start(bf16[2,256,512]{2,1,0:T(8,128)(2,1)} %shard_map.104), channel_id=1, source_target_pairs={{0,96},{8,104},{16,112},{24,120},{32,64},{40,72},{48,80},{56,88},{... | collective-permute-start | bytes 1572872 | tf_op jit(solution)/shard_map/ppermute | solution.py:337
  59.7 22.0 %collective-permute-start.11 = (bf16[1,128,2048]{2,1,0:T(8,128)(2,1)}, bf16[1,128,2048]{2,1,0:T(8,128)(2,1)}, u32[]{:S(2)}, u32[]{:S(2)}) collective-permute-start(bf16[1,128,2048]{2,1,0:T(8,128)(2,1)} %refs_0_.3), channel_id=1, source_target_pairs={{0,8},{8,16},{16,24},{24,0},{32,40},{40,48},{48,56},{56,32},{1,9},... | collective-permute-start | bytes 1572872 | tf_op jit(solution)/shard_map/ppermute | solution.py:317
  59.9 21.9 %collective-permute-start.12 = (bf16[1,128,2048]{2,1,0:T(8,128)(2,1)}, bf16[1,128,2048]{2,1,0:T(8,128)(2,1)}, u32[]{:S(2)}, u32[]{:S(2)}) collective-permute-start(bf16[1,128,2048]{2,1,0:T(8,128)(2,1)} %refs_0_.3), channel_id=1, source_target_pairs={{0,24},{8,0},{16,8},{24,16},{32,56},{40,32},{48,40},{56,48},{1,25}... | collective-permute-start | bytes 1572872 | tf_op jit(solution)/shard_map/ppermute | solution.py:317
  62.9 22.5 %collective-permute-start.15 = (bf16[1,128,2048]{2,1,0:T(8,128)(2,1)}, bf16[1,128,2048]{2,1,0:T(8,128)(2,1)S(1)}, u32[]{:S(2)}, u32[]{:S(2)}) collective-permute-start(bf16[1,128,2048]{2,1,0:T(8,128)(2,1)} %collective-permute-done.10.refs_1_), channel_id=1, source_target_pairs={{0,8},{8,16},{16,24},{24,0},{32,40},{40,48},{48,56},{56,32},{1,9},... | collective-permute-start | bytes 1572872 | tf_op jit(solution)/shard_map/ppermute | solution.py:317
  63.0 25.7 %collective-permute-start.16 = (bf16[1,128,2048]{2,1,0:T(8,128)(2,1)}, bf16[1,128,2048]{2,1,0:T(8,128)(2,1)S(1)}, u32[]{:S(2)}, u32[]{:S(2)}) collective-permute-start(bf16[1,128,2048]{2,1,0:T(8,128)(2,1)} %collective-permute-done.10.refs_1_), channel_id=1, source_target_pairs={{0,24},{8,0},{16,8},{24,16},{32,56},{40,32},{48,40},{56,48},{1,25}... | collective-permute-start | bytes 1572872 | tf_op jit(solution)/shard_map/ppermute | solution.py:317
  69.7 12.0 %collective-permute-start.14 = (bf16[1,128,2048]{2,1,0:T(8,128)(2,1)}, bf16[1,128,2048]{2,1,0:T(8,128)(2,1)S(1)}, u32[]{:S(2)}, u32[]{:S(2)}) collective-permute-start(bf16[1,128,2048]{2,1,0:T(8,128)(2,1)} %collective-permute-done.13.refs_4_), channel_id=1, source_target_pairs={{0,32},{8,40},{16,48},{24,56},{32,0},{40,8},{48,16},{56,24},{1,33}... | collective-permute-start | bytes 1572872 | tf_op jit(solution)/shard_map/ppermute | solution.py:334
  88.7 1.8 %copy-start.2 = (bf16[1,128,2048]{2,1,0:T(8,128)(2,1)}, bf16[1,128,2048]{2,1,0:T(8,128)(2,1)S(1)}, u32[]{:S(2)}) copy-start(bf16[1,128,2048]{2,1,0:T(8,128)(2,1)S(1)} %collective-permute-done.16.refs_1_) | copy-start | bytes 1572868
  90.5 0.8 copy-start
  91.3 4.9 %collective-permute-start.17 = (bf16[4,256,256]{2,1,0:T(8,128)(2,1)}, bf16[4,256,256]{2,1,0:T(8,128)(2,1)S(1)}, u32[]{:S(2)}, u32[]{:S(2)}) collective-permute-start(bf16[4,256,256]{2,1,0:T(8,128)(2,1)} %shard_map.110), channel_id=1, source_target_pairs={{0,1},{1,0},{2,3},{3,2},{4,5},{5,4},{6,7},{7,6},{8,9},{9,8},{10,11... | collective-permute-start | bytes 1572872 | tf_op jit(solution)/shard_map/ppermute | solution.py:397
  93.1 1.0 copy-start.1
  94.2 1.0 copy-start.3
  96.3 6.5 %collective-permute-start.18 = (bf16[256,256]{1,0:T(8,128)(2,1)S(1)}, bf16[256,256]{1,0:T(8,128)(2,1)S(1)}, u32[]{:S(2)}, u32[]{:S(2)}) collective-permute-start(bf16[256,256]{1,0:T(8,128)(2,1)S(1)} %get-tuple-element.25), channel_id=1, source_target_pairs={{0,2},{2,4},{4,6},{6,0},{1,3},{3,5},{5,7},{7,1},{8,10},{10,12},{12... | collective-permute-start | bytes 393224 | tf_op jit(solution)/shard_map/ppermute | solution.py:409
  97.8 8.8 %collective-permute-start.19 = (bf16[256,256]{1,0:T(8,128)(2,1)S(1)}, bf16[256,256]{1,0:T(8,128)(2,1)S(1)}, u32[]{:S(2)}, u32[]{:S(2)}) collective-permute-start(bf16[256,256]{1,0:T(8,128)(2,1)S(1)} %get-tuple-element.26), channel_id=1, source_target_pairs={{0,4},{2,6},{4,0},{6,2},{1,5},{3,7},{5,1},{7,3},{8,12},{10,14},{12... | collective-permute-start | bytes 393224 | tf_op jit(solution)/shard_map/ppermute | solution.py:409
  100.2 6.4 %collective-permute-start.20 = (bf16[256,256]{1,0:T(8,128)(2,1)S(1)}, bf16[256,256]{1,0:T(8,128)(2,1)S(1)}, u32[]{:S(2)}, u32[]{:S(2)}) collective-permute-start(bf16[256,256]{1,0:T(8,128)(2,1)S(1)} %get-tuple-element.27), channel_id=1, source_target_pairs={{0,6},{2,0},{4,2},{6,4},{1,7},{3,1},{5,3},{7,5},{8,14},{10,8},{12,... | collective-permute-start | bytes 393224 | tf_op jit(solution)/shard_map/ppermute | solution.py:409
  106.7 6.3 %collective-permute-start.21 = (bf16[256,256]{1,0:T(8,128)(2,1)S(1)}, bf16[256,256]{1,0:T(8,128)(2,1)S(1)}, u32[]{:S(2)}, u32[]{:S(2)}) collective-permute-start(bf16[256,256]{1,0:T(8,128)(2,1)S(1)} %get-tuple-element.29), channel_id=1, source_target_pairs={{0,96},{8,104},{16,112},{24,120},{32,64},{40,72},{48,80},{56,88},{... | collective-permute-start | bytes 393224 | tf_op jit(solution)/shard_map/ppermute | solution.py:413
  114.1 19.5 %all-to-all-start.2 = ((bf16[8,256,256]{2,1,0:T(8,128)(2,1)}), bf16[8,256,256]{2,1,0:T(8,128)(2,1)S(1)}, u32[]{:S(2)}, u32[]{:S(2)}) async-start(bf16[8,256,256]{2,1,0:T(8,128)(2,1)} %shard_map.113), calls=%async_computation.2 | async-start | bytes 2097152 | tf_op jit(solution)/shard_map/all_to_all | solution.py:415
  117.7 24.6 %collective-permute-start.3 = (bf16[256,2048]{1,0:T(8,128)(2,1)}, bf16[256,2048]{1,0:T(8,128)(2,1)}, u32[]{:S(2)}, u32[]{:S(2)}) collective-permute-start(bf16[256,2048]{1,0:T(8,128)(2,1)} %refs_0_.2), channel_id=1, source_target_pairs={{0,2},{2,4},{4,6},{6,0},{1,3},{3,5},{5,7},{7,1},{8,10},{10,12},{12... | collective-permute-start | bytes 3145736 | tf_op jit(solution)/shard_map/ppermute | solution.py:324
  118.2 47.2 %collective-permute-start.4 = (bf16[256,2048]{1,0:T(8,128)(2,1)}, bf16[256,2048]{1,0:T(8,128)(2,1)}, u32[]{:S(2)}, u32[]{:S(2)}) collective-permute-start(bf16[256,2048]{1,0:T(8,128)(2,1)} %refs_0_.2), channel_id=1, source_target_pairs={{0,4},{2,6},{4,0},{6,2},{1,5},{3,7},{5,1},{7,3},{8,12},{10,14},{12... | collective-permute-start | bytes 3145736 | tf_op jit(solution)/shard_map/ppermute | solution.py:324
  121.0 46.9 %collective-permute-start.5 = (bf16[256,2048]{1,0:T(8,128)(2,1)}, bf16[256,2048]{1,0:T(8,128)(2,1)}, u32[]{:S(2)}, u32[]{:S(2)}) collective-permute-start(bf16[256,2048]{1,0:T(8,128)(2,1)} %refs_0_.2), channel_id=1, source_target_pairs={{0,6},{2,0},{4,2},{6,4},{1,7},{3,1},{5,3},{7,5},{8,14},{10,8},{12,... | collective-permute-start | bytes 3145736 | tf_op jit(solution)/shard_map/ppermute | solution.py:324
  133.6 38.5 %all-to-all-start.1 = ((bf16[8,128,1024]{2,1,0:T(8,128)(2,1)}), bf16[8,128,1024]{2,1,0:T(8,128)(2,1)S(1)}, u32[]{:S(2)}, u32[]{:S(2)}) async-start(bf16[8,128,1024]{2,1,0:T(8,128)(2,1)} %bitcast.29), calls=%async_computation.1 | async-start | bytes 4194304 | tf_op jit(solution)/shard_map/all_to_all | solution.py:362
  137.2 32.3 %collective-permute-start.6 = (bf16[256,2048]{1,0:T(8,128)(2,1)}, bf16[256,2048]{1,0:T(8,128)(2,1)}, u32[]{:S(2)}, u32[]{:S(2)}) collective-permute-start(bf16[256,2048]{1,0:T(8,128)(2,1)} %refs_0_.2), channel_id=1, source_target_pairs={{0,1},{1,0},{2,3},{3,2},{4,5},{5,4},{6,7},{7,6},{8,9},{9,8},{10,11... | collective-permute-start | bytes 3145736 | tf_op jit(solution)/shard_map/ppermute | solution.py:327
  142.3 27.2 %collective-permute-start.7 = (bf16[256,2048]{1,0:T(8,128)(2,1)}, bf16[256,2048]{1,0:T(8,128)(2,1)}, u32[]{:S(2)}, u32[]{:S(2)}) collective-permute-start(bf16[256,2048]{1,0:T(8,128)(2,1)} %collective-permute-done.3.refs_1_), channel_id=1, source_target_pairs={{0,1},{1,0},{2,3},{3,2},{4,5},{5,4},{6,7},{7,6},{8,9},{9,8},{10,11... | collective-permute-start | bytes 3145736 | tf_op jit(solution)/shard_map/ppermute | solution.py:327
  165.5 5.1 %collective-permute-start.8 = (bf16[256,2048]{1,0:T(8,128)(2,1)}, bf16[256,2048]{1,0:T(8,128)(2,1)}, u32[]{:S(2)}, u32[]{:S(2)}) collective-permute-start(bf16[256,2048]{1,0:T(8,128)(2,1)} %collective-permute-done.4.refs_2_), channel_id=1, source_target_pairs={{0,1},{1,0},{2,3},{3,2},{4,5},{5,4},{6,7},{7,6},{8,9},{9,8},{10,11... | collective-permute-start | bytes 3145736 | tf_op jit(solution)/shard_map/ppermute | solution.py:327
  167.9 4.1 %collective-permute-start.9 = (bf16[256,2048]{1,0:T(8,128)(2,1)}, bf16[256,2048]{1,0:T(8,128)(2,1)}, u32[]{:S(2)}, u32[]{:S(2)}) collective-permute-start(bf16[256,2048]{1,0:T(8,128)(2,1)} %collective-permute-done.5.refs_3_), channel_id=1, source_target_pairs={{0,1},{1,0},{2,3},{3,2},{4,5},{5,4},{6,7},{7,6},{8,9},{9,8},{10,11... | collective-permute-start | bytes 3145736 | tf_op jit(solution)/shard_map/ppermute | solution.py:327
